TPU v7x, 32 devices: a whole 2x2x4 slice. The times are simulated.
32 devices in a mesh: sp: 16 (over z, y, core), tp: 2 (over x).
Axes of the slice: x: 2, y: 2, z: 4, core: 2. Of those that a mesh axis runs over, the one named last changes fastest.
Arguments:
- tokens: bfloat16 [4096, 2048], P('sp'), may hold values from -28 to 28
- query_weight: bfloat16 [2048, 1536], P(None, 'tp'), may hold values from -0.125 to 0.125
- key_weight: bfloat16 [2048, 1536], P(None, 'tp'), may hold values from -0.125 to 0.125
- value_weight: bfloat16 [2048, 1536], P(None, 'tp'), may hold values from -0.125 to 0.125
- out_weight: bfloat16 [512, 2048], P(None, 'tp'), may hold values from -1 to 1
Outputs:
- mixed: bfloat16 [4096, 2048], P('sp', 'tp')
- total_log: float32 [4, 4096], P('tp', 'sp')
All inputs are finite; a program needn't handle non-finite values.
Results may differ from a plain program's by a relative error of at most 0.012.
The roundings to bfloat16 on the way count: a program that leaves them out, or rounds other values in their place, can miss the bound.
Values may be sent and summed in bfloat16 or wider, within the bound.
A program may use at most 64 MiB of HBM per device.

v0:
```python
import functools
import jax
import jax.numpy as jnp
from jax import lax
from jax.experimental import pallas as pl
from jax.experimental.pallas import tpu as pltpu
from jax.sharding import PartitionSpec as P

HEADS = 4
HEAD_DIM = 128
NEAR_WINDOW = 128
MIDDLE_WINDOW = 512
MIDDLE_DILATION = 4
FAR_WINDOW = 2048
FAR_DILATION = 16


def from_behind(block, axis, distance):
    devices = range(lax.axis_size(axis))
    route = [(i - distance, i) for i in devices if i - distance in devices]
    return lax.ppermute(block, axis, route)


def window_table():
    return ((NEAR_WINDOW, 1), (MIDDLE_WINDOW, MIDDLE_DILATION), (FAR_WINDOW, FAR_DILATION))


def tail_counts(row_count, distance, held_rows):
    counts = []
    for entry, available in zip(window_table(), held_rows):
        counts.append(max(0, min(available, entry[0] - (distance - 1) * row_count)))
    return counts


def pack_tails(sources, counts):
    selected = [
        source[:, source.shape[1] - amount :]
        for source, amount in zip(sources, counts)
        if amount > 0
    ]
    return jnp.concatenate(selected, axis=1)


def unpack_rows(packed, counts):
    result = []
    cursor = 0
    for amount in counts:
        result.append(packed[:, cursor : cursor + amount])
        cursor = cursor + amount
    return result


def attend_group(group_queries, buffer, window, dilation, first_key, slopes_here):
    row_count = group_queries.shape[0]
    head_count = group_queries.shape[1]
    head_size = group_queries.shape[2]
    query_split = group_queries.reshape(row_count // dilation, dilation, head_count, head_size)
    key_split = buffer[0].reshape(-1, dilation, head_count, head_size)
    value_split = buffer[1].reshape(-1, dilation, head_count, head_size)
    scores = jnp.einsum(
        "mrhe,nrhe->rhmn", query_split, key_split, preferred_element_type=jnp.float32
    ) * head_size ** (-0.5)
    grid_shape = (row_count // dilation, key_split.shape[0])
    query_slot = lax.broadcasted_iota(jnp.int32, grid_shape, 0)
    key_slot = lax.broadcasted_iota(jnp.int32, grid_shape, 1)
    spacing = query_slot + window // dilation - key_slot
    residue = lax.broadcasted_iota(jnp.int32, (dilation, 1, 1), 0)
    key_place = first_key + residue + dilation * key_slot[None]
    valid = (spacing[None] >= 0) & (spacing[None] <= window // dilation) & (key_place >= 0)
    scores = (
        scores
        - slopes_here[None, :, None, None] * (dilation * spacing).astype(jnp.float32)[None, None]
    )
    masked = jnp.where(valid[:, None], scores, -jnp.inf)
    highest = jnp.max(masked, axis=-1, keepdims=True)
    log_sum = highest + jnp.log(jnp.sum(jnp.exp(masked - highest), axis=-1, keepdims=True))
    probs = jnp.exp(masked - log_sum).astype(jnp.bfloat16)
    attended = jnp.einsum("rhmn,nrhe->mrhe", probs, value_split, preferred_element_type=jnp.float32)
    attended = attended.reshape(row_count, head_count, head_size)
    log_rows = jnp.transpose(log_sum[..., 0], (1, 2, 0)).reshape(head_count, row_count)
    return (attended, log_rows)


def local(tokens, query_weight, key_weight, value_weight, out_weight):
    rows_here = tokens.shape[0]
    local_heads = query_weight.shape[1] // (3 * HEAD_DIM)

    def project(weight_matrix):
        product = jnp.dot(tokens, weight_matrix, preferred_element_type=jnp.float32)
        return product.astype(jnp.bfloat16).reshape(rows_here, local_heads, 3, HEAD_DIM)

    queries = project(query_weight)
    keys_all = project(key_weight)
    values_all = project(value_weight)
    table = window_table()
    own = [jnp.stack((keys_all[:, :, index], values_all[:, :, index])) for index in range(3)]
    held = list(own)
    span_now = 1
    while span_now * rows_here < FAR_WINDOW + rows_here:
        counts = tail_counts(rows_here, span_now, [item.shape[1] for item in held])
        packed = pack_tails(held, counts)
        arrived = from_behind(packed, "sp", span_now)
        pieces_in = unpack_rows(arrived, counts)
        for index in range(3):
            if counts[index] > 0:
                joined = jnp.concatenate((pieces_in[index], held[index]), axis=1)
                held[index] = joined
        span_now = span_now * 2
    priors = [held[index][:, : table[index][0]] for index in range(3)]
    position_start = lax.axis_index("sp") * rows_here
    head_ids = (
        lax.axis_index("tp") * local_heads + jnp.arange(local_heads, dtype=jnp.int32)
    ).astype(jnp.float32)
    outputs = []
    logs = []
    for index, (window, dilation) in enumerate(table):
        buffer = jnp.concatenate((priors[index], own[index]), axis=1)
        slopes_here = 2.0 ** (3.0 - 8.0 * (head_ids + 1.0) / HEADS) / window
        attended, log_rows = attend_group(
            queries[:, :, index], buffer, window, dilation, position_start - window, slopes_here
        )
        outputs.append(attended)
        logs.append(log_rows)
    stacked_logs = jnp.stack(logs)
    highest = jnp.max(stacked_logs, axis=0)
    total_log = highest + jnp.log(jnp.sum(jnp.exp(stacked_logs - highest), axis=0))
    mixing = jnp.exp(stacked_logs - total_log)
    merged = outputs[0] * jnp.transpose(mixing[0])[:, :, None]
    merged = merged + outputs[1] * jnp.transpose(mixing[1])[:, :, None]
    merged = merged + outputs[2] * jnp.transpose(mixing[2])[:, :, None]
    merged = merged.astype(jnp.bfloat16).reshape(rows_here, local_heads * HEAD_DIM)
    mixed = jnp.dot(
        lax.all_gather(merged, "tp", axis=1, tiled=True),
        out_weight,
        preferred_element_type=jnp.float32,
    ).astype(jnp.bfloat16)
    return (mixed, total_log)


MESH = pl.DeviceIdType.MESH
MASKED = -1e30


def attend(query, key, value, slope, distance, valid):
    scores = lax.dot_general(
        query, key, (((1,), (1,)), ((), ())), preferred_element_type=jnp.float32
    ) * HEAD_DIM ** (-0.5)
    scores = jnp.where(valid, scores - slope * distance, MASKED)
    highest = jnp.max(scores, axis=-1, keepdims=True)
    weights = jnp.exp(scores - highest)
    total = jnp.sum(weights, axis=-1, keepdims=True)
    probs = (weights * (1.0 / total)).astype(jnp.bfloat16)
    attended = jnp.dot(probs, value, preferred_element_type=jnp.float32)
    return attended, highest + jnp.log(total)


def swap_matrix(rows, width):
    shift = width.bit_length() - 1
    row = lax.broadcasted_iota(jnp.int32, (rows, rows), 0)
    column = lax.broadcasted_iota(jnp.int32, (rows, rows), 1)
    source = ((row & (width - 1)) << shift) + (row >> shift)
    return jnp.where(column == source, 1.0, 0.0).astype(jnp.bfloat16)


def kernel(
    n, n_tp, local_heads,
    tok_hbm, wq_hbm, wk_hbm, wv_hbm,
    both_ref, totals_ref,
    tok, weight, far_send, far_held, back_send, back_held,
    mid_query, mid_own, mid_held, via_held, near_query, near_own, near_held,
    merged_own, merged_held,
    load_sem, far_ssem, far_rsem, back_ssem, back_rsem,
    mid_ssem, mid_rsem, via_ssem, via_rsem, near_ssem, near_rsem, merged_ssem, merged_rsem,
):
    me = lax.axis_index("sp")
    tp = lax.axis_index("tp")
    rows = tok.shape[0]
    width = local_heads * HEAD_DIM
    chunk = rows // n
    peer = 1 - tp

    loads = {}
    tok_load = pltpu.make_async_copy(tok_hbm, tok, load_sem.at[0])
    tok_load.start()
    count = 1
    for group in (2, 1, 0):
        loads[group] = []
        for part, source in enumerate((wq_hbm, wk_hbm, wv_hbm)):
            for head in range(local_heads):
                copy = pltpu.make_async_copy(
                    source.at[:, pl.ds((head * 3 + group) * HEAD_DIM, HEAD_DIM)],
                    weight.at[group, :, pl.ds((part * local_heads + head) * HEAD_DIM, HEAD_DIM)],
                    load_sem.at[count],
                )
                copy.start()
                loads[group].append(copy)
                count += 1

    barrier = pltpu.get_barrier_semaphore()

    def greet(k, carry):
        pl.semaphore_signal(barrier, inc=1, device_id=(lax.rem(me + k, n), tp), device_id_type=MESH)
        return carry

    lax.fori_loop(1, n, greet, 0)
    pl.semaphore_signal(barrier, inc=1, device_id=(me, peer), device_id_type=MESH)

    @pl.when(me < 2)
    def _():
        mid_held[0] = jnp.zeros((2, rows, width), jnp.bfloat16)

    @pl.when(me < 1)
    def _():
        mid_held[1] = jnp.zeros((2, rows, width), jnp.bfloat16)
        near_held[...] = jnp.zeros((NEAR_WINDOW, 2 * width), jnp.bfloat16)

    def project(group, first, extent):
        return jnp.dot(
            tok[...], weight[group, :, first : first + extent], preferred_element_type=jnp.float32
        ).astype(jnp.bfloat16)

    def at_rows(index):
        return pl.ds(pl.multiple_of(index * chunk, chunk), chunk)

    swap = swap_matrix(rows, n)
    tok_load.wait()
    for part in range(3):
        for copy in loads[2][part * local_heads : (part + 1) * local_heads]:
            copy.wait()
        block = project(2, part * width, width)
        far_send[:, part * width : (part + 1) * width] = jnp.dot(
            swap, block, preferred_element_type=jnp.float32
        ).astype(jnp.bfloat16)
    far_held[at_rows(me), :] = far_send[at_rows(me), :]

    def exchange(source, target, ssem, rsem, k, outgoing):
        to = lax.rem(me + k, n)
        come = lax.rem(me + n - k, n)
        return pltpu.make_async_remote_copy(
            src_ref=source.at[at_rows(to)],
            dst_ref=target.at[at_rows(me if outgoing else come)],
            send_sem=ssem.at[k],
            recv_sem=rsem.at[k],
            device_id=(to, tp),
            device_id_type=MESH,
        )

    def far_copy(k, outgoing):
        return exchange(far_send, far_held, far_ssem, far_rsem, k, outgoing)

    def back_copy(k, outgoing):
        return exchange(back_send, back_held, back_ssem, back_rsem, k, outgoing)

    def each(action):
        def step(k, carry):
            action(k)
            return carry

        lax.fori_loop(1, n, step, 0)

    pl.semaphore_wait(barrier, n)
    each(lambda k: far_copy(k, True).start())

    for copy in loads[1]:
        copy.wait()
    mid_own[0] = project(1, width, width)
    mid_own[1] = project(1, 2 * width, width)

    def mid_copy(slot, hop, source, part, sem):
        return pltpu.make_async_remote_copy(
            src_ref=source,
            dst_ref=mid_held.at[slot, part],
            send_sem=mid_ssem.at[sem, part],
            recv_sem=mid_rsem.at[slot, part],
            device_id=(lax.rem(me + hop + n, n), tp),
            device_id_type=MESH,
        )

    def via_copy():
        return pltpu.make_async_remote_copy(
            src_ref=mid_own.at[1],
            dst_ref=via_held,
            send_sem=via_ssem,
            recv_sem=via_rsem,
            device_id=(lax.rem(me + -2 + n, n), tp),
            device_id_type=MESH,
        )

    def near_copy():
        return pltpu.make_async_remote_copy(
            src_ref=near_own.at[pl.ds(rows - NEAR_WINDOW, NEAR_WINDOW)],
            dst_ref=near_held,
            send_sem=near_ssem,
            recv_sem=near_rsem,
            device_id=(lax.rem(me + 1, n), tp),
            device_id_type=MESH,
        )

    even = lax.rem(me, 2) == 0
    sends_one = me + 1 < n
    sends_two = even & (me + 2 < n)
    relays = even & (me >= 1)

    crosses = (lax.rem(me, 4) >= 2) & sends_one & (me + 4 - lax.rem(me, 4) < n)
    forwards = (lax.rem(me, 4) < 2) & (me + 4 - lax.rem(me, 4) < n)
    forward_even = forwards & even
    forward_odd = forwards & jnp.logical_not(even)

    @pl.when(crosses)
    def _():
        via_copy().start()

    @pl.when(sends_two)
    def _():
        mid_copy(0, 2, mid_own.at[0], 0, 0).start()

    @pl.when(sends_one)
    def _():
        mid_copy(1, 1, mid_own.at[0], 0, 1).start()

    @pl.when(sends_two & jnp.logical_not(crosses))
    def _():
        mid_copy(0, 2, mid_own.at[1], 1, 0).start()

    own_value_one = sends_one & jnp.logical_not(crosses & jnp.logical_not(even))

    @pl.when(own_value_one)
    def _():
        mid_copy(1, 1, mid_own.at[1], 1, 1).start()

    for copy in loads[0]:
        copy.wait()
    near_own[:, :width] = project(0, width, width)
    near_own[:, width:] = project(0, 2 * width, width)

    @pl.when(sends_one)
    def _():
        near_copy().start()

    mid_query[...] = project(1, 0, width)
    near_query[...] = project(0, 0, width)

    def slope_of(head, window):
        number = tp * local_heads + head
        slope = jnp.float32(0.0)
        for index in range(HEADS):
            value = 2.0 ** (3.0 - 8.0 * (index + 1.0) / HEADS) / window
            slope = jnp.where(number == index, jnp.float32(value), slope)
        return slope

    def spacing(row_count, key_count, offset):
        row = lax.broadcasted_iota(jnp.int32, (row_count, key_count), 0)
        column = lax.broadcasted_iota(jnp.int32, (row_count, key_count), 1)
        return row + offset - column, column

    each(lambda k: far_copy(k, False).wait_recv())

    @pl.when(forwards)
    def _():
        via_copy().wait_recv()

    @pl.when(forward_even)
    def _():
        mid_copy(0, 4, via_held, 1, 3).start()

    @pl.when(forward_odd)
    def _():
        mid_copy(1, 3, via_held, 1, 3).start()

    reach = FAR_WINDOW // FAR_DILATION
    apart, column = spacing(rows, rows, 0)
    valid = (apart >= 0) & (apart <= reach)
    distance = (apart * FAR_DILATION).astype(jnp.float32)
    lane = lax.broadcasted_iota(jnp.int32, (rows, HEAD_DIM), 1)
    packed = jnp.zeros((rows, HEAD_DIM), jnp.float32)
    for head in range(local_heads):
        at = head * HEAD_DIM
        attended, log_sum = attend(
            far_held[:, at : at + HEAD_DIM],
            far_held[:, width + at : width + at + HEAD_DIM],
            far_held[:, 2 * width + at : 2 * width + at + HEAD_DIM],
            slope_of(head, FAR_WINDOW), distance, valid,
        )
        back_send[:, at : at + HEAD_DIM] = attended.astype(jnp.bfloat16)
        rest = log_sum
        for term in range(3):
            piece = rest.astype(jnp.bfloat16).astype(jnp.float32)
            packed = jnp.where(lane == 3 * head + term, piece, packed)
            rest = rest - piece
    back_send[:, width:] = packed.astype(jnp.bfloat16)
    back_held[at_rows(me), :] = back_send[at_rows(me), :]
    each(lambda k: back_copy(k, True).start())

    @pl.when(me >= 1)
    def _():
        near_copy().wait_recv()
        mid_copy(1, 1, mid_own.at[0], 0, 1).wait_recv()
        mid_copy(1, 1, mid_own.at[1], 1, 1).wait_recv()

    @pl.when(relays)
    def _():
        mid_copy(0, 1, mid_held.at[1, 0], 0, 2).start()
        mid_copy(0, 1, mid_held.at[1, 1], 1, 2).start()

    apart, column = spacing(rows, NEAR_WINDOW + rows, NEAR_WINDOW)
    valid = (apart >= 0) & (apart <= NEAR_WINDOW) & (column + me * rows >= NEAR_WINDOW)
    distance = apart.astype(jnp.float32)
    near = []
    for head in range(local_heads):
        at = head * HEAD_DIM
        key = jnp.concatenate((near_held[:, at : at + HEAD_DIM], near_own[:, at : at + HEAD_DIM]), axis=0)
        at2 = width + at
        value = jnp.concatenate((near_held[:, at2 : at2 + HEAD_DIM], near_own[:, at2 : at2 + HEAD_DIM]), axis=0)
        near.append(attend(near_query[:, at : at + HEAD_DIM], key, value, slope_of(head, NEAR_WINDOW), distance, valid))

    @pl.when(me >= 2)
    def _():
        mid_copy(0, 2, mid_own.at[0], 0, 0).wait_recv()
        mid_copy(0, 2, mid_own.at[1], 1, 0).wait_recv()

    apart, column = spacing(rows, MIDDLE_WINDOW + rows, MIDDLE_WINDOW)
    valid = (apart >= 0) & (apart <= MIDDLE_WINDOW) & ((apart & (MIDDLE_DILATION - 1)) == 0)
    valid = valid & (column + me * rows >= MIDDLE_WINDOW)
    distance = apart.astype(jnp.float32)
    middle = []
    for head in range(local_heads):
        at = head * HEAD_DIM
        key = jnp.concatenate([x[:, at : at + HEAD_DIM] for x in (mid_held[0, 0], mid_held[1, 0], mid_own[0])], axis=0)
        value = jnp.concatenate([x[:, at : at + HEAD_DIM] for x in (mid_held[0, 1], mid_held[1, 1], mid_own[1])], axis=0)
        middle.append(attend(mid_query[:, at : at + HEAD_DIM], key, value, slope_of(head, MIDDLE_WINDOW), distance, valid))

    each(lambda k: back_copy(k, False).wait_recv())
    far = jnp.dot(swap, back_held[...], preferred_element_type=jnp.float32)
    parts = far[:, width:]
    totals = jnp.zeros((rows, HEAD_DIM), jnp.float32)
    for head in range(local_heads):
        at = head * HEAD_DIM
        far_log = jnp.sum(
            jnp.where((lane >= 3 * head) & (lane < 3 * head + 3), parts, 0.0), axis=-1, keepdims=True
        )
        near_log, middle_log = near[head][1], middle[head][1]
        highest = jnp.maximum(jnp.maximum(near_log, middle_log), far_log)
        total = highest + jnp.log(
            jnp.exp(near_log - highest) + jnp.exp(middle_log - highest) + jnp.exp(far_log - highest)
        )
        merged = near[head][0] * jnp.exp(near_log - total)
        merged = merged + middle[head][0] * jnp.exp(middle_log - total)
        merged = merged + far[:, at : at + HEAD_DIM] * jnp.exp(far_log - total)
        merged_own[:, at : at + HEAD_DIM] = merged.astype(jnp.bfloat16)
        totals = jnp.where(lane == head, total, totals)

    swap_merged = pltpu.make_async_remote_copy(
        src_ref=merged_own,
        dst_ref=merged_held,
        send_sem=merged_ssem,
        recv_sem=merged_rsem,
        device_id=(me, peer),
        device_id_type=MESH,
    )
    swap_merged.start()
    totals_ref[...] = totals
    both_ref[tp] = merged_own[...]
    swap_merged.wait_recv()
    both_ref[peer] = merged_held[...]

    swap_merged.wait_send()
    each(lambda k: far_copy(k, True).wait_send())
    each(lambda k: back_copy(k, True).wait_send())

    @pl.when(crosses)
    def _():
        via_copy().wait_send()

    @pl.when(sends_two)
    def _():
        mid_copy(0, 2, mid_own.at[0], 0, 0).wait_send()

    @pl.when(sends_two & jnp.logical_not(crosses))
    def _():
        mid_copy(0, 2, mid_own.at[1], 1, 0).wait_send()

    @pl.when(sends_one)
    def _():
        mid_copy(1, 1, mid_own.at[0], 0, 1).wait_send()
        near_copy().wait_send()

    @pl.when(own_value_one)
    def _():
        mid_copy(1, 1, mid_own.at[1], 1, 1).wait_send()

    @pl.when(forward_even)
    def _():
        mid_copy(0, 4, via_held, 1, 3).wait_send()

    @pl.when(forward_odd)
    def _():
        mid_copy(1, 3, via_held, 1, 3).wait_send()

    @pl.when(relays)
    def _():
        mid_copy(0, 1, mid_held.at[1, 0], 0, 2).wait_send()
        mid_copy(0, 1, mid_held.at[1, 1], 1, 2).wait_send()


def mix(both_ref, totals_ref, wo_ref, mixed_ref, log_ref):
    width = both_ref.shape[2]
    product = jnp.dot(both_ref[0], wo_ref[:width], preferred_element_type=jnp.float32)
    product = product + jnp.dot(both_ref[1], wo_ref[width:], preferred_element_type=jnp.float32)
    mixed_ref[...] = product.astype(jnp.bfloat16)
    log_ref[...] = jnp.transpose(totals_ref[...])[: log_ref.shape[0]]


def fused(n, n_tp, tokens, query_weight, key_weight, value_weight, out_weight):
    rows, depth = tokens.shape
    columns = query_weight.shape[1]
    local_heads = columns // (3 * HEAD_DIM)
    width = local_heads * HEAD_DIM
    dma = pltpu.SemaphoreType.DMA
    half = jnp.bfloat16
    both, totals = pl.pallas_call(
        functools.partial(kernel, n, n_tp, local_heads),
        out_shape=(
            jax.ShapeDtypeStruct((n_tp, rows, width), half),
            jax.ShapeDtypeStruct((rows, HEAD_DIM), jnp.float32),
        ),
        in_specs=[pl.BlockSpec(memory_space=pl.ANY)] * 4,
        out_specs=(pl.BlockSpec(memory_space=pltpu.VMEM), pl.BlockSpec(memory_space=pltpu.VMEM)),
        scratch_shapes=[
            pltpu.VMEM((rows, depth), half),
            pltpu.VMEM((3, depth, columns), half),
            pltpu.VMEM((rows, columns), half),
            pltpu.VMEM((rows, columns), half),
            pltpu.VMEM((rows, width + HEAD_DIM), half),
            pltpu.VMEM((rows, width + HEAD_DIM), half),
            pltpu.VMEM((rows, width), half),
            pltpu.VMEM((2, rows, width), half),
            pltpu.VMEM((2, 2, rows, width), half),
            pltpu.VMEM((rows, width), half),
            pltpu.VMEM((rows, width), half),
            pltpu.VMEM((rows, 2 * width), half),
            pltpu.VMEM((NEAR_WINDOW, 2 * width), half),
            pltpu.VMEM((rows, width), half),
            pltpu.VMEM((rows, width), half),
            dma((1 + 9 * local_heads,)),
            dma((n,)), dma((n,)), dma((n,)), dma((n,)),
            dma((4, 2)), dma((2, 2)), dma(()), dma(()), dma(()), dma(()), dma(()), dma(()),
        ],
        compiler_params=pltpu.CompilerParams(
            collective_id=0, has_side_effects=True, vmem_limit_bytes=54000 * 1024
        ),
    )(tokens, query_weight, key_weight, value_weight)
    whole = pl.BlockSpec(memory_space=pltpu.VMEM)
    return pl.pallas_call(
        mix,
        out_shape=(
            jax.ShapeDtypeStruct((rows, out_weight.shape[1]), half),
            jax.ShapeDtypeStruct((local_heads, rows), jnp.float32),
        ),
        in_specs=[whole] * 3,
        out_specs=(whole, whole),
        compiler_params=pltpu.CompilerParams(vmem_limit_bytes=16000 * 1024),
    )(both, totals, out_weight)


def solution(mesh):
    n, n_tp = mesh.shape["sp"], mesh.shape["tp"]
    if n == FAR_DILATION and n_tp == 2:
        body = functools.partial(fused, n, n_tp)
    else:
        body = local
    return jax.shard_map(
        body,
        mesh=mesh,
        in_specs=(P("sp", None), P(None, "tp"), P(None, "tp"), P(None, "tp"), P(None, "tp")),
        out_specs=(P("sp", "tp"), P("tp", "sp")),
        check_vma=False,
    )
```

profile of v0, /device:TPU:16, one launch (start us, length us, event | category | flops | bytes accessed | tf_op | source)
XLA Modules:
  0.0 33.4 jit_solution(6030548355033686006)
XLA Ops:
  0.6 0.0 copy-start
  0.6 31.5 %shard_map.68 = (bf16[2,256,256]{2,1,0:T(8,128)(2,1)S(1)}, f32[256,128]{1,0:T(8,128)S(1)}) custom-call(bf16[256,2048]{1,0:T(8,128)(2,1)} %tok_hbm.1, bf16[2048,768]{1,0:T(8,128)(2,1)} %wq_hbm.1, bf16[2048,768]{1,0:T(8,128)(2,1)} %wk_hbm.1, bf16[2048,768]{1,0:T(8,128)(2,1)} %wv_hbm.1), custom_call_target="tpu_custom_call" | custom-call | tf_op jit(solution)/shard_map/pallas_call | solution.py:520
  32.2 0.0 copy-done
  32.2 1.2 %shard_map.69 = (bf16[256,1024]{1,0:T(8,128)(2,1)}, f32[2,256]{1,0:T(2,128)}) custom-call(bf16[2,256,256]{2,1,0:T(8,128)(2,1)S(1)} %get-tuple-element.4.both_ref, f32[256,128]{1,0:T(8,128)S(1)} %get-tuple-element.5.totals_ref, bf16[512,1024]{1,0:T(8,128)(2,1)S(1)} %copy-done), custom_call_target="tpu_custom_call" | custom-call | tf_op jit(solution)/shard_map/pallas_call | solution.py:553
Async XLA Ops:
  0.6 31.6 %copy-start = (bf16[512,1024]{1,0:T(8,128)(2,1)S(1)}, bf16[512,1024]{1,0:T(8,128)(2,1)}, u32[]{:S(2)}) copy-start(bf16[512,1024]{1,0:T(8,128)(2,1)} %wo_ref.1) | copy-start | bytes 3145732
where the time goes:
time: 33.7 us; the launch traced here: 33.4 us
  Pallas kernels  32.8 us (97%)
  between operations  0.65 us (2%)
    pallas_call x1, Pallas kernels, fused(): pl.pallas_call(functools.partial(kernel, n, n_tp, local_heads), out_shape...  31.5 us
    pallas_call x1, Pallas kernels, fused(): pl.pallas_call(mix, out_shape=(jax.ShapeDtypeStruct((rows, out_weight.sha...  1.24 us

commit v1 on v0

v1 whole, which is shorter than its diff:
```python
import functools
import jax
import jax.numpy as jnp
from jax import lax
from jax.experimental import pallas as pl
from jax.experimental.pallas import tpu as pltpu
from jax.sharding import PartitionSpec as P

HEADS = 4
HEAD_DIM = 128
NEAR_WINDOW = 128
MIDDLE_WINDOW = 512
MIDDLE_DILATION = 4
FAR_WINDOW = 2048
FAR_DILATION = 16


def from_behind(block, axis, distance):
    devices = range(lax.axis_size(axis))
    route = [(i - distance, i) for i in devices if i - distance in devices]
    return lax.ppermute(block, axis, route)


def window_table():
    return ((NEAR_WINDOW, 1), (MIDDLE_WINDOW, MIDDLE_DILATION), (FAR_WINDOW, FAR_DILATION))


def tail_counts(row_count, distance, held_rows):
    counts = []
    for entry, available in zip(window_table(), held_rows):
        counts.append(max(0, min(available, entry[0] - (distance - 1) * row_count)))
    return counts


def pack_tails(sources, counts):
    selected = [
        source[:, source.shape[1] - amount :]
        for source, amount in zip(sources, counts)
        if amount > 0
    ]
    return jnp.concatenate(selected, axis=1)


def unpack_rows(packed, counts):
    result = []
    cursor = 0
    for amount in counts:
        result.append(packed[:, cursor : cursor + amount])
        cursor = cursor + amount
    return result


def attend_group(group_queries, buffer, window, dilation, first_key, slopes_here):
    row_count = group_queries.shape[0]
    head_count = group_queries.shape[1]
    head_size = group_queries.shape[2]
    query_split = group_queries.reshape(row_count // dilation, dilation, head_count, head_size)
    key_split = buffer[0].reshape(-1, dilation, head_count, head_size)
    value_split = buffer[1].reshape(-1, dilation, head_count, head_size)
    scores = jnp.einsum(
        "mrhe,nrhe->rhmn", query_split, key_split, preferred_element_type=jnp.float32
    ) * head_size ** (-0.5)
    grid_shape = (row_count // dilation, key_split.shape[0])
    query_slot = lax.broadcasted_iota(jnp.int32, grid_shape, 0)
    key_slot = lax.broadcasted_iota(jnp.int32, grid_shape, 1)
    spacing = query_slot + window // dilation - key_slot
    residue = lax.broadcasted_iota(jnp.int32, (dilation, 1, 1), 0)
    key_place = first_key + residue + dilation * key_slot[None]
    valid = (spacing[None] >= 0) & (spacing[None] <= window // dilation) & (key_place >= 0)
    scores = (
        scores
        - slopes_here[None, :, None, None] * (dilation * spacing).astype(jnp.float32)[None, None]
    )
    masked = jnp.where(valid[:, None], scores, -jnp.inf)
    highest = jnp.max(masked, axis=-1, keepdims=True)
    log_sum = highest + jnp.log(jnp.sum(jnp.exp(masked - highest), axis=-1, keepdims=True))
    probs = jnp.exp(masked - log_sum).astype(jnp.bfloat16)
    attended = jnp.einsum("rhmn,nrhe->mrhe", probs, value_split, preferred_element_type=jnp.float32)
    attended = attended.reshape(row_count, head_count, head_size)
    log_rows = jnp.transpose(log_sum[..., 0], (1, 2, 0)).reshape(head_count, row_count)
    return (attended, log_rows)


def local(tokens, query_weight, key_weight, value_weight, out_weight):
    rows_here = tokens.shape[0]
    local_heads = query_weight.shape[1] // (3 * HEAD_DIM)

    def project(weight_matrix):
        product = jnp.dot(tokens, weight_matrix, preferred_element_type=jnp.float32)
        return product.astype(jnp.bfloat16).reshape(rows_here, local_heads, 3, HEAD_DIM)

    queries = project(query_weight)
    keys_all = project(key_weight)
    values_all = project(value_weight)
    table = window_table()
    own = [jnp.stack((keys_all[:, :, index], values_all[:, :, index])) for index in range(3)]
    held = list(own)
    span_now = 1
    while span_now * rows_here < FAR_WINDOW + rows_here:
        counts = tail_counts(rows_here, span_now, [item.shape[1] for item in held])
        packed = pack_tails(held, counts)
        arrived = from_behind(packed, "sp", span_now)
        pieces_in = unpack_rows(arrived, counts)
        for index in range(3):
            if counts[index] > 0:
                joined = jnp.concatenate((pieces_in[index], held[index]), axis=1)
                held[index] = joined
        span_now = span_now * 2
    priors = [held[index][:, : table[index][0]] for index in range(3)]
    position_start = lax.axis_index("sp") * rows_here
    head_ids = (
        lax.axis_index("tp") * local_heads + jnp.arange(local_heads, dtype=jnp.int32)
    ).astype(jnp.float32)
    outputs = []
    logs = []
    for index, (window, dilation) in enumerate(table):
        buffer = jnp.concatenate((priors[index], own[index]), axis=1)
        slopes_here = 2.0 ** (3.0 - 8.0 * (head_ids + 1.0) / HEADS) / window
        attended, log_rows = attend_group(
            queries[:, :, index], buffer, window, dilation, position_start - window, slopes_here
        )
        outputs.append(attended)
        logs.append(log_rows)
    stacked_logs = jnp.stack(logs)
    highest = jnp.max(stacked_logs, axis=0)
    total_log = highest + jnp.log(jnp.sum(jnp.exp(stacked_logs - highest), axis=0))
    mixing = jnp.exp(stacked_logs - total_log)
    merged = outputs[0] * jnp.transpose(mixing[0])[:, :, None]
    merged = merged + outputs[1] * jnp.transpose(mixing[1])[:, :, None]
    merged = merged + outputs[2] * jnp.transpose(mixing[2])[:, :, None]
    merged = merged.astype(jnp.bfloat16).reshape(rows_here, local_heads * HEAD_DIM)
    mixed = jnp.dot(
        lax.all_gather(merged, "tp", axis=1, tiled=True),
        out_weight,
        preferred_element_type=jnp.float32,
    ).astype(jnp.bfloat16)
    return (mixed, total_log)


MESH = pl.DeviceIdType.MESH
MASKED = -1e30


def weigh(query, key, slope, distance, valid):
    scores = lax.dot_general(
        query, key, (((1,), (1,)), ((), ())), preferred_element_type=jnp.float32
    ) * HEAD_DIM ** (-0.5)
    scores = jnp.where(valid, scores - slope * distance, MASKED)
    highest = jnp.max(scores, axis=-1, keepdims=True)
    weights = jnp.exp(scores - highest)
    total = jnp.sum(weights, axis=-1, keepdims=True)
    probs = (weights * (1.0 / total)).astype(jnp.bfloat16)
    return probs, highest + jnp.log(total)


def attend(query, key, value, slope, distance, valid):
    probs, log_sum = weigh(query, key, slope, distance, valid)
    return jnp.dot(probs, value, preferred_element_type=jnp.float32), log_sum


def swap_matrix(rows, width):
    shift = width.bit_length() - 1
    row = lax.broadcasted_iota(jnp.int32, (rows, rows), 0)
    column = lax.broadcasted_iota(jnp.int32, (rows, rows), 1)
    source = ((row & (width - 1)) << shift) + (row >> shift)
    return jnp.where(column == source, 1.0, 0.0).astype(jnp.bfloat16)


def kernel(
    n, local_heads,
    tok_hbm, wq_hbm, wk_hbm, wv_hbm, wo_hbm,
    partial_ref, peer_ref, totals_ref,
    tok, weight, wo, far_send, far_held, back_send, back_held, log_send, log_held,
    mid_query, mid_own, mid_held, via_held, near_query, near_own, near_held, via_near,
    base, factor, merged_own, merged_held,
    load_sem, far_ssem, far_rsem, back_ssem, back_rsem, log_ssem, log_rsem,
    mid_ssem, mid_rsem, via_ssem, via_rsem, near_ssem, near_rsem, merged_ssem, merged_rsem,
):
    me = lax.axis_index("sp")
    tp = lax.axis_index("tp")
    rows = tok.shape[0]
    width = local_heads * HEAD_DIM
    chunk = rows // n
    shift = n.bit_length() - 1
    peer = 1 - tp
    sources = (wq_hbm, wk_hbm, wv_hbm)

    tok_load = pltpu.make_async_copy(tok_hbm, tok, load_sem.at[0])
    tok_load.start()
    wo_load = pltpu.make_async_copy(wo_hbm, wo, load_sem.at[1])
    loads = {}
    count = 2
    for group in (2, 1, 0):
        loads[group] = []
        if group == 2:
            order = [(part, head) for head in range(local_heads) for part in range(3)]
        else:
            order = [(part, head) for part in (1, 2, 0) for head in range(local_heads)]
        for place, (part, head) in enumerate(order):
            loads[group].append(pltpu.make_async_copy(
                sources[part].at[:, pl.ds((head * 3 + group) * HEAD_DIM, HEAD_DIM)],
                weight.at[group, :, pl.ds(place * HEAD_DIM, HEAD_DIM)],
                load_sem.at[count],
            ))
            count += 1
    for copy in loads[2]:
        copy.start()

    barrier = pltpu.get_barrier_semaphore()

    def greet(k, carry):
        pl.semaphore_signal(barrier, inc=1, device_id=(lax.rem(me + k, n), tp), device_id_type=MESH)
        return carry

    lax.fori_loop(1, n, greet, 0)
    pl.semaphore_signal(barrier, inc=1, device_id=(me, peer), device_id_type=MESH)

    @pl.when(me < 2)
    def _():
        mid_held[0] = jnp.zeros((2, rows, width), jnp.bfloat16)

    @pl.when(me < 1)
    def _():
        mid_held[1] = jnp.zeros((2, rows, width), jnp.bfloat16)
        near_held[...] = jnp.zeros((2, NEAR_WINDOW, width), jnp.bfloat16)

    def project(group, block):
        for copy in loads[group][block * local_heads : (block + 1) * local_heads]:
            copy.wait()
        return jnp.dot(
            tok[...], weight[group, :, block * width : (block + 1) * width],
            preferred_element_type=jnp.float32,
        ).astype(jnp.bfloat16)

    def at_rows(index):
        return pl.ds(pl.multiple_of(index * chunk, chunk), chunk)

    swap = swap_matrix(rows, n)

    def swapped(block):
        return jnp.dot(swap, block, preferred_element_type=jnp.float32).astype(jnp.bfloat16)

    def each(action):
        def step(k, carry):
            action(k)
            return carry

        lax.fori_loop(1, n, step, 0)

    def exchange(source, target, ssem, rsem, k, outgoing):
        to = lax.rem(me + k, n)
        come = lax.rem(me + n - k, n)
        place = at_rows(me if outgoing else come)
        return pltpu.make_async_remote_copy(
            src_ref=source.at[at_rows(to)],
            dst_ref=target.at[place],
            send_sem=ssem.at[k],
            recv_sem=rsem.at[k],
            device_id=(to, tp),
            device_id_type=MESH,
        )

    def far_copy(block, k, outgoing):
        return exchange(
            far_send.at[block], far_held.at[block], far_ssem.at[block], far_rsem.at[block], k, outgoing
        )

    def back_copy(head, k, outgoing):
        return exchange(
            back_send.at[head], back_held.at[head], back_ssem.at[head], back_rsem.at[head], k, outgoing
        )

    def log_copy(k, outgoing):
        to = lax.rem(me + k, n)
        come = lax.rem(me + n - k, n)
        return pltpu.make_async_remote_copy(
            src_ref=log_send.at[to],
            dst_ref=log_held.at[me if outgoing else come],
            send_sem=log_ssem.at[k],
            recv_sem=log_rsem.at[k],
            device_id=(to, tp),
            device_id_type=MESH,
        )

    tok_load.wait()
    for block in range(3):
        far_send[block] = swapped(project(2, block))
        if block == 0:
            for copy in loads[1]:
                copy.start()
            pl.semaphore_wait(barrier, n)
        each(lambda k: far_copy(block, k, True).start())
        far_held[block, at_rows(me), :] = far_send[block, at_rows(me), :]
    for copy in loads[0]:
        copy.start()
    wo_load.start()

    def mid_copy(slot, hop, source, part, sem):
        return pltpu.make_async_remote_copy(
            src_ref=source,
            dst_ref=mid_held.at[slot, part],
            send_sem=mid_ssem.at[sem, part],
            recv_sem=mid_rsem.at[slot, part],
            device_id=(lax.rem(me + hop + n, n), tp),
            device_id_type=MESH,
        )

    def near_copy(hop, source, part, sem):
        return pltpu.make_async_remote_copy(
            src_ref=source,
            dst_ref=near_held.at[part],
            send_sem=near_ssem.at[sem],
            recv_sem=near_rsem.at[part],
            device_id=(lax.rem(me + hop, n), tp),
            device_id_type=MESH,
        )

    def via_copy(which, source, target):
        return pltpu.make_async_remote_copy(
            src_ref=source,
            dst_ref=target,
            send_sem=via_ssem.at[which],
            recv_sem=via_rsem.at[which],
            device_id=(lax.rem(me + -2 + n, n), tp),
            device_id_type=MESH,
        )

    near_tail = pl.ds(rows - NEAR_WINDOW, NEAR_WINDOW)
    key_two = mid_copy(0, 2, mid_own.at[0], 0, 0)
    key_one = mid_copy(1, 1, mid_own.at[0], 0, 1)
    value_two = mid_copy(0, 2, mid_own.at[1], 1, 0)
    value_one = mid_copy(1, 1, mid_own.at[1], 1, 1)
    near_key = near_copy(1, near_own.at[0, near_tail], 0, 0)
    near_value = near_copy(1, near_own.at[1, near_tail], 1, 1)
    via_mid = via_copy(0, mid_own.at[1], via_held)
    via_last = via_copy(1, near_own.at[1, near_tail], via_near)
    onward_even = mid_copy(0, 4, via_held, 1, 3)
    onward_odd = mid_copy(1, 3, via_held, 1, 3)
    onward_near = near_copy(3, via_near, 1, 2)
    relay_key = mid_copy(0, 1, mid_held.at[1, 0], 0, 2)
    relay_value = mid_copy(0, 1, mid_held.at[1, 1], 1, 2)

    even = lax.rem(me, 2) == 0
    odd = jnp.logical_not(even)
    sends_one = me + 1 < n
    sends_two = even & (me + 2 < n)
    relays = even & (me >= 1)
    above = me + 4 - lax.rem(me, 4) < n
    crosses = (lax.rem(me, 4) >= 2) & above
    stays = jnp.logical_not(crosses)
    forwards = (lax.rem(me, 4) < 2) & above
    direct = sends_one & jnp.logical_not(crosses & odd)

    mid_own[0] = project(1, 0)
    mid_own[1] = project(1, 1)

    @pl.when(crosses)
    def _():
        via_mid.start()

    @pl.when(sends_two & stays)
    def _():
        key_two.start()
        value_two.start()

    @pl.when(direct)
    def _():
        key_one.start()
        value_one.start()

    near_own[0] = project(0, 0)
    near_own[1] = project(0, 1)

    @pl.when(crosses & odd)
    def _():
        via_last.start()

    @pl.when(direct)
    def _():
        near_key.start()
        near_value.start()

    mid_query[...] = swapped(project(1, 2))
    near_query[...] = swapped(project(0, 2))

    def slope_of(head, window):
        number = tp * local_heads + head
        slope = jnp.float32(0.0)
        for index in range(HEADS):
            value = 2.0 ** (3.0 - 8.0 * (index + 1.0) / HEADS) / window
            slope = jnp.where(number == index, jnp.float32(value), slope)
        return slope

    def spacing(row_count, key_count, offset, scattered):
        row = lax.broadcasted_iota(jnp.int32, (row_count, key_count), 0)
        column = lax.broadcasted_iota(jnp.int32, (row_count, key_count), 1)
        if scattered:
            row = ((row & (n - 1)) << shift) + (row >> shift)
        return row + offset - column, column

    each(lambda k: far_copy(0, k, False).wait_recv())
    each(lambda k: far_copy(1, k, False).wait_recv())

    @pl.when(crosses & even)
    def _():
        key_two.start()

    @pl.when(crosses & odd)
    def _():
        key_one.start()
        near_key.start()

    @pl.when(forwards)
    def _():
        via_mid.wait_recv()

    @pl.when(forwards & even)
    def _():
        onward_even.start()

    @pl.when(forwards & odd)
    def _():
        onward_odd.start()
        via_last.wait_recv()
        onward_near.start()

    reach = FAR_WINDOW // FAR_DILATION
    apart, _ = spacing(rows, rows, 0, False)
    valid = (apart >= 0) & (apart <= reach)
    distance = (apart * FAR_DILATION).astype(jnp.float32)
    lane = lax.broadcasted_iota(jnp.int32, (rows, HEAD_DIM), 1)
    slot = lax.broadcasted_iota(jnp.int32, (rows, HEAD_DIM), 0) & (chunk - 1)
    packed = jnp.zeros((rows, HEAD_DIM), jnp.float32)

    def far_part(head, part):
        block, half = divmod(head * 3 + part, local_heads)
        return far_held[block, :, half * HEAD_DIM : (half + 1) * HEAD_DIM]

    for head in range(local_heads):
        if head == local_heads - 1:
            each(lambda k: far_copy(2, k, False).wait_recv())
        probs, log_sum = weigh(
            far_part(head, 0), far_part(head, 1), slope_of(head, FAR_WINDOW), distance, valid
        )
        packed = jnp.where(lane == head * chunk + slot, log_sum, packed)
        if head == local_heads - 1:
            log_send[...] = jnp.sum(packed.reshape(n, chunk, HEAD_DIM), axis=1, keepdims=True)
            each(lambda k: log_copy(k, True).start())
            log_held[me] = log_send[me]
        back_send[head] = jnp.dot(
            probs, far_part(head, 2), preferred_element_type=jnp.float32
        ).astype(jnp.bfloat16)
        each(lambda k: back_copy(head, k, True).start())
        back_held[head, at_rows(me), :] = back_send[head, at_rows(me), :]

    @pl.when(me >= 1)
    def _():
        near_key.wait_recv()
        near_value.wait_recv()
        key_one.wait_recv()
        value_one.wait_recv()

    @pl.when(relays)
    def _():
        relay_key.start()
        relay_value.start()

    apart, column = spacing(rows, NEAR_WINDOW + rows, NEAR_WINDOW, True)
    valid = (apart >= 0) & (apart <= NEAR_WINDOW) & (column + me * rows >= NEAR_WINDOW)
    distance = apart.astype(jnp.float32)
    near = []
    for head in range(local_heads):
        at = pl.ds(head * HEAD_DIM, HEAD_DIM)
        key = jnp.concatenate((near_held[0, :, at], near_own[0, :, at]), axis=0)
        value = jnp.concatenate((near_held[1, :, at], near_own[1, :, at]), axis=0)
        near.append(attend(near_query[:, at], key, value, slope_of(head, NEAR_WINDOW), distance, valid))

    @pl.when(me >= 2)
    def _():
        key_two.wait_recv()
        value_two.wait_recv()

    apart, column = spacing(rows, MIDDLE_WINDOW + rows, MIDDLE_WINDOW, True)
    valid = (apart >= 0) & (apart <= MIDDLE_WINDOW) & ((apart & (MIDDLE_DILATION - 1)) == 0)
    valid = valid & (column + me * rows >= MIDDLE_WINDOW)
    distance = apart.astype(jnp.float32)
    pairs = []
    for head in range(local_heads):
        at = pl.ds(head * HEAD_DIM, HEAD_DIM)
        key = jnp.concatenate((mid_held[0, 0, :, at], mid_held[1, 0, :, at], mid_own[0, :, at]), axis=0)
        value = jnp.concatenate((mid_held[0, 1, :, at], mid_held[1, 1, :, at], mid_own[1, :, at]), axis=0)
        middle, middle_log = attend(
            mid_query[:, at], key, value, slope_of(head, MIDDLE_WINDOW), distance, valid
        )
        near_log = near[head][1]
        highest = jnp.maximum(near_log, middle_log)
        near_share, middle_share = jnp.exp(near_log - highest), jnp.exp(middle_log - highest)
        base[head] = near[head][0] * near_share + middle * middle_share
        pairs.append((highest, near_share + middle_share))

    each(lambda k: log_copy(k, False).wait_recv())

    spread = jnp.broadcast_to(log_held[...], (n, chunk, HEAD_DIM)).reshape(rows, HEAD_DIM)
    terms = jnp.zeros((rows, HEAD_DIM), jnp.float32)
    for head in range(local_heads):
        far_log = jnp.sum(
            jnp.where(lane == head * chunk + slot, spread, 0.0), axis=-1, keepdims=True
        )
        pair_log, pair_sum = pairs[head]
        highest = jnp.maximum(pair_log, far_log)
        total = highest + jnp.log(pair_sum * jnp.exp(pair_log - highest) + jnp.exp(far_log - highest))
        base[head] = base[head] * jnp.exp(pair_log - total)
        factor[head] = jnp.broadcast_to(jnp.exp(far_log - total), (rows, HEAD_DIM))
        rest = total
        for term in range(3):
            piece = rest.astype(jnp.bfloat16).astype(jnp.float32)
            terms = jnp.where(lane == 3 * head + term, piece, terms)
            rest = rest - piece

    def merged_copy(k, outgoing):
        place = at_rows(lax.rem(me + n - k, n))
        return pltpu.make_async_remote_copy(
            src_ref=merged_own.at[place],
            dst_ref=merged_held.at[place],
            send_sem=merged_ssem.at[k],
            recv_sem=merged_rsem.at[k],
            device_id=(me, peer),
            device_id_type=MESH,
        )

    def merge(k):
        place = at_rows(lax.rem(me + n - k, n))
        for head in range(local_heads):
            mixed = base[head, place, :] + back_held[head, place, :].astype(jnp.float32) * factor[head, place, :]
            merged_own[place, head * HEAD_DIM : (head + 1) * HEAD_DIM] = mixed.astype(jnp.bfloat16)
        merged_copy(k, True).start()

    merge(0)

    def arrive(k):
        for head in range(local_heads):
            back_copy(head, k, False).wait_recv()
        merge(k)

    each(arrive)

    totals = jnp.dot(swap, terms.astype(jnp.bfloat16), preferred_element_type=jnp.float32)
    summed = jnp.zeros((rows, HEAD_DIM), jnp.float32)
    for head in range(local_heads):
        total = jnp.sum(
            jnp.where((lane >= 3 * head) & (lane < 3 * head + 3), totals, 0.0), axis=-1, keepdims=True
        )
        summed = jnp.where(lane == head, total, summed)
    totals_ref[...] = summed
    wo_load.wait()
    partial_ref[...] = jnp.dot(
        swapped(merged_own[...]), wo[pl.ds(pl.multiple_of(tp * width, width), width), :],
        preferred_element_type=jnp.float32,
    )

    merged_copy(0, False).wait_recv()
    each(lambda k: merged_copy(k, False).wait_recv())
    peer_ref[...] = swapped(merged_held[...])

    merged_copy(0, True).wait_send()
    each(lambda k: merged_copy(k, True).wait_send())
    for block in range(3):
        each(lambda k: far_copy(block, k, True).wait_send())
    each(lambda k: log_copy(k, True).wait_send())
    for head in range(local_heads):
        each(lambda k: back_copy(head, k, True).wait_send())

    @pl.when(crosses)
    def _():
        via_mid.wait_send()

    @pl.when(crosses & odd)
    def _():
        via_last.wait_send()

    @pl.when(sends_two)
    def _():
        key_two.wait_send()

    @pl.when(sends_two & stays)
    def _():
        value_two.wait_send()

    @pl.when(sends_one)
    def _():
        key_one.wait_send()
        near_key.wait_send()

    @pl.when(direct)
    def _():
        value_one.wait_send()
        near_value.wait_send()

    @pl.when(forwards & even)
    def _():
        onward_even.wait_send()

    @pl.when(forwards & odd)
    def _():
        onward_odd.wait_send()
        onward_near.wait_send()

    @pl.when(relays)
    def _():
        relay_key.wait_send()
        relay_value.wait_send()


def mix(partial_ref, peer_ref, totals_ref, wo_ref, mixed_hbm, log_ref, out, sem):
    width = peer_ref.shape[1]
    steps = out.shape[0]
    piece = out.shape[2]
    at = pl.ds(pl.multiple_of((1 - lax.axis_index("tp")) * width, width), width)
    copies = []
    for step in range(steps):
        columns = pl.ds(step * piece, piece)
        product = jnp.dot(peer_ref[...], wo_ref[at, columns], preferred_element_type=jnp.float32)
        out[step] = (partial_ref[:, columns] + product).astype(jnp.bfloat16)
        copies.append(pltpu.make_async_copy(out.at[step], mixed_hbm.at[:, columns], sem.at[step]))
        copies[-1].start()
    log_ref[...] = jnp.transpose(totals_ref[...])[: log_ref.shape[0]]
    for copy in copies:
        copy.wait()


def fused(n, tokens, query_weight, key_weight, value_weight, out_weight):
    rows, depth = tokens.shape
    columns = query_weight.shape[1]
    out_columns = out_weight.shape[1]
    local_heads = columns // (3 * HEAD_DIM)
    width = local_heads * HEAD_DIM
    dma = pltpu.SemaphoreType.DMA
    half = jnp.bfloat16
    full = jnp.float32
    whole = pl.BlockSpec(memory_space=pltpu.VMEM)
    anywhere = pl.BlockSpec(memory_space=pl.ANY)
    partial, peer, totals = pl.pallas_call(
        functools.partial(kernel, n, local_heads),
        out_shape=(
            jax.ShapeDtypeStruct((rows, out_columns), full),
            jax.ShapeDtypeStruct((rows, width), half),
            jax.ShapeDtypeStruct((rows, HEAD_DIM), full),
        ),
        in_specs=[anywhere] * 5,
        out_specs=(whole, whole, whole),
        scratch_shapes=[
            pltpu.VMEM((rows, depth), half),
            pltpu.VMEM((3, depth, columns), half),
            pltpu.VMEM(out_weight.shape, half),
            pltpu.VMEM((3, rows, width), half),
            pltpu.VMEM((3, rows, width), half),
            pltpu.VMEM((local_heads, rows, HEAD_DIM), half),
            pltpu.VMEM((local_heads, rows, HEAD_DIM), half),
            pltpu.VMEM((n, 1, HEAD_DIM), full),
            pltpu.VMEM((n, 1, HEAD_DIM), full),
            pltpu.VMEM((rows, width), half),
            pltpu.VMEM((2, rows, width), half),
            pltpu.VMEM((2, 2, rows, width), half),
            pltpu.VMEM((rows, width), half),
            pltpu.VMEM((rows, width), half),
            pltpu.VMEM((2, rows, width), half),
            pltpu.VMEM((2, NEAR_WINDOW, width), half),
            pltpu.VMEM((NEAR_WINDOW, width), half),
            pltpu.VMEM((local_heads, rows, HEAD_DIM), full),
            pltpu.VMEM((local_heads, rows, HEAD_DIM), full),
            pltpu.VMEM((rows, width), half),
            pltpu.VMEM((rows, width), half),
            dma((2 + 9 * local_heads,)),
            dma((3, n)), dma((3, n)), dma((local_heads, n)), dma((local_heads, n)), dma((n,)), dma((n,)),
            dma((4, 2)), dma((2, 2)), dma((2,)), dma((2,)), dma((3,)), dma((2,)), dma((n,)), dma((n,)),
        ],
        compiler_params=pltpu.CompilerParams(
            collective_id=0, has_side_effects=True, vmem_limit_bytes=54000 * 1024
        ),
    )(tokens, query_weight, key_weight, value_weight, out_weight)
    pieces = out_columns // width
    return pl.pallas_call(
        mix,
        out_shape=(
            jax.ShapeDtypeStruct((rows, out_columns), half),
            jax.ShapeDtypeStruct((local_heads, rows), full),
        ),
        in_specs=[whole] * 4,
        out_specs=(anywhere, whole),
        scratch_shapes=[pltpu.VMEM((pieces, rows, width), half), dma((pieces,))],
        compiler_params=pltpu.CompilerParams(vmem_limit_bytes=16000 * 1024),
    )(partial, peer, totals, out_weight)


def solution(mesh):
    n, n_tp = mesh.shape["sp"], mesh.shape["tp"]
    if n == FAR_DILATION and n_tp == 2:
        body = functools.partial(fused, n)
    else:
        body = local
    return jax.shard_map(
        body,
        mesh=mesh,
        in_specs=(P("sp", None), P(None, "tp"), P(None, "tp"), P(None, "tp"), P(None, "tp")),
        out_specs=(P("sp", "tp"), P("tp", "sp")),
        check_vma=False,
    )
```

time: 33.7 us -> 36.4 us (1.080)
  local copies, waits for them, and re-layouts: 0.01 us -> 1.22 us
  Pallas kernels: 32.8 us -> 34 us
    pallas_call x2, Pallas kernels: 32.8 us -> 34 us  [the longest x1 32.4 us: fused(): pl.pallas_call(functools.partial(kernel, n, local_heads), out_shape=(jax....]
    unnamed x2 -> x4, local copies, waits for them, and re-layouts: 0.01 us -> 1.22 us
where the time goes in v1:
time: 36.4 us; the launch traced here: 35.9 us
  Pallas kernels  34 us (93%)
  local copies, waits for them, and re-layouts  1.22 us (3%)
  between operations  0.66 us (2%)
    pallas_call x1, Pallas kernels, fused(): pl.pallas_call(functools.partial(kernel, n, local_heads), out_shape=(jax....  32.4 us
    pallas_call x1, Pallas kernels, fused(): pl.pallas_call(mix, out_shape=(jax.ShapeDtypeStruct((rows, out_columns),...  1.63 us
    unnamed x4, local copies, waits for them, and re-layouts  1.22 us

profile of v1, /device:TPU:16, one launch (start us, length us, event | category | flops | bytes accessed | tf_op | source)
XLA Modules:
  0.0 35.9 jit_solution(17746075785619813937)
XLA Ops:
  0.6 0.0 copy-start
  0.6 32.4 %shard_map.68 = (f32[256,1024]{1,0:T(8,128)}, bf16[256,256]{1,0:T(8,128)(2,1)S(1)}, f32[256,128]{1,0:T(8,128)S(1)}) custom-call(bf16[256,2048]{1,0:T(8,128)(2,1)} %tok_hbm.1, bf16[2048,768]{1,0:T(8,128)(2,1)} %wq_hbm.1, bf16[2048,768]{1,0:T(8,128)(2,1)} %wk_hbm.1, bf16[2048,768]{1,0:T(8,128)(2,1)} %wv_hbm.1, bf16[512,1024]{1,0:T(8,128)(2,1)} %wo_ref.1), custom_call_target="tpu_custom_call" | custom-call | tf_op jit(solution)/shard_map/pallas_call | solution.py:642
  33.0 0.0 copy-done
  33.0 0.0 copy-start.1
  33.0 1.2 %copy-done.1 = f32[256,1024]{1,0:T(8,128)S(1)} copy-done((f32[256,1024]{1,0:T(8,128)S(1)}, f32[256,1024]{1,0:T(8,128)}, u32[]{:S(2)}) %copy-start.1) | copy-done | bytes 1048600
  34.2 1.6 %shard_map.69 = (bf16[256,1024]{1,0:T(8,128)(2,1)}, f32[2,256]{1,0:T(2,128)}) custom-call(f32[256,1024]{1,0:T(8,128)S(1)} %copy-done.1, bf16[256,256]{1,0:T(8,128)(2,1)S(1)} %get-tuple-element.6.peer_ref, f32[256,128]{1,0:T(8,128)S(1)} %get-tuple-element.7.totals_ref, bf16[512,1024]{1,0:T(8,128)(2,1)S(1)} %copy-done), custom_call_target="tpu_custom_call" | custom-call | tf_op jit(solution)/shard_map/pallas_call | solution.py:682
Async XLA Ops:
  0.6 32.4 %copy-start = (bf16[512,1024]{1,0:T(8,128)(2,1)S(1)}, bf16[512,1024]{1,0:T(8,128)(2,1)}, u32[]{:S(2)}) copy-start(bf16[512,1024]{1,0:T(8,128)(2,1)} %wo_ref.1) | copy-start | bytes 3145732
  33.0 1.2 %copy-start.1 = (f32[256,1024]{1,0:T(8,128)S(1)}, f32[256,1024]{1,0:T(8,128)}, u32[]{:S(2)}) copy-start(f32[256,1024]{1,0:T(8,128)} %get-tuple-element.5.partial_ref) | copy-start | bytes 3145732

commit v2 on v1

v2 whole, which is shorter than its diff:
```python
import functools
import jax
import jax.numpy as jnp
from jax import lax
from jax.experimental import pallas as pl
from jax.experimental.pallas import tpu as pltpu
from jax.sharding import PartitionSpec as P

HEADS = 4
HEAD_DIM = 128
NEAR_WINDOW = 128
MIDDLE_WINDOW = 512
MIDDLE_DILATION = 4
FAR_WINDOW = 2048
FAR_DILATION = 16


def from_behind(block, axis, distance):
    devices = range(lax.axis_size(axis))
    route = [(i - distance, i) for i in devices if i - distance in devices]
    return lax.ppermute(block, axis, route)


def window_table():
    return ((NEAR_WINDOW, 1), (MIDDLE_WINDOW, MIDDLE_DILATION), (FAR_WINDOW, FAR_DILATION))


def tail_counts(row_count, distance, held_rows):
    counts = []
    for entry, available in zip(window_table(), held_rows):
        counts.append(max(0, min(available, entry[0] - (distance - 1) * row_count)))
    return counts


def pack_tails(sources, counts):
    selected = [
        source[:, source.shape[1] - amount :]
        for source, amount in zip(sources, counts)
        if amount > 0
    ]
    return jnp.concatenate(selected, axis=1)


def unpack_rows(packed, counts):
    result = []
    cursor = 0
    for amount in counts:
        result.append(packed[:, cursor : cursor + amount])
        cursor = cursor + amount
    return result


def attend_group(group_queries, buffer, window, dilation, first_key, slopes_here):
    row_count = group_queries.shape[0]
    head_count = group_queries.shape[1]
    head_size = group_queries.shape[2]
    query_split = group_queries.reshape(row_count // dilation, dilation, head_count, head_size)
    key_split = buffer[0].reshape(-1, dilation, head_count, head_size)
    value_split = buffer[1].reshape(-1, dilation, head_count, head_size)
    scores = jnp.einsum(
        "mrhe,nrhe->rhmn", query_split, key_split, preferred_element_type=jnp.float32
    ) * head_size ** (-0.5)
    grid_shape = (row_count // dilation, key_split.shape[0])
    query_slot = lax.broadcasted_iota(jnp.int32, grid_shape, 0)
    key_slot = lax.broadcasted_iota(jnp.int32, grid_shape, 1)
    spacing = query_slot + window // dilation - key_slot
    residue = lax.broadcasted_iota(jnp.int32, (dilation, 1, 1), 0)
    key_place = first_key + residue + dilation * key_slot[None]
    valid = (spacing[None] >= 0) & (spacing[None] <= window // dilation) & (key_place >= 0)
    scores = (
        scores
        - slopes_here[None, :, None, None] * (dilation * spacing).astype(jnp.float32)[None, None]
    )
    masked = jnp.where(valid[:, None], scores, -jnp.inf)
    highest = jnp.max(masked, axis=-1, keepdims=True)
    log_sum = highest + jnp.log(jnp.sum(jnp.exp(masked - highest), axis=-1, keepdims=True))
    probs = jnp.exp(masked - log_sum).astype(jnp.bfloat16)
    attended = jnp.einsum("rhmn,nrhe->mrhe", probs, value_split, preferred_element_type=jnp.float32)
    attended = attended.reshape(row_count, head_count, head_size)
    log_rows = jnp.transpose(log_sum[..., 0], (1, 2, 0)).reshape(head_count, row_count)
    return (attended, log_rows)


def local(tokens, query_weight, key_weight, value_weight, out_weight):
    rows_here = tokens.shape[0]
    local_heads = query_weight.shape[1] // (3 * HEAD_DIM)

    def project(weight_matrix):
        product = jnp.dot(tokens, weight_matrix, preferred_element_type=jnp.float32)
        return product.astype(jnp.bfloat16).reshape(rows_here, local_heads, 3, HEAD_DIM)

    queries = project(query_weight)
    keys_all = project(key_weight)
    values_all = project(value_weight)
    table = window_table()
    own = [jnp.stack((keys_all[:, :, index], values_all[:, :, index])) for index in range(3)]
    held = list(own)
    span_now = 1
    while span_now * rows_here < FAR_WINDOW + rows_here:
        counts = tail_counts(rows_here, span_now, [item.shape[1] for item in held])
        packed = pack_tails(held, counts)
        arrived = from_behind(packed, "sp", span_now)
        pieces_in = unpack_rows(arrived, counts)
        for index in range(3):
            if counts[index] > 0:
                joined = jnp.concatenate((pieces_in[index], held[index]), axis=1)
                held[index] = joined
        span_now = span_now * 2
    priors = [held[index][:, : table[index][0]] for index in range(3)]
    position_start = lax.axis_index("sp") * rows_here
    head_ids = (
        lax.axis_index("tp") * local_heads + jnp.arange(local_heads, dtype=jnp.int32)
    ).astype(jnp.float32)
    outputs = []
    logs = []
    for index, (window, dilation) in enumerate(table):
        buffer = jnp.concatenate((priors[index], own[index]), axis=1)
        slopes_here = 2.0 ** (3.0 - 8.0 * (head_ids + 1.0) / HEADS) / window
        attended, log_rows = attend_group(
            queries[:, :, index], buffer, window, dilation, position_start - window, slopes_here
        )
        outputs.append(attended)
        logs.append(log_rows)
    stacked_logs = jnp.stack(logs)
    highest = jnp.max(stacked_logs, axis=0)
    total_log = highest + jnp.log(jnp.sum(jnp.exp(stacked_logs - highest), axis=0))
    mixing = jnp.exp(stacked_logs - total_log)
    merged = outputs[0] * jnp.transpose(mixing[0])[:, :, None]
    merged = merged + outputs[1] * jnp.transpose(mixing[1])[:, :, None]
    merged = merged + outputs[2] * jnp.transpose(mixing[2])[:, :, None]
    merged = merged.astype(jnp.bfloat16).reshape(rows_here, local_heads * HEAD_DIM)
    mixed = jnp.dot(
        lax.all_gather(merged, "tp", axis=1, tiled=True),
        out_weight,
        preferred_element_type=jnp.float32,
    ).astype(jnp.bfloat16)
    return (mixed, total_log)


MESH = pl.DeviceIdType.MESH
MASKED = -1e30


def scores_of(query, key):
    return lax.dot_general(
        query, key, (((1,), (1,)), ((), ())), preferred_element_type=jnp.float32
    ) * HEAD_DIM ** (-0.5)


def weigh(scores, slope, distance, valid):
    scores = jnp.where(valid, scores - slope * distance, MASKED)
    highest = jnp.max(scores, axis=-1, keepdims=True)
    weights = jnp.exp(scores - highest)
    return highest, weights, jnp.sum(weights, axis=-1, keepdims=True)


def apply(weights, value):
    return jnp.dot(weights.astype(jnp.bfloat16), value, preferred_element_type=jnp.float32)


def one_hot(rows, token_of_row):
    row = lax.broadcasted_iota(jnp.int32, (rows, rows), 0)
    column = lax.broadcasted_iota(jnp.int32, (rows, rows), 1)
    return jnp.where(column == token_of_row(row), 1.0, 0.0).astype(jnp.bfloat16)


def kernel(
    n, local_heads,
    tok_hbm, wq_hbm, wk_hbm, wv_hbm, wo_hbm,
    partial_ref, peer_ref, totals_ref,
    tok, weight, wo, first_send, first_held, second_send, second_held, back_send, back_held, log_send, log_held,
    mid_query, mid_own, mid_held, via_held, near_query, near_own, near_held,
    base, stats, terms, merged_own, merged_held, near_sum,
    load_sem, first_sem, second_sem, back_ssem, back_rsem, log_ssem, log_rsem,
    mid_ssem, mid_rsem, via_ssem, via_rsem, near_ssem, near_rsem, merged_ssem, merged_rsem,
):
    me = lax.axis_index("sp")
    tp = lax.axis_index("tp")
    rows = tok.shape[0]
    width = local_heads * HEAD_DIM
    chunk = rows // n
    classes = MIDDLE_DILATION
    members = n // classes
    stretch = rows // classes
    peer = 1 - tp
    sources = (wq_hbm, wk_hbm, wv_hbm)

    tok_load = pltpu.make_async_copy(tok_hbm, tok, load_sem.at[0])
    tok_load.start()
    wo_load = pltpu.make_async_copy(wo_hbm, wo, load_sem.at[1])
    loads = []
    order = [(2, part, head) for head in range(local_heads) for part in range(3)]
    for group, part in ((0, 0), (0, 1), (0, 2), (1, 0)):
        order += [(group, part, head) for head in range(local_heads)]
    middle = [(1, part, head) for part in (1, 2) for head in range(local_heads)]
    order[2 * local_heads : 2 * local_heads] = middle
    for place, (group, part, head) in enumerate(order):
        loads.append(pltpu.make_async_copy(
            sources[part].at[:, pl.ds((head * 3 + group) * HEAD_DIM, HEAD_DIM)],
            weight.at[:, pl.ds(place * HEAD_DIM, HEAD_DIM)],
            load_sem.at[2 + place],
        ))
    early = 4 * local_heads
    for copy in loads[:early]:
        copy.start()

    barrier = pltpu.get_barrier_semaphore()

    def greet(k, carry):
        pl.semaphore_signal(barrier, inc=1, device_id=(lax.rem(me + k, n), tp), device_id_type=MESH)
        return carry

    lax.fori_loop(1, n, greet, 0)
    pl.semaphore_signal(barrier, inc=1, device_id=(me, peer), device_id_type=MESH)

    @pl.when(me < 2)
    def _():
        mid_held[0] = jnp.zeros((2, rows, width), jnp.bfloat16)

    @pl.when(me < 1)
    def _():
        mid_held[1] = jnp.zeros((2, rows, width), jnp.bfloat16)
        near_held[...] = jnp.zeros((2, NEAR_WINDOW, width), jnp.bfloat16)

    def project(first, last):
        for copy in loads[first * local_heads : last * local_heads]:
            copy.wait()
        return jnp.dot(
            tok[...], weight[:, first * width : last * width], preferred_element_type=jnp.float32
        ).astype(jnp.bfloat16)

    def at_rows(index):
        return pl.ds(pl.multiple_of(index * chunk, chunk), chunk)

    def scatter_token(row):
        group, index = row // chunk, row % chunk
        return index * n + (group % members) * classes + group // members

    def gather_row(token):
        index, residue = token // n, token % n
        return ((residue % classes) * members + residue // classes) * chunk + index

    def class_token(row):
        return (row % stretch) * classes + row // stretch

    to_scattered = one_hot(rows, scatter_token)
    to_tokens = one_hot(rows, gather_row)
    to_classes = one_hot(rows, class_token)

    def moved(matrix, block):
        return jnp.dot(matrix, block, preferred_element_type=jnp.float32).astype(jnp.bfloat16)

    def each(action):
        def step(k, carry):
            action(k)
            return carry

        lax.fori_loop(1, n, step, 0)

    plane = me // members
    upper = me // (n // 2)

    def target_of(k):
        rising = k - 1 + jnp.where(k - 1 >= me, 1, 0)
        falling = n - k - jnp.where(n - k <= me, 1, 0)
        return jnp.where(upper == 1, rising, falling)


    def far_copy(source, target, sem, k):
        to = target_of(k)
        return pltpu.make_async_remote_copy(
            src_ref=source.at[at_rows(to)],
            dst_ref=target.at[at_rows(me)],
            send_sem=sem.at[0],
            recv_sem=sem.at[1],
            device_id=(to, tp),
            device_id_type=MESH,
        )

    def far_whole(source, target, sem):
        others = pl.ds(0, rows - chunk)
        return pltpu.make_async_remote_copy(
            src_ref=source.at[others],
            dst_ref=target.at[others],
            send_sem=sem.at[0],
            recv_sem=sem.at[1],
            device_id=(lax.rem(me + 1, n), tp),
            device_id_type=MESH,
        )

    def back_copy(k):
        to = target_of(k)
        return pltpu.make_async_remote_copy(
            src_ref=back_send.at[at_rows(to)],
            dst_ref=back_held.at[at_rows(me)],
            send_sem=back_ssem,
            recv_sem=back_rsem.at[plane],
            device_id=(to, tp),
            device_id_type=MESH,
        )

    def back_whole(count, group):
        some = pl.ds(0, count * chunk)
        return pltpu.make_async_remote_copy(
            src_ref=back_send.at[some],
            dst_ref=back_held.at[some],
            send_sem=back_ssem,
            recv_sem=back_rsem.at[group],
            device_id=(lax.rem(me + 1, n), tp),
            device_id_type=MESH,
        )

    def log_copy(k):
        to = target_of(k)
        return pltpu.make_async_remote_copy(
            src_ref=log_send.at[to],
            dst_ref=log_held.at[me],
            send_sem=log_ssem,
            recv_sem=log_rsem.at[plane],
            device_id=(to, tp),
            device_id_type=MESH,
        )

    def log_whole(count, group):
        some = pl.ds(0, count)
        return pltpu.make_async_remote_copy(
            src_ref=log_send.at[some],
            dst_ref=log_held.at[some],
            send_sem=log_ssem,
            recv_sem=log_rsem.at[group],
            device_id=(lax.rem(me + 1, n), tp),
            device_id_type=MESH,
        )

    tok_load.wait()
    first_send[...] = moved(to_scattered, project(0, 2))
    for copy in loads[early:]:
        copy.start()
    pl.semaphore_wait(barrier, n)
    each(lambda k: far_copy(first_send, first_held, first_sem, k).start())
    first_held[at_rows(me), :] = first_send[at_rows(me), :]

    def mid_copy(slot, hop, source, part, sem):
        return pltpu.make_async_remote_copy(
            src_ref=source,
            dst_ref=mid_held.at[slot, part],
            send_sem=mid_ssem.at[sem, part],
            recv_sem=mid_rsem.at[slot, part],
            device_id=(lax.rem(me + hop + n, n), tp),
            device_id_type=MESH,
        )

    def near_copy(hop, source, part, sem):
        return pltpu.make_async_remote_copy(
            src_ref=source,
            dst_ref=near_held.at[part],
            send_sem=near_ssem.at[sem],
            recv_sem=near_rsem.at[part],
            device_id=(lax.rem(me + hop, n), tp),
            device_id_type=MESH,
        )

    def via_copy(which, source, target):
        return pltpu.make_async_remote_copy(
            src_ref=source,
            dst_ref=target,
            send_sem=via_ssem.at[which],
            recv_sem=via_rsem.at[which],
            device_id=(lax.rem(me + -2 + n, n), tp),
            device_id_type=MESH,
        )

    near_tail = pl.ds(rows - NEAR_WINDOW, NEAR_WINDOW)
    key_two = mid_copy(0, 2, mid_own.at[0], 0, 0)
    key_one = mid_copy(1, 1, mid_own.at[0], 0, 1)
    value_two = mid_copy(0, 2, mid_own.at[1], 1, 0)
    value_one = mid_copy(1, 1, mid_own.at[1], 1, 1)
    near_key = near_copy(1, near_own.at[0, near_tail], 0, 0)
    near_value = near_copy(1, near_own.at[1, near_tail], 1, 1)
    via_mid = via_copy(0, mid_own.at[1], via_held)
    onward_even = mid_copy(0, 4, via_held, 1, 3)
    onward_odd = mid_copy(1, 3, via_held, 1, 3)
    relay_key = mid_copy(0, 1, mid_held.at[1, 0], 0, 2)
    relay_value = mid_copy(0, 1, mid_held.at[1, 1], 1, 2)

    even = lax.rem(me, 2) == 0
    odd = jnp.logical_not(even)
    sends_one = me + 1 < n
    sends_two = even & (me + 2 < n)
    relays = even & (me >= 1)
    above = me + 4 - lax.rem(me, 4) < n
    crosses = (lax.rem(me, 4) >= 2) & above
    stays = jnp.logical_not(crosses)
    forwards = (lax.rem(me, 4) < 2) & above
    direct = sends_one & jnp.logical_not(crosses & odd)

    pair = moved(to_classes, project(2, 4))
    mid_own[0] = pair[:, :width]
    mid_own[1] = pair[:, width:]

    @pl.when(crosses)
    def _():
        via_mid.start()

    pair = moved(to_scattered, project(4, 6))
    second_send[...] = pair[:, :width]
    near_query[...] = pair[:, width:]
    each(lambda k: far_copy(second_send, second_held, second_sem, k).start())
    second_held[at_rows(me), :] = second_send[at_rows(me), :]
    wo_load.start()

    @pl.when(sends_two & stays)
    def _():
        key_two.start()
        value_two.start()

    @pl.when(direct)
    def _():
        key_one.start()
        value_one.start()

    pair = project(6, 8)
    near_own[0] = pair[:, :width]
    near_own[1] = pair[:, width:]

    @pl.when(direct)
    def _():
        near_key.start()
        near_value.start()

    @pl.when(crosses & even)
    def _():
        key_two.start()

    @pl.when(crosses & odd)
    def _():
        near_key.start()
        near_value.start()
        key_one.start()

    mid_query[...] = moved(to_scattered, project(8, 9))

    def slope_of(head, window):
        number = tp * local_heads + head
        slope = jnp.float32(0.0)
        for index in range(HEADS):
            value = 2.0 ** (3.0 - 8.0 * (index + 1.0) / HEADS) / window
            slope = jnp.where(number == index, jnp.float32(value), slope)
        return slope

    def grid(row_count, key_count):
        row = lax.broadcasted_iota(jnp.int32, (row_count, key_count), 0)
        column = lax.broadcasted_iota(jnp.int32, (row_count, key_count), 1)
        return row, column

    row, column = grid(rows, rows)
    apart = scatter_token(row) - column
    valid = (apart >= 0) & (apart <= NEAR_WINDOW)
    distance = apart.astype(jnp.float32)
    near = []
    for head in range(local_heads):
        at = pl.ds(head * HEAD_DIM, HEAD_DIM)
        highest, weights, total = weigh(
            scores_of(near_query[:, at], near_own[0, :, at]), slope_of(head, NEAR_WINDOW), distance, valid
        )
        near_sum[head] = apply(weights, near_own[1, :, at])
        near.append((highest, total))

    @pl.when(forwards)
    def _():
        via_mid.wait_recv()

    @pl.when(forwards & even)
    def _():
        onward_even.start()

    @pl.when(forwards & odd)
    def _():
        onward_odd.start()

    far_whole(first_send, first_held, first_sem).wait_recv()
    far_whole(second_send, second_held, second_sem).wait_recv()

    row, column = grid(rows, rows)
    apart = row - column
    valid = (apart >= 0) & (apart <= FAR_WINDOW // FAR_DILATION)
    distance = (apart * FAR_DILATION).astype(jnp.float32)
    lane = lax.broadcasted_iota(jnp.int32, (rows, HEAD_DIM), 1)
    slot = lax.broadcasted_iota(jnp.int32, (rows, HEAD_DIM), 0) & (chunk - 1)
    packed = jnp.zeros((rows, HEAD_DIM), jnp.float32)

    def far_part(head, part):
        place = head * 3 + part
        if place < 2 * local_heads:
            return first_held[:, place * HEAD_DIM : (place + 1) * HEAD_DIM]
        place -= 2 * local_heads
        return second_held[:, place * HEAD_DIM : (place + 1) * HEAD_DIM]

    for head in range(local_heads):
        highest, weights, total = weigh(
            scores_of(far_part(head, 0), far_part(head, 1)), slope_of(head, FAR_WINDOW), distance, valid
        )
        packed = jnp.where(lane == head * chunk + slot, highest + jnp.log(total), packed)
        back_send[:, head * HEAD_DIM : (head + 1) * HEAD_DIM] = apply(
            weights * (1.0 / total), far_part(head, 2)
        ).astype(jnp.bfloat16)
    log_send[...] = jnp.sum(packed.reshape(n, chunk, HEAD_DIM), axis=1, keepdims=True)

    def send_back(k):
        log_copy(k).start()
        back_copy(k).start()

    each(send_back)
    log_held[me] = log_send[me]
    back_held[at_rows(me), :] = back_send[at_rows(me), :]

    @pl.when(me >= 1)
    def _():
        near_key.wait_recv()
        near_value.wait_recv()
        key_one.wait_recv()
        value_one.wait_recv()

    @pl.when(relays)
    def _():
        relay_key.start()
        relay_value.start()

    row, column = grid(rows, NEAR_WINDOW)
    apart = scatter_token(row) + NEAR_WINDOW - column
    valid = (apart >= 0) & (apart <= NEAR_WINDOW) & (column + me * rows >= NEAR_WINDOW)
    distance = apart.astype(jnp.float32)
    for head in range(local_heads):
        at = pl.ds(head * HEAD_DIM, HEAD_DIM)
        own_high, own_total = near[head]
        high, weights, total = weigh(
            scores_of(near_query[:, at], near_held[0, :, at]), slope_of(head, NEAR_WINDOW), distance, valid
        )
        highest = jnp.maximum(own_high, high)
        own_share, share = jnp.exp(own_high - highest), jnp.exp(high - highest)
        near_sum[head] = near_sum[head] * own_share + apply(weights, near_held[1, :, at]) * share
        near[head] = (highest, own_total * own_share + total * share)

    @pl.when(me >= 2)
    def _():
        key_two.wait_recv()
        value_two.wait_recv()

    keys = MIDDLE_WINDOW // classes + stretch
    row, column = grid(rows, keys)
    apart = (row % chunk) * members + (row // chunk) % members + MIDDLE_WINDOW // classes - column
    valid = (apart >= 0) & (apart <= MIDDLE_WINDOW // classes)
    valid = valid & (column + me * stretch >= MIDDLE_WINDOW // classes)
    distance = (apart * classes).astype(jnp.float32)

    def class_rows(part, group, at):
        of_class = pl.ds(group * stretch, stretch)
        return jnp.concatenate(
            (mid_held[0, part, of_class, at], mid_held[1, part, of_class, at], mid_own[part, of_class, at]), axis=0
        )

    for head in range(local_heads):
        at = pl.ds(head * HEAD_DIM, HEAD_DIM)
        scores = jnp.concatenate([
            scores_of(mid_query[group * stretch : (group + 1) * stretch, at], class_rows(0, group, at))
            for group in range(classes)
        ], axis=0)
        high, weights, total = weigh(scores, slope_of(head, MIDDLE_WINDOW), distance, valid)
        middle = jnp.concatenate([
            apply(weights[group * stretch : (group + 1) * stretch], class_rows(1, group, at))
            for group in range(classes)
        ], axis=0)
        near_high, near_total = near[head]
        highest = jnp.maximum(near_high, high)
        near_share, share = jnp.exp(near_high - highest), jnp.exp(high - highest)
        base[head] = near_sum[head] * near_share + middle * share
        stats[2 * head] = highest
        stats[2 * head + 1] = near_total * near_share + total * share

    def merged_copy(group):
        place = pl.ds(pl.multiple_of(group * members * chunk, members * chunk), members * chunk)
        return pltpu.make_async_remote_copy(
            src_ref=merged_own.at[place],
            dst_ref=merged_held.at[place],
            send_sem=merged_ssem.at[group],
            recv_sem=merged_rsem.at[group],
            device_id=(me, peer),
            device_id_type=MESH,
        )

    block = members * chunk
    lane = lax.broadcasted_iota(jnp.int32, (block, HEAD_DIM), 1)
    slot = lax.broadcasted_iota(jnp.int32, (block, HEAD_DIM), 0) & (chunk - 1)
    for step in range(n // members):
        group = lax.rem(plane + step, n // members)
        count = members - 1 if step == 0 else members
        log_whole(count, group).wait_recv()
        back_whole(count, group).wait_recv()
        place = pl.ds(pl.multiple_of(group * block, block), block)
        held = log_held[pl.ds(group * members, members)]
        spread = jnp.broadcast_to(held, (members, chunk, HEAD_DIM)).reshape(block, HEAD_DIM)
        split = jnp.zeros((block, HEAD_DIM), jnp.float32)
        for head in range(local_heads):
            at = pl.ds(head * HEAD_DIM, HEAD_DIM)
            far_log = jnp.sum(
                jnp.where(lane == head * chunk + slot, spread, 0.0), axis=-1, keepdims=True
            )
            pair_log, pair_sum = stats[2 * head, place], stats[2 * head + 1, place]
            highest = jnp.maximum(pair_log, far_log)
            pair_share, far_share = jnp.exp(pair_log - highest), jnp.exp(far_log - highest)
            mass = pair_sum * pair_share + far_share
            inverse = 1.0 / mass
            merged = base[head, place] * (pair_share * inverse)
            merged = merged + back_held[place, at].astype(jnp.float32) * (far_share * inverse)
            merged_own[place, at] = merged.astype(jnp.bfloat16)
            rest = highest + jnp.log(mass)
            for term in range(3):
                piece = rest.astype(jnp.bfloat16).astype(jnp.float32)
                split = jnp.where(lane == 3 * head + term, piece, split)
                rest = rest - piece
        terms[place] = split.astype(jnp.bfloat16)
        merged_copy(group).start()

    lane = lax.broadcasted_iota(jnp.int32, (rows, HEAD_DIM), 1)
    totals = jnp.dot(to_tokens, terms[...], preferred_element_type=jnp.float32)
    summed = jnp.zeros((rows, HEAD_DIM), jnp.float32)
    for head in range(local_heads):
        total = jnp.sum(
            jnp.where((lane >= 3 * head) & (lane < 3 * head + 3), totals, 0.0), axis=-1, keepdims=True
        )
        summed = jnp.where(lane == head, total, summed)
    totals_ref[...] = summed
    wo_load.wait()
    partial_ref[...] = jnp.dot(
        moved(to_tokens, merged_own[...]), wo[pl.ds(pl.multiple_of(tp * width, width), width), :],
        preferred_element_type=jnp.float32,
    )

    far_whole(first_send, first_held, first_sem).wait_send()
    far_whole(second_send, second_held, second_sem).wait_send()
    log_whole(n - 1, 0).wait_send()
    back_whole(n - 1, 0).wait_send()

    @pl.when(crosses)
    def _():
        via_mid.wait_send()

    @pl.when(sends_two)
    def _():
        key_two.wait_send()

    @pl.when(sends_two & stays)
    def _():
        value_two.wait_send()

    @pl.when(sends_one)
    def _():
        key_one.wait_send()
        near_key.wait_send()
        near_value.wait_send()

    @pl.when(direct)
    def _():
        value_one.wait_send()

    @pl.when(forwards & even)
    def _():
        onward_even.wait_send()

    @pl.when(forwards & odd)
    def _():
        onward_odd.wait_send()

    @pl.when(relays)
    def _():
        relay_key.wait_send()
        relay_value.wait_send()

    for group in range(n // members):
        merged_copy(group).wait_recv()
    peer_ref[...] = moved(to_tokens, merged_held[...])
    for group in range(n // members):
        merged_copy(group).wait_send()


def mix(partial_ref, peer_ref, totals_ref, wo_ref, mixed_hbm, log_ref, out, sem):
    width = peer_ref.shape[1]
    steps = out.shape[0]
    piece = out.shape[2]
    at = pl.ds(pl.multiple_of((1 - lax.axis_index("tp")) * width, width), width)
    copies = []
    for step in range(steps):
        columns = pl.ds(step * piece, piece)
        product = jnp.dot(peer_ref[...], wo_ref[at, columns], preferred_element_type=jnp.float32)
        out[step] = (partial_ref[:, columns] + product).astype(jnp.bfloat16)
        copies.append(pltpu.make_async_copy(out.at[step], mixed_hbm.at[:, columns], sem.at[step]))
        copies[-1].start()
    log_ref[...] = jnp.transpose(totals_ref[...])[: log_ref.shape[0]]
    for copy in copies:
        copy.wait()


def fused(n, tokens, query_weight, key_weight, value_weight, out_weight):
    rows, depth = tokens.shape
    columns = query_weight.shape[1]
    out_columns = out_weight.shape[1]
    local_heads = columns // (3 * HEAD_DIM)
    width = local_heads * HEAD_DIM
    planes = MIDDLE_DILATION
    dma = pltpu.SemaphoreType.DMA
    half = jnp.bfloat16
    full = jnp.float32
    whole = pl.BlockSpec(memory_space=pltpu.VMEM)
    anywhere = pl.BlockSpec(memory_space=pl.ANY)
    partial, peer, totals = pl.pallas_call(
        functools.partial(kernel, n, local_heads),
        out_shape=(
            jax.ShapeDtypeStruct((rows, out_columns), full),
            jax.ShapeDtypeStruct((rows, width), half),
            jax.ShapeDtypeStruct((rows, HEAD_DIM), full),
        ),
        in_specs=[anywhere] * 5,
        out_specs=(whole, whole, whole),
        scratch_shapes=[
            pltpu.VMEM((rows, depth), half),
            pltpu.VMEM((depth, 3 * columns), half),
            pltpu.VMEM(out_weight.shape, half),
            pltpu.VMEM((rows, 2 * width), half),
            pltpu.VMEM((rows, 2 * width), half),
            pltpu.VMEM((rows, width), half),
            pltpu.VMEM((rows, width), half),
            pltpu.VMEM((rows, width), half),
            pltpu.VMEM((rows, width), half),
            pltpu.VMEM((n, 1, HEAD_DIM), full),
            pltpu.VMEM((n, 1, HEAD_DIM), full),
            pltpu.VMEM((rows, width), half),
            pltpu.VMEM((2, rows, width), half),
            pltpu.VMEM((2, 2, rows, width), half),
            pltpu.VMEM((rows, width), half),
            pltpu.VMEM((rows, width), half),
            pltpu.VMEM((2, rows, width), half),
            pltpu.VMEM((2, NEAR_WINDOW, width), half),
            pltpu.VMEM((local_heads, rows, HEAD_DIM), full),
            pltpu.VMEM((2 * local_heads, rows, 1), full),
            pltpu.VMEM((rows, HEAD_DIM), half),
            pltpu.VMEM((rows, width), half),
            pltpu.VMEM((rows, width), half),
            pltpu.VMEM((local_heads, rows, HEAD_DIM), full),
            dma((2 + 9 * local_heads,)),
            dma((2,)), dma((2,)), dma(()), dma((planes,)), dma(()), dma((planes,)),
            dma((4, 2)), dma((2, 2)), dma((1,)), dma((1,)), dma((2,)), dma((2,)), dma((planes,)), dma((planes,)),
        ],
        compiler_params=pltpu.CompilerParams(
            collective_id=0, has_side_effects=True, vmem_limit_bytes=53000 * 1024
        ),
    )(tokens, query_weight, key_weight, value_weight, out_weight)
    pieces = out_columns // width
    return pl.pallas_call(
        mix,
        out_shape=(
            jax.ShapeDtypeStruct((rows, out_columns), half),
            jax.ShapeDtypeStruct((local_heads, rows), full),
        ),
        in_specs=[whole] * 4,
        out_specs=(anywhere, whole),
        scratch_shapes=[pltpu.VMEM((pieces, rows, width), half), dma((pieces,))],
        compiler_params=pltpu.CompilerParams(vmem_limit_bytes=16000 * 1024),
    )(partial, peer, totals, out_weight)


def solution(mesh):
    n, n_tp = mesh.shape["sp"], mesh.shape["tp"]
    if n == FAR_DILATION and n_tp == 2:
        body = functools.partial(fused, n)
    else:
        body = local
    return jax.shard_map(
        body,
        mesh=mesh,
        in_specs=(P("sp", None), P(None, "tp"), P(None, "tp"), P(None, "tp"), P(None, "tp")),
        out_specs=(P("sp", "tp"), P("tp", "sp")),
        check_vma=False,
    )
```

time: 36.4 us -> 30.1 us (0.83)
  Pallas kernels: 34 us -> 28.9 us
  local copies, waits for them, and re-layouts: 1.22 us -> 0.01 us
    pallas_call x1, Pallas kernels: 32.4 us -> 27.3 us  [fused(): pl.pallas_call(functools.partial(kernel, n, local_heads), out_shape=(jax....]
    unnamed x4 -> x2, local copies, waits for them, and re-layouts: 1.22 us -> 0.01 us
where the time goes in v2:
time: 30.1 us; the launch traced here: 29.6 us
  Pallas kernels  28.9 us (96%)
  between operations  0.65 us (2%)
    pallas_call x1, Pallas kernels, fused(): pl.pallas_call(functools.partial(kernel, n, local_heads), out_shape=(jax....  27.3 us
    pallas_call x1, Pallas kernels, fused(): pl.pallas_call(mix, out_shape=(jax.ShapeDtypeStruct((rows, out_columns),...  1.64 us

profile of v2, /device:TPU:16, one launch (start us, length us, event | category | flops | bytes accessed | tf_op | source)
XLA Modules:
  0.0 29.6 jit_solution(13463007132476997098)
XLA Ops:
  0.6 0.0 copy-start
  0.6 27.3 %shard_map.68 = (f32[256,1024]{1,0:T(8,128)S(1)}, bf16[256,256]{1,0:T(8,128)(2,1)S(1)}, f32[256,128]{1,0:T(8,128)S(1)}) custom-call(bf16[256,2048]{1,0:T(8,128)(2,1)} %tok_hbm.1, bf16[2048,768]{1,0:T(8,128)(2,1)} %wq_hbm.1, bf16[2048,768]{1,0:T(8,128)(2,1)} %wk_hbm.1, bf16[2048,768]{1,0:T(8,128)(2,1)} %wv_hbm.1, bf16[512,1024]{1,0:T(8,128)(2,1)} %wo_ref.1), custom_call_target="tpu_custom_call" | custom-call | tf_op jit(solution)/shard_map/pallas_call | solution.py:715
  27.9 0.0 copy-done
  28.0 1.6 %shard_map.69 = (bf16[256,1024]{1,0:T(8,128)(2,1)}, f32[2,256]{1,0:T(2,128)}) custom-call(f32[256,1024]{1,0:T(8,128)S(1)} %get-tuple-element.5.partial_ref, bf16[256,256]{1,0:T(8,128)(2,1)S(1)} %get-tuple-element.6.peer_ref, f32[256,128]{1,0:T(8,128)S(1)} %get-tuple-element.7.totals_ref, bf16[512,1024]{1,0:T(8,128)(2,1)S(1)} %copy-done), custom_call_target="tpu_custom_call" | custom-call | tf_op jit(solution)/shard_map/pallas_call | solution.py:758
Async XLA Ops:
  0.6 27.3 %copy-start = (bf16[512,1024]{1,0:T(8,128)(2,1)S(1)}, bf16[512,1024]{1,0:T(8,128)(2,1)}, u32[]{:S(2)}) copy-start(bf16[512,1024]{1,0:T(8,128)(2,1)} %wo_ref.1) | copy-start | bytes 3145732

commit v3 on v2

--- a/solution.py
+++ b/solution.py
@@ -170,7 +170,7 @@
     partial_ref, peer_ref, totals_ref,
     tok, weight, wo, first_send, first_held, second_send, second_held, back_send, back_held, log_send, log_held,
     mid_query, mid_own, mid_held, via_held, near_query, near_own, near_held,
-    base, stats, terms, merged_own, merged_held, near_sum,
+    stats, terms, merged_own, merged_held, near_sum,
     load_sem, first_sem, second_sem, back_ssem, back_rsem, log_ssem, log_rsem,
     mid_ssem, mid_rsem, via_ssem, via_rsem, near_ssem, near_rsem, merged_ssem, merged_rsem,
 ):
@@ -200,8 +200,9 @@
             weight.at[:, pl.ds(place * HEAD_DIM, HEAD_DIM)],
             load_sem.at[2 + place],
         ))
+    first = 2 * local_heads
     early = 4 * local_heads
-    for copy in loads[:early]:
+    for copy in loads[:first]:
         copy.start()
 
     barrier = pltpu.get_barrier_semaphore()
@@ -212,6 +213,8 @@
 
     lax.fori_loop(1, n, greet, 0)
     pl.semaphore_signal(barrier, inc=1, device_id=(me, peer), device_id_type=MESH)
+    for copy in loads[first:early]:
+        copy.start()
 
     @pl.when(me < 2)
     def _():
@@ -220,7 +223,6 @@
     @pl.when(me < 1)
     def _():
         mid_held[1] = jnp.zeros((2, rows, width), jnp.bfloat16)
-        near_held[...] = jnp.zeros((2, NEAR_WINDOW, width), jnp.bfloat16)
 
     def project(first, last):
         for copy in loads[first * local_heads : last * local_heads]:
@@ -434,9 +436,9 @@
 
     @pl.when(crosses & odd)
     def _():
+        key_one.start()
         near_key.start()
         near_value.start()
-        key_one.start()
 
     mid_query[...] = moved(to_scattered, project(8, 9))
 
@@ -457,14 +459,14 @@
     apart = scatter_token(row) - column
     valid = (apart >= 0) & (apart <= NEAR_WINDOW)
     distance = apart.astype(jnp.float32)
-    near = []
     for head in range(local_heads):
         at = pl.ds(head * HEAD_DIM, HEAD_DIM)
         highest, weights, total = weigh(
             scores_of(near_query[:, at], near_own[0, :, at]), slope_of(head, NEAR_WINDOW), distance, valid
         )
         near_sum[head] = apply(weights, near_own[1, :, at])
-        near.append((highest, total))
+        stats[2 * head] = highest
+        stats[2 * head + 1] = total
 
     @pl.when(forwards)
     def _():
@@ -514,32 +516,38 @@
     log_held[me] = log_send[me]
     back_held[at_rows(me), :] = back_send[at_rows(me), :]
 
-    @pl.when(me >= 1)
-    def _():
+    def near_rest():
         near_key.wait_recv()
         near_value.wait_recv()
+        row, column = grid(rows, NEAR_WINDOW)
+        apart = scatter_token(row) + NEAR_WINDOW - column
+        valid = (apart >= 0) & (apart <= NEAR_WINDOW)
+        distance = apart.astype(jnp.float32)
+        for head in range(local_heads):
+            at = pl.ds(head * HEAD_DIM, HEAD_DIM)
+            high, weights, total = weigh(
+                scores_of(near_query[:, at], near_held[0, :, at]), slope_of(head, NEAR_WINDOW), distance, valid
+            )
+            own_high = stats[2 * head]
+            highest = jnp.maximum(own_high, high)
+            own_share, share = jnp.exp(own_high - highest), jnp.exp(high - highest)
+            near_sum[head] = near_sum[head] * own_share + apply(weights, near_held[1, :, at]) * share
+            stats[2 * head] = highest
+            stats[2 * head + 1] = stats[2 * head + 1] * own_share + total * share
+
+    @pl.when(odd)
+    def _():
+        near_rest()
+
+    @pl.when(me >= 1)
+    def _():
+        value_one.wait_recv()
         key_one.wait_recv()
-        value_one.wait_recv()
 
     @pl.when(relays)
     def _():
+        relay_value.start()
         relay_key.start()
-        relay_value.start()
-
-    row, column = grid(rows, NEAR_WINDOW)
-    apart = scatter_token(row) + NEAR_WINDOW - column
-    valid = (apart >= 0) & (apart <= NEAR_WINDOW) & (column + me * rows >= NEAR_WINDOW)
-    distance = apart.astype(jnp.float32)
-    for head in range(local_heads):
-        at = pl.ds(head * HEAD_DIM, HEAD_DIM)
-        own_high, own_total = near[head]
-        high, weights, total = weigh(
-            scores_of(near_query[:, at], near_held[0, :, at]), slope_of(head, NEAR_WINDOW), distance, valid
-        )
-        highest = jnp.maximum(own_high, high)
-        own_share, share = jnp.exp(own_high - highest), jnp.exp(high - highest)
-        near_sum[head] = near_sum[head] * own_share + apply(weights, near_held[1, :, at]) * share
-        near[head] = (highest, own_total * own_share + total * share)
 
     @pl.when(me >= 2)
     def _():
@@ -570,12 +578,16 @@
             apply(weights[group * stretch : (group + 1) * stretch], class_rows(1, group, at))
             for group in range(classes)
         ], axis=0)
-        near_high, near_total = near[head]
+        near_high = stats[2 * head]
         highest = jnp.maximum(near_high, high)
         near_share, share = jnp.exp(near_high - highest), jnp.exp(high - highest)
-        base[head] = near_sum[head] * near_share + middle * share
+        near_sum[head] = near_sum[head] * near_share + middle * share
         stats[2 * head] = highest
-        stats[2 * head + 1] = near_total * near_share + total * share
+        stats[2 * head + 1] = stats[2 * head + 1] * near_share + total * share
+
+    @pl.when(even & (me >= 1))
+    def _():
+        near_rest()
 
     def merged_copy(group):
         place = pl.ds(pl.multiple_of(group * members * chunk, members * chunk), members * chunk)
@@ -610,7 +622,7 @@
             pair_share, far_share = jnp.exp(pair_log - highest), jnp.exp(far_log - highest)
             mass = pair_sum * pair_share + far_share
             inverse = 1.0 / mass
-            merged = base[head, place] * (pair_share * inverse)
+            merged = near_sum[head, place] * (pair_share * inverse)
             merged = merged + back_held[place, at].astype(jnp.float32) * (far_share * inverse)
             merged_own[place, at] = merged.astype(jnp.bfloat16)
             rest = highest + jnp.log(mass)
@@ -683,21 +695,12 @@
         merged_copy(group).wait_send()
 
 
-def mix(partial_ref, peer_ref, totals_ref, wo_ref, mixed_hbm, log_ref, out, sem):
+def mix(partial_ref, peer_ref, totals_ref, wo_ref, mixed_ref, log_ref):
     width = peer_ref.shape[1]
-    steps = out.shape[0]
-    piece = out.shape[2]
     at = pl.ds(pl.multiple_of((1 - lax.axis_index("tp")) * width, width), width)
-    copies = []
-    for step in range(steps):
-        columns = pl.ds(step * piece, piece)
-        product = jnp.dot(peer_ref[...], wo_ref[at, columns], preferred_element_type=jnp.float32)
-        out[step] = (partial_ref[:, columns] + product).astype(jnp.bfloat16)
-        copies.append(pltpu.make_async_copy(out.at[step], mixed_hbm.at[:, columns], sem.at[step]))
-        copies[-1].start()
+    product = jnp.dot(peer_ref[...], wo_ref[at], preferred_element_type=jnp.float32)
+    mixed_ref[...] = (partial_ref[...] + product).astype(jnp.bfloat16)
     log_ref[...] = jnp.transpose(totals_ref[...])[: log_ref.shape[0]]
-    for copy in copies:
-        copy.wait()
 
 
 def fused(n, tokens, query_weight, key_weight, value_weight, out_weight):
@@ -740,7 +743,6 @@
             pltpu.VMEM((rows, width), half),
             pltpu.VMEM((2, rows, width), half),
             pltpu.VMEM((2, NEAR_WINDOW, width), half),
-            pltpu.VMEM((local_heads, rows, HEAD_DIM), full),
             pltpu.VMEM((2 * local_heads, rows, 1), full),
             pltpu.VMEM((rows, HEAD_DIM), half),
             pltpu.VMEM((rows, width), half),
@@ -754,7 +756,6 @@
             collective_id=0, has_side_effects=True, vmem_limit_bytes=53000 * 1024
         ),
     )(tokens, query_weight, key_weight, value_weight, out_weight)
-    pieces = out_columns // width
     return pl.pallas_call(
         mix,
         out_shape=(
@@ -762,8 +763,7 @@
             jax.ShapeDtypeStruct((local_heads, rows), full),
         ),
         in_specs=[whole] * 4,
-        out_specs=(anywhere, whole),
-        scratch_shapes=[pltpu.VMEM((pieces, rows, width), half), dma((pieces,))],
+        out_specs=(whole, whole),
         compiler_params=pltpu.CompilerParams(vmem_limit_bytes=16000 * 1024),
     )(partial, peer, totals, out_weight)
 

time: 30.1 us -> 29.1 us (0.967)
  the two profiles are of different devices: /device:TPU:16 before, /device:TPU:0 now
where the time goes in v3:
time: 29.1 us; the launch traced here: 28.9 us
  Pallas kernels  28.3 us (97%)
  between operations  0.65 us (2%)
    pallas_call x1, Pallas kernels, fused(): pl.pallas_call(functools.partial(kernel, n, local_heads), out_shape=(jax....  27.2 us
    pallas_call x1, Pallas kernels, fused(): pl.pallas_call(mix, out_shape=(jax.ShapeDtypeStruct((rows, out_columns),...  1.11 us

profile of v3, /device:TPU:0, one launch (start us, length us, event | category | flops | bytes accessed | tf_op | source)
XLA Modules:
  0.0 28.9 jit_solution(11554038181314015917)
XLA Ops:
  0.6 0.0 copy-start
  0.6 27.2 %shard_map.68 = (f32[256,1024]{1,0:T(8,128)S(1)}, bf16[256,256]{1,0:T(8,128)(2,1)S(1)}, f32[256,128]{1,0:T(8,128)S(1)}) custom-call(bf16[256,2048]{1,0:T(8,128)(2,1)} %tok_hbm.1, bf16[2048,768]{1,0:T(8,128)(2,1)} %wq_hbm.1, bf16[2048,768]{1,0:T(8,128)(2,1)} %wk_hbm.1, bf16[2048,768]{1,0:T(8,128)(2,1)} %wv_hbm.1, bf16[512,1024]{1,0:T(8,128)(2,1)} %wo_ref.1), custom_call_target="tpu_custom_call" | custom-call | tf_op jit(solution)/shard_map/pallas_call | solution.py:718
  27.8 0.0 copy-done
  27.8 1.1 %shard_map.69 = (bf16[256,1024]{1,0:T(8,128)(2,1)}, f32[2,256]{1,0:T(2,128)}) custom-call(f32[256,1024]{1,0:T(8,128)S(1)} %get-tuple-element.5.partial_ref, bf16[256,256]{1,0:T(8,128)(2,1)S(1)} %get-tuple-element.6.peer_ref, f32[256,128]{1,0:T(8,128)S(1)} %get-tuple-element.7.totals_ref, bf16[512,1024]{1,0:T(8,128)(2,1)S(1)} %copy-done), custom_call_target="tpu_custom_call" | custom-call | tf_op jit(solution)/shard_map/pallas_call | solution.py:759
Async XLA Ops:
  0.6 27.2 %copy-start = (bf16[512,1024]{1,0:T(8,128)(2,1)S(1)}, bf16[512,1024]{1,0:T(8,128)(2,1)}, u32[]{:S(2)}) copy-start(bf16[512,1024]{1,0:T(8,128)(2,1)} %wo_ref.1) | copy-start | bytes 3145732

commit v4 on v3

--- a/solution.py
+++ b/solution.py
@@ -158,9 +158,19 @@
     return jnp.dot(weights.astype(jnp.bfloat16), value, preferred_element_type=jnp.float32)
 
 
+def split_by(value, size):
+    shift = size.bit_length() - 1
+    return value >> shift, value & (size - 1)
+
+
+def grid(row_count, key_count):
+    row = lax.broadcasted_iota(jnp.int32, (row_count, 1), 0)
+    column = lax.broadcasted_iota(jnp.int32, (row_count, key_count), 1)
+    return row, column
+
+
 def one_hot(rows, token_of_row):
-    row = lax.broadcasted_iota(jnp.int32, (rows, rows), 0)
-    column = lax.broadcasted_iota(jnp.int32, (rows, rows), 1)
+    row, column = grid(rows, rows)
     return jnp.where(column == token_of_row(row), 1.0, 0.0).astype(jnp.bfloat16)
 
 
@@ -170,8 +180,8 @@
     partial_ref, peer_ref, totals_ref,
     tok, weight, wo, first_send, first_held, second_send, second_held, back_send, back_held, log_send, log_held,
     mid_query, mid_own, mid_held, via_held, near_query, near_own, near_held,
-    stats, terms, merged_own, merged_held, near_sum,
-    load_sem, first_sem, second_sem, back_ssem, back_rsem, log_ssem, log_rsem,
+    stats, merged_own, merged_held, near_sum,
+    load_sem, half_sem, first_sem, second_sem, back_ssem, back_rsem, log_ssem, log_rsem,
     mid_ssem, mid_rsem, via_ssem, via_rsem, near_ssem, near_rsem, merged_ssem, merged_rsem,
 ):
     me = lax.axis_index("sp")
@@ -185,25 +195,35 @@
     peer = 1 - tp
     sources = (wq_hbm, wk_hbm, wv_hbm)
 
-    tok_load = pltpu.make_async_copy(tok_hbm, tok, load_sem.at[0])
-    tok_load.start()
-    wo_load = pltpu.make_async_copy(wo_hbm, wo, load_sem.at[1])
+    depth = tok.shape[1]
+    halves = (pl.ds(0, depth // 2), pl.ds(depth // 2, depth // 2))
+    tok_loads = [
+        pltpu.make_async_copy(tok_hbm.at[:, part], tok.at[:, part], half_sem.at[side, 0])
+        for side, part in enumerate(halves)
+    ]
+    wo_load = pltpu.make_async_copy(wo_hbm, wo, load_sem.at[0])
     loads = []
     order = [(2, part, head) for head in range(local_heads) for part in range(3)]
     for group, part in ((0, 0), (0, 1), (0, 2), (1, 0)):
         order += [(group, part, head) for head in range(local_heads)]
     middle = [(1, part, head) for part in (1, 2) for head in range(local_heads)]
     order[2 * local_heads : 2 * local_heads] = middle
-    for place, (group, part, head) in enumerate(order):
-        loads.append(pltpu.make_async_copy(
-            sources[part].at[:, pl.ds((head * 3 + group) * HEAD_DIM, HEAD_DIM)],
-            weight.at[:, pl.ds(place * HEAD_DIM, HEAD_DIM)],
-            load_sem.at[2 + place],
-        ))
     first = 2 * local_heads
     early = 4 * local_heads
-    for copy in loads[:first]:
-        copy.start()
+    for place, (group, part, head) in enumerate(order):
+        source = sources[part].at[:, pl.ds((head * 3 + group) * HEAD_DIM, HEAD_DIM)]
+        target = weight.at[:, pl.ds(place * HEAD_DIM, HEAD_DIM)]
+        if place < first:
+            loads.append([
+                pltpu.make_async_copy(source.at[side], target.at[side], half_sem.at[index, 1 + place])
+                for index, side in enumerate(halves)
+            ])
+        else:
+            loads.append(pltpu.make_async_copy(source, target, load_sem.at[1 + place]))
+    for side in range(2):
+        tok_loads[side].start()
+        for copy in loads[:first]:
+            copy[side].start()
 
     barrier = pltpu.get_barrier_semaphore()
 
@@ -235,15 +255,18 @@
         return pl.ds(pl.multiple_of(index * chunk, chunk), chunk)
 
     def scatter_token(row):
-        group, index = row // chunk, row % chunk
-        return index * n + (group % members) * classes + group // members
+        group, index = split_by(row, chunk)
+        high, low = split_by(group, members)
+        return index * n + low * classes + high
 
     def gather_row(token):
-        index, residue = token // n, token % n
-        return ((residue % classes) * members + residue // classes) * chunk + index
+        index, residue = split_by(token, n)
+        high, low = split_by(residue, classes)
+        return (low * members + high) * chunk + index
 
     def class_token(row):
-        return (row % stretch) * classes + row // stretch
+        group, index = split_by(row, stretch)
+        return index * classes + group
 
     to_scattered = one_hot(rows, scatter_token)
     to_tokens = one_hot(rows, gather_row)
@@ -253,13 +276,9 @@
         return jnp.dot(matrix, block, preferred_element_type=jnp.float32).astype(jnp.bfloat16)
 
     def each(action):
-        def step(k, carry):
+        for k in range(1, n):
             action(k)
-            return carry
-
-        lax.fori_loop(1, n, step, 0)
-
-    plane = me // members
+
     upper = me // (n // 2)
 
     def target_of(k):
@@ -290,52 +309,58 @@
             device_id_type=MESH,
         )
 
-    def back_copy(k):
+    def back_copy(head, k):
         to = target_of(k)
         return pltpu.make_async_remote_copy(
-            src_ref=back_send.at[at_rows(to)],
-            dst_ref=back_held.at[at_rows(me)],
-            send_sem=back_ssem,
-            recv_sem=back_rsem.at[plane],
+            src_ref=back_send.at[head, at_rows(to)],
+            dst_ref=back_held.at[head, at_rows(me)],
+            send_sem=back_ssem.at[head],
+            recv_sem=back_rsem.at[head],
             device_id=(to, tp),
             device_id_type=MESH,
         )
 
-    def back_whole(count, group):
-        some = pl.ds(0, count * chunk)
-        return pltpu.make_async_remote_copy(
-            src_ref=back_send.at[some],
-            dst_ref=back_held.at[some],
-            send_sem=back_ssem,
-            recv_sem=back_rsem.at[group],
+    def back_whole(head):
+        others = pl.ds(0, rows - chunk)
+        return pltpu.make_async_remote_copy(
+            src_ref=back_send.at[head, others],
+            dst_ref=back_held.at[head, others],
+            send_sem=back_ssem.at[head],
+            recv_sem=back_rsem.at[head],
             device_id=(lax.rem(me + 1, n), tp),
             device_id_type=MESH,
         )
 
-    def log_copy(k):
+    def log_copy(head, k):
         to = target_of(k)
         return pltpu.make_async_remote_copy(
-            src_ref=log_send.at[to],
-            dst_ref=log_held.at[me],
-            send_sem=log_ssem,
-            recv_sem=log_rsem.at[plane],
+            src_ref=log_send.at[head, to],
+            dst_ref=log_held.at[head, me],
+            send_sem=log_ssem.at[head],
+            recv_sem=log_rsem.at[head],
             device_id=(to, tp),
             device_id_type=MESH,
         )
 
-    def log_whole(count, group):
-        some = pl.ds(0, count)
-        return pltpu.make_async_remote_copy(
-            src_ref=log_send.at[some],
-            dst_ref=log_held.at[some],
-            send_sem=log_ssem,
-            recv_sem=log_rsem.at[group],
+    def log_whole(head):
+        others = pl.ds(0, n - 1)
+        return pltpu.make_async_remote_copy(
+            src_ref=log_send.at[head, others],
+            dst_ref=log_held.at[head, others],
+            send_sem=log_ssem.at[head],
+            recv_sem=log_rsem.at[head],
             device_id=(lax.rem(me + 1, n), tp),
             device_id_type=MESH,
         )
 
-    tok_load.wait()
-    first_send[...] = moved(to_scattered, project(0, 2))
+    product = None
+    for side, part in enumerate(halves):
+        tok_loads[side].wait()
+        for copy in loads[:first]:
+            copy[side].wait()
+        term = jnp.dot(tok[:, part], weight[part, : 2 * width], preferred_element_type=jnp.float32)
+        product = term if product is None else product + term
+    first_send[...] = moved(to_scattered, product.astype(jnp.bfloat16))
     for copy in loads[early:]:
         copy.start()
     pl.semaphore_wait(barrier, n)
@@ -413,30 +438,28 @@
 
     @pl.when(sends_two & stays)
     def _():
+        value_two.start()
         key_two.start()
-        value_two.start()
 
     @pl.when(direct)
     def _():
+        value_one.start()
         key_one.start()
-        value_one.start()
+
+    @pl.when(crosses & even)
+    def _():
+        key_two.start()
+
+    @pl.when(crosses & odd)
+    def _():
+        key_one.start()
 
     pair = project(6, 8)
     near_own[0] = pair[:, :width]
     near_own[1] = pair[:, width:]
 
-    @pl.when(direct)
-    def _():
-        near_key.start()
-        near_value.start()
-
-    @pl.when(crosses & even)
-    def _():
-        key_two.start()
-
-    @pl.when(crosses & odd)
-    def _():
-        key_one.start()
+    @pl.when(sends_one)
+    def _():
         near_key.start()
         near_value.start()
 
@@ -450,71 +473,41 @@
             slope = jnp.where(number == index, jnp.float32(value), slope)
         return slope
 
-    def grid(row_count, key_count):
-        row = lax.broadcasted_iota(jnp.int32, (row_count, key_count), 0)
-        column = lax.broadcasted_iota(jnp.int32, (row_count, key_count), 1)
-        return row, column
-
     row, column = grid(rows, rows)
     apart = scatter_token(row) - column
     valid = (apart >= 0) & (apart <= NEAR_WINDOW)
     distance = apart.astype(jnp.float32)
-    for head in range(local_heads):
-        at = pl.ds(head * HEAD_DIM, HEAD_DIM)
-        highest, weights, total = weigh(
-            scores_of(near_query[:, at], near_own[0, :, at]), slope_of(head, NEAR_WINDOW), distance, valid
-        )
-        near_sum[head] = apply(weights, near_own[1, :, at])
-        stats[2 * head] = highest
-        stats[2 * head + 1] = total
-
-    @pl.when(forwards)
-    def _():
-        via_mid.wait_recv()
-
-    @pl.when(forwards & even)
-    def _():
-        onward_even.start()
-
-    @pl.when(forwards & odd)
-    def _():
-        onward_odd.start()
-
-    far_whole(first_send, first_held, first_sem).wait_recv()
-    far_whole(second_send, second_held, second_sem).wait_recv()
-
-    row, column = grid(rows, rows)
-    apart = row - column
-    valid = (apart >= 0) & (apart <= FAR_WINDOW // FAR_DILATION)
-    distance = (apart * FAR_DILATION).astype(jnp.float32)
-    lane = lax.broadcasted_iota(jnp.int32, (rows, HEAD_DIM), 1)
-    slot = lax.broadcasted_iota(jnp.int32, (rows, HEAD_DIM), 0) & (chunk - 1)
-    packed = jnp.zeros((rows, HEAD_DIM), jnp.float32)
-
-    def far_part(head, part):
-        place = head * 3 + part
-        if place < 2 * local_heads:
-            return first_held[:, place * HEAD_DIM : (place + 1) * HEAD_DIM]
-        place -= 2 * local_heads
-        return second_held[:, place * HEAD_DIM : (place + 1) * HEAD_DIM]
-
-    for head in range(local_heads):
-        highest, weights, total = weigh(
-            scores_of(far_part(head, 0), far_part(head, 1)), slope_of(head, FAR_WINDOW), distance, valid
-        )
-        packed = jnp.where(lane == head * chunk + slot, highest + jnp.log(total), packed)
-        back_send[:, head * HEAD_DIM : (head + 1) * HEAD_DIM] = apply(
-            weights * (1.0 / total), far_part(head, 2)
-        ).astype(jnp.bfloat16)
-    log_send[...] = jnp.sum(packed.reshape(n, chunk, HEAD_DIM), axis=1, keepdims=True)
-
-    def send_back(k):
-        log_copy(k).start()
-        back_copy(k).start()
-
-    each(send_back)
-    log_held[me] = log_send[me]
-    back_held[at_rows(me), :] = back_send[at_rows(me), :]
+    heads = [pl.ds(head * HEAD_DIM, HEAD_DIM) for head in range(local_heads)]
+
+    def join(parts):
+        held = [(stats[2 * head], stats[2 * head + 1], near_sum[head]) for head in range(local_heads)]
+        joined = []
+        for (high, total, part), (held_high, held_total, held_part) in zip(parts, held):
+            highest = jnp.maximum(held_high, high)
+            held_share, share = jnp.exp(held_high - highest), jnp.exp(high - highest)
+            joined.append((
+                highest, held_total * held_share + total * share, held_part * held_share + part * share
+            ))
+        keep(joined)
+
+    def keep(parts):
+        for head, (high, total, part) in enumerate(parts):
+            stats[2 * head] = high
+            stats[2 * head + 1] = total
+            near_sum[head] = part
+
+    def partial_of(query, key_value, slopes, distance, valid):
+        weighed = [
+            weigh(scores_of(query[:, at], key_value[0, :, at]), slope, distance, valid)
+            for at, slope in zip(heads, slopes)
+        ]
+        return [
+            (high, total, apply(weights, key_value[1, :, at]))
+            for at, (high, weights, total) in zip(heads, weighed)
+        ]
+
+    near_slopes = [slope_of(head, NEAR_WINDOW) for head in range(local_heads)]
+    keep(partial_of(near_query, near_own, near_slopes, distance, valid))
 
     def near_rest():
         near_key.wait_recv()
@@ -523,21 +516,68 @@
         apart = scatter_token(row) + NEAR_WINDOW - column
         valid = (apart >= 0) & (apart <= NEAR_WINDOW)
         distance = apart.astype(jnp.float32)
-        for head in range(local_heads):
-            at = pl.ds(head * HEAD_DIM, HEAD_DIM)
-            high, weights, total = weigh(
-                scores_of(near_query[:, at], near_held[0, :, at]), slope_of(head, NEAR_WINDOW), distance, valid
+        join(partial_of(near_query, near_held, near_slopes, distance, valid))
+
+    @pl.when(odd)
+    def _():
+        near_rest()
+
+    @pl.when(forwards)
+    def _():
+        via_mid.wait_recv()
+
+    @pl.when(forwards & even)
+    def _():
+        onward_even.start()
+
+    @pl.when(forwards & odd)
+    def _():
+        onward_odd.start()
+
+    far_whole(first_send, first_held, first_sem).wait_recv()
+
+    reach = FAR_WINDOW // FAR_DILATION
+    lane = lax.broadcasted_iota(jnp.int32, (rows, HEAD_DIM), 1)
+    slot = lax.broadcasted_iota(jnp.int32, (rows, HEAD_DIM), 0) & (chunk - 1)
+    of_slot = lane == slot
+
+    def far_part(head, part, first_row, last_row):
+        place = head * 3 + part
+        source = first_held
+        if place >= 2 * local_heads:
+            place -= 2 * local_heads
+            source = second_held
+        return source[first_row:last_row, place * HEAD_DIM : (place + 1) * HEAD_DIM]
+
+    for head in range(local_heads):
+        if head == local_heads - 1:
+            far_whole(second_send, second_held, second_sem).wait_recv()
+        logs = []
+        shares = []
+        for first_row, last_row in ((0, reach), (reach, rows)):
+            row, column = grid(last_row - first_row, last_row)
+            apart = row + first_row - column
+            highest, weights, total = weigh(
+                scores_of(far_part(head, 0, first_row, last_row), far_part(head, 1, 0, last_row)),
+                slope_of(head, FAR_WINDOW), (apart * FAR_DILATION).astype(jnp.float32),
+                (apart >= 0) & (apart <= reach),
             )
-            own_high = stats[2 * head]
-            highest = jnp.maximum(own_high, high)
-            own_share, share = jnp.exp(own_high - highest), jnp.exp(high - highest)
-            near_sum[head] = near_sum[head] * own_share + apply(weights, near_held[1, :, at]) * share
-            stats[2 * head] = highest
-            stats[2 * head + 1] = stats[2 * head + 1] * own_share + total * share
-
-    @pl.when(odd)
-    def _():
-        near_rest()
+            logs.append(highest + jnp.log(total))
+            shares.append(weights * (1.0 / total))
+        packed = jnp.where(of_slot, jnp.concatenate(logs, axis=0), 0.0)
+        log_send[head] = jnp.sum(packed.reshape(n, chunk, HEAD_DIM), axis=1, keepdims=True)
+        for (first_row, last_row), share in zip(((0, reach), (reach, rows)), shares):
+            back_send[head, first_row:last_row] = apply(
+                share, far_part(head, 2, 0, last_row)
+            ).astype(jnp.bfloat16)
+
+        def send_back(k):
+            log_copy(head, k).start()
+            back_copy(head, k).start()
+
+        each(send_back)
+        log_held[head, me] = log_send[head, me]
+        back_held[head, at_rows(me), :] = back_send[head, at_rows(me), :]
 
     @pl.when(me >= 1)
     def _():
@@ -556,7 +596,8 @@
 
     keys = MIDDLE_WINDOW // classes + stretch
     row, column = grid(rows, keys)
-    apart = (row % chunk) * members + (row // chunk) % members + MIDDLE_WINDOW // classes - column
+    group, index = split_by(row, chunk)
+    apart = index * members + split_by(group, members)[1] + MIDDLE_WINDOW // classes - column
     valid = (apart >= 0) & (apart <= MIDDLE_WINDOW // classes)
     valid = valid & (column + me * stretch >= MIDDLE_WINDOW // classes)
     distance = (apart * classes).astype(jnp.float32)
@@ -567,74 +608,57 @@
             (mid_held[0, part, of_class, at], mid_held[1, part, of_class, at], mid_own[part, of_class, at]), axis=0
         )
 
-    for head in range(local_heads):
-        at = pl.ds(head * HEAD_DIM, HEAD_DIM)
+    weighed = []
+    for head, at in enumerate(heads):
         scores = jnp.concatenate([
             scores_of(mid_query[group * stretch : (group + 1) * stretch, at], class_rows(0, group, at))
             for group in range(classes)
         ], axis=0)
-        high, weights, total = weigh(scores, slope_of(head, MIDDLE_WINDOW), distance, valid)
-        middle = jnp.concatenate([
+        weighed.append(weigh(scores, slope_of(head, MIDDLE_WINDOW), distance, valid))
+    join([
+        (high, total, jnp.concatenate([
             apply(weights[group * stretch : (group + 1) * stretch], class_rows(1, group, at))
             for group in range(classes)
-        ], axis=0)
-        near_high = stats[2 * head]
-        highest = jnp.maximum(near_high, high)
-        near_share, share = jnp.exp(near_high - highest), jnp.exp(high - highest)
-        near_sum[head] = near_sum[head] * near_share + middle * share
-        stats[2 * head] = highest
-        stats[2 * head + 1] = stats[2 * head + 1] * near_share + total * share
+        ], axis=0))
+        for at, (high, weights, total) in zip(heads, weighed)
+    ])
 
     @pl.when(even & (me >= 1))
     def _():
         near_rest()
 
-    def merged_copy(group):
-        place = pl.ds(pl.multiple_of(group * members * chunk, members * chunk), members * chunk)
-        return pltpu.make_async_remote_copy(
-            src_ref=merged_own.at[place],
-            dst_ref=merged_held.at[place],
-            send_sem=merged_ssem.at[group],
-            recv_sem=merged_rsem.at[group],
+    def merged_copy(head):
+        return pltpu.make_async_remote_copy(
+            src_ref=merged_own.at[head],
+            dst_ref=merged_held.at[head],
+            send_sem=merged_ssem.at[head],
+            recv_sem=merged_rsem.at[head],
             device_id=(me, peer),
             device_id_type=MESH,
         )
 
-    block = members * chunk
-    lane = lax.broadcasted_iota(jnp.int32, (block, HEAD_DIM), 1)
-    slot = lax.broadcasted_iota(jnp.int32, (block, HEAD_DIM), 0) & (chunk - 1)
-    for step in range(n // members):
-        group = lax.rem(plane + step, n // members)
-        count = members - 1 if step == 0 else members
-        log_whole(count, group).wait_recv()
-        back_whole(count, group).wait_recv()
-        place = pl.ds(pl.multiple_of(group * block, block), block)
-        held = log_held[pl.ds(group * members, members)]
-        spread = jnp.broadcast_to(held, (members, chunk, HEAD_DIM)).reshape(block, HEAD_DIM)
-        split = jnp.zeros((block, HEAD_DIM), jnp.float32)
-        for head in range(local_heads):
-            at = pl.ds(head * HEAD_DIM, HEAD_DIM)
-            far_log = jnp.sum(
-                jnp.where(lane == head * chunk + slot, spread, 0.0), axis=-1, keepdims=True
-            )
-            pair_log, pair_sum = stats[2 * head, place], stats[2 * head + 1, place]
-            highest = jnp.maximum(pair_log, far_log)
-            pair_share, far_share = jnp.exp(pair_log - highest), jnp.exp(far_log - highest)
-            mass = pair_sum * pair_share + far_share
-            inverse = 1.0 / mass
-            merged = near_sum[head, place] * (pair_share * inverse)
-            merged = merged + back_held[place, at].astype(jnp.float32) * (far_share * inverse)
-            merged_own[place, at] = merged.astype(jnp.bfloat16)
-            rest = highest + jnp.log(mass)
-            for term in range(3):
-                piece = rest.astype(jnp.bfloat16).astype(jnp.float32)
-                split = jnp.where(lane == 3 * head + term, piece, split)
-                rest = rest - piece
-        terms[place] = split.astype(jnp.bfloat16)
-        merged_copy(group).start()
-
-    lane = lax.broadcasted_iota(jnp.int32, (rows, HEAD_DIM), 1)
-    totals = jnp.dot(to_tokens, terms[...], preferred_element_type=jnp.float32)
+    split = jnp.zeros((rows, HEAD_DIM), jnp.float32)
+    for head in range(local_heads):
+        log_whole(head).wait_recv()
+        spread = jnp.broadcast_to(log_held[head], (n, chunk, HEAD_DIM)).reshape(rows, HEAD_DIM)
+        far_log = jnp.sum(jnp.where(of_slot, spread, 0.0), axis=-1, keepdims=True)
+        pair_log, pair_sum = stats[2 * head], stats[2 * head + 1]
+        highest = jnp.maximum(pair_log, far_log)
+        pair_share, far_share = jnp.exp(pair_log - highest), jnp.exp(far_log - highest)
+        mass = pair_sum * pair_share + far_share
+        inverse = 1.0 / mass
+        back_whole(head).wait_recv()
+        merged = near_sum[head] * (pair_share * inverse)
+        merged = merged + back_held[head].astype(jnp.float32) * (far_share * inverse)
+        merged_own[head] = merged.astype(jnp.bfloat16)
+        merged_copy(head).start()
+        rest = highest + jnp.log(mass)
+        for term in range(3):
+            piece = rest.astype(jnp.bfloat16).astype(jnp.float32)
+            split = jnp.where(lane == 3 * head + term, piece, split)
+            rest = rest - piece
+
+    totals = jnp.dot(to_tokens, split.astype(jnp.bfloat16), preferred_element_type=jnp.float32)
     summed = jnp.zeros((rows, HEAD_DIM), jnp.float32)
     for head in range(local_heads):
         total = jnp.sum(
@@ -644,14 +668,15 @@
     totals_ref[...] = summed
     wo_load.wait()
     partial_ref[...] = jnp.dot(
-        moved(to_tokens, merged_own[...]), wo[pl.ds(pl.multiple_of(tp * width, width), width), :],
+        moved(to_tokens, jnp.concatenate([merged_own[head] for head in range(local_heads)], axis=1)), wo[pl.ds(pl.multiple_of(tp * width, width), width), :],
         preferred_element_type=jnp.float32,
     )
 
     far_whole(first_send, first_held, first_sem).wait_send()
     far_whole(second_send, second_held, second_sem).wait_send()
-    log_whole(n - 1, 0).wait_send()
-    back_whole(n - 1, 0).wait_send()
+    for head in range(local_heads):
+        log_whole(head).wait_send()
+        back_whole(head).wait_send()
 
     @pl.when(crosses)
     def _():
@@ -688,11 +713,11 @@
         relay_key.wait_send()
         relay_value.wait_send()
 
-    for group in range(n // members):
-        merged_copy(group).wait_recv()
-    peer_ref[...] = moved(to_tokens, merged_held[...])
-    for group in range(n // members):
-        merged_copy(group).wait_send()
+    for head in range(local_heads):
+        merged_copy(head).wait_recv()
+    peer_ref[...] = moved(to_tokens, jnp.concatenate([merged_held[head] for head in range(local_heads)], axis=1))
+    for head in range(local_heads):
+        merged_copy(head).wait_send()
 
 
 def mix(partial_ref, peer_ref, totals_ref, wo_ref, mixed_ref, log_ref):
@@ -709,7 +734,6 @@
     out_columns = out_weight.shape[1]
     local_heads = columns // (3 * HEAD_DIM)
     width = local_heads * HEAD_DIM
-    planes = MIDDLE_DILATION
     dma = pltpu.SemaphoreType.DMA
     half = jnp.bfloat16
     full = jnp.float32
@@ -732,10 +756,10 @@
             pltpu.VMEM((rows, 2 * width), half),
             pltpu.VMEM((rows, width), half),
             pltpu.VMEM((rows, width), half),
-            pltpu.VMEM((rows, width), half),
-            pltpu.VMEM((rows, width), half),
-            pltpu.VMEM((n, 1, HEAD_DIM), full),
-            pltpu.VMEM((n, 1, HEAD_DIM), full),
+            pltpu.VMEM((local_heads, rows, HEAD_DIM), half),
+            pltpu.VMEM((local_heads, rows, HEAD_DIM), half),
+            pltpu.VMEM((local_heads, n, 1, HEAD_DIM), full),
+            pltpu.VMEM((local_heads, n, 1, HEAD_DIM), full),
             pltpu.VMEM((rows, width), half),
             pltpu.VMEM((2, rows, width), half),
             pltpu.VMEM((2, 2, rows, width), half),
@@ -744,13 +768,12 @@
             pltpu.VMEM((2, rows, width), half),
             pltpu.VMEM((2, NEAR_WINDOW, width), half),
             pltpu.VMEM((2 * local_heads, rows, 1), full),
-            pltpu.VMEM((rows, HEAD_DIM), half),
-            pltpu.VMEM((rows, width), half),
-            pltpu.VMEM((rows, width), half),
+            pltpu.VMEM((local_heads, rows, HEAD_DIM), half),
+            pltpu.VMEM((local_heads, rows, HEAD_DIM), half),
             pltpu.VMEM((local_heads, rows, HEAD_DIM), full),
-            dma((2 + 9 * local_heads,)),
-            dma((2,)), dma((2,)), dma(()), dma((planes,)), dma(()), dma((planes,)),
-            dma((4, 2)), dma((2, 2)), dma((1,)), dma((1,)), dma((2,)), dma((2,)), dma((planes,)), dma((planes,)),
+            dma((1 + 9 * local_heads,)), dma((2, 1 + 2 * local_heads)), dma((2,)), dma((2,)),
+            dma((local_heads,)), dma((local_heads,)), dma((local_heads,)), dma((local_heads,)),
+            dma((4, 2)), dma((2, 2)), dma((1,)), dma((1,)), dma((2,)), dma((2,)), dma((local_heads,)), dma((local_heads,)),
         ],
         compiler_params=pltpu.CompilerParams(
             collective_id=0, has_side_effects=True, vmem_limit_bytes=53000 * 1024

time: 29.1 us -> 28.6 us (0.983)
  the two profiles are of different devices: /device:TPU:0 before, /device:TPU:16 now
where the time goes in v4:
time: 28.6 us; the launch traced here: 28.5 us
  Pallas kernels  27.8 us (97%)
  between operations  0.65 us (2%)
    pallas_call x1, Pallas kernels, fused(): pl.pallas_call(functools.partial(kernel, n, local_heads), out_shape=(jax....  26.7 us
    pallas_call x1, Pallas kernels, fused(): pl.pallas_call(mix, out_shape=(jax.ShapeDtypeStruct((rows, out_columns),...  1.11 us

profile of v4, /device:TPU:16, one launch (start us, length us, event | category | flops | bytes accessed | tf_op | source)
XLA Modules:
  0.0 28.5 jit_solution(7427446942619085381)
XLA Ops:
  0.6 0.0 copy-start
  0.6 26.7 %shard_map.68 = (f32[256,1024]{1,0:T(8,128)S(1)}, bf16[256,256]{1,0:T(8,128)(2,1)S(1)}, f32[256,128]{1,0:T(8,128)S(1)}) custom-call(bf16[256,2048]{1,0:T(8,128)(2,1)} %tok_hbm.1, bf16[2048,768]{1,0:T(8,128)(2,1)} %wq_hbm.1, bf16[2048,768]{1,0:T(8,128)(2,1)} %wk_hbm.1, bf16[2048,768]{1,0:T(8,128)(2,1)} %wv_hbm.1, bf16[512,1024]{1,0:T(8,128)(2,1)} %wo_ref.1), custom_call_target="tpu_custom_call" | custom-call | tf_op jit(solution)/shard_map/pallas_call | solution.py:742
  27.3 0.0 copy-done
  27.3 1.1 %shard_map.69 = (bf16[256,1024]{1,0:T(8,128)(2,1)}, f32[2,256]{1,0:T(2,128)}) custom-call(f32[256,1024]{1,0:T(8,128)S(1)} %get-tuple-element.5.partial_ref, bf16[256,256]{1,0:T(8,128)(2,1)S(1)} %get-tuple-element.6.peer_ref, f32[256,128]{1,0:T(8,128)S(1)} %get-tuple-element.7.totals_ref, bf16[512,1024]{1,0:T(8,128)(2,1)S(1)} %copy-done), custom_call_target="tpu_custom_call" | custom-call | tf_op jit(solution)/shard_map/pallas_call | solution.py:782
Async XLA Ops:
  0.6 26.7 %copy-start = (bf16[512,1024]{1,0:T(8,128)(2,1)S(1)}, bf16[512,1024]{1,0:T(8,128)(2,1)}, u32[]{:S(2)}) copy-start(bf16[512,1024]{1,0:T(8,128)(2,1)} %wo_ref.1) | copy-start | bytes 3145732

commit v5 on v4

--- a/solution.py
+++ b/solution.py
@@ -178,9 +178,9 @@
     n, local_heads,
     tok_hbm, wq_hbm, wk_hbm, wv_hbm, wo_hbm,
     partial_ref, peer_ref, totals_ref,
-    tok, weight, wo, first_send, first_held, second_send, second_held, back_send, back_held, log_send, log_held,
-    mid_query, mid_own, mid_held, via_held, near_query, near_own, near_held,
-    stats, merged_own, merged_held, near_sum,
+    tok, scattered, product, weight, wo, first_send, first_held, second_send, second_held, back_send, back_held, log_send, log_held, probs,
+    mid_query, mid_own, mid_held, via_held, near_query, near_low, near_own, near_held,
+    stats, terms, merged_own, merged_held, near_sum,
     load_sem, half_sem, first_sem, second_sem, back_ssem, back_rsem, log_ssem, log_rsem,
     mid_ssem, mid_rsem, via_ssem, via_rsem, near_ssem, near_rsem, merged_ssem, merged_rsem,
 ):
@@ -192,6 +192,8 @@
     classes = MIDDLE_DILATION
     members = n // classes
     stretch = rows // classes
+    part_rows = chunk // 2
+    low_rows = rows // 2
     peer = 1 - tp
     sources = (wq_hbm, wk_hbm, wv_hbm)
 
@@ -203,11 +205,9 @@
     ]
     wo_load = pltpu.make_async_copy(wo_hbm, wo, load_sem.at[0])
     loads = []
-    order = [(2, part, head) for head in range(local_heads) for part in range(3)]
-    for group, part in ((0, 0), (0, 1), (0, 2), (1, 0)):
+    order = [(2, part, head) for head in range(local_heads) for part in (0, 1)]
+    for group, part in ((1, 1), (1, 2), (2, 2), (0, 0), (0, 1), (0, 2), (1, 0)):
         order += [(group, part, head) for head in range(local_heads)]
-    middle = [(1, part, head) for part in (1, 2) for head in range(local_heads)]
-    order[2 * local_heads : 2 * local_heads] = middle
     first = 2 * local_heads
     early = 4 * local_heads
     for place, (group, part, head) in enumerate(order):
@@ -220,8 +220,9 @@
             ])
         else:
             loads.append(pltpu.make_async_copy(source, target, load_sem.at[1 + place]))
+    for copy in tok_loads:
+        copy.start()
     for side in range(2):
-        tok_loads[side].start()
         for copy in loads[:first]:
             copy[side].start()
 
@@ -244,11 +245,11 @@
     def _():
         mid_held[1] = jnp.zeros((2, rows, width), jnp.bfloat16)
 
-    def project(first, last):
+    def project(source, first, last):
         for copy in loads[first * local_heads : last * local_heads]:
             copy.wait()
         return jnp.dot(
-            tok[...], weight[:, first * width : last * width], preferred_element_type=jnp.float32
+            source[...], weight[:, first * width : last * width], preferred_element_type=jnp.float32
         ).astype(jnp.bfloat16)
 
     def at_rows(index):
@@ -262,7 +263,12 @@
     def gather_row(token):
         index, residue = split_by(token, n)
         high, low = split_by(residue, classes)
-        return (low * members + high) * chunk + index
+        side, inner = split_by(index, part_rows)
+        return side * low_rows + (low * members + high) * part_rows + inner
+
+    def low_row(row):
+        group, inner = split_by(row, part_rows)
+        return group * chunk + inner
 
     def class_token(row):
         group, index = split_by(row, stretch)
@@ -309,58 +315,64 @@
             device_id_type=MESH,
         )
 
-    def back_copy(head, k):
+    plane = me // members
+    planes = n // members
+
+    def back_copy(k):
         to = target_of(k)
         return pltpu.make_async_remote_copy(
-            src_ref=back_send.at[head, at_rows(to)],
-            dst_ref=back_held.at[head, at_rows(me)],
-            send_sem=back_ssem.at[head],
-            recv_sem=back_rsem.at[head],
+            src_ref=back_send.at[at_rows(to)],
+            dst_ref=back_held.at[at_rows(me)],
+            send_sem=back_ssem,
+            recv_sem=back_rsem.at[plane],
             device_id=(to, tp),
             device_id_type=MESH,
         )
 
-    def back_whole(head):
-        others = pl.ds(0, rows - chunk)
-        return pltpu.make_async_remote_copy(
-            src_ref=back_send.at[head, others],
-            dst_ref=back_held.at[head, others],
-            send_sem=back_ssem.at[head],
-            recv_sem=back_rsem.at[head],
+    def back_some(count, group):
+        some = pl.ds(0, count * chunk)
+        return pltpu.make_async_remote_copy(
+            src_ref=back_send.at[some],
+            dst_ref=back_held.at[some],
+            send_sem=back_ssem,
+            recv_sem=back_rsem.at[group],
             device_id=(lax.rem(me + 1, n), tp),
             device_id_type=MESH,
         )
 
-    def log_copy(head, k):
+    def log_copy(k):
         to = target_of(k)
         return pltpu.make_async_remote_copy(
-            src_ref=log_send.at[head, to],
-            dst_ref=log_held.at[head, me],
-            send_sem=log_ssem.at[head],
-            recv_sem=log_rsem.at[head],
+            src_ref=log_send.at[to],
+            dst_ref=log_held.at[me],
+            send_sem=log_ssem,
+            recv_sem=log_rsem.at[plane],
             device_id=(to, tp),
             device_id_type=MESH,
         )
 
-    def log_whole(head):
-        others = pl.ds(0, n - 1)
-        return pltpu.make_async_remote_copy(
-            src_ref=log_send.at[head, others],
-            dst_ref=log_held.at[head, others],
-            send_sem=log_ssem.at[head],
-            recv_sem=log_rsem.at[head],
+    def log_some(count, group):
+        some = pl.ds(0, count)
+        return pltpu.make_async_remote_copy(
+            src_ref=log_send.at[some],
+            dst_ref=log_held.at[some],
+            send_sem=log_ssem,
+            recv_sem=log_rsem.at[group],
             device_id=(lax.rem(me + 1, n), tp),
             device_id_type=MESH,
         )
 
-    product = None
+    for copy, part in zip(tok_loads, halves):
+        copy.wait()
+        scattered[:, part] = moved(to_scattered, tok[:, part])
     for side, part in enumerate(halves):
-        tok_loads[side].wait()
         for copy in loads[:first]:
             copy[side].wait()
-        term = jnp.dot(tok[:, part], weight[part, : 2 * width], preferred_element_type=jnp.float32)
-        product = term if product is None else product + term
-    first_send[...] = moved(to_scattered, product.astype(jnp.bfloat16))
+        term = jnp.dot(scattered[:, part], weight[part, : 2 * width], preferred_element_type=jnp.float32)
+        if side == 0:
+            product[...] = term
+        else:
+            first_send[...] = (product[...] + term).astype(jnp.bfloat16)
     for copy in loads[early:]:
         copy.start()
     pl.semaphore_wait(barrier, n)
@@ -421,7 +433,7 @@
     forwards = (lax.rem(me, 4) < 2) & above
     direct = sends_one & jnp.logical_not(crosses & odd)
 
-    pair = moved(to_classes, project(2, 4))
+    pair = moved(to_classes, project(tok, 2, 4))
     mid_own[0] = pair[:, :width]
     mid_own[1] = pair[:, width:]
 
@@ -429,9 +441,10 @@
     def _():
         via_mid.start()
 
-    pair = moved(to_scattered, project(4, 6))
+    pair = project(scattered, 4, 6)
     second_send[...] = pair[:, :width]
     near_query[...] = pair[:, width:]
+    near_low[...] = moved(one_hot(rows, low_row)[:low_rows], pair[:, width:])
     each(lambda k: far_copy(second_send, second_held, second_sem, k).start())
     second_held[at_rows(me), :] = second_send[at_rows(me), :]
     wo_load.start()
@@ -454,7 +467,7 @@
     def _():
         key_one.start()
 
-    pair = project(6, 8)
+    pair = project(tok, 6, 8)
     near_own[0] = pair[:, :width]
     near_own[1] = pair[:, width:]
 
@@ -463,7 +476,7 @@
         near_key.start()
         near_value.start()
 
-    mid_query[...] = moved(to_scattered, project(8, 9))
+    mid_query[...] = project(scattered, 8, 9)
 
     def slope_of(head, window):
         number = tp * local_heads + head
@@ -479,8 +492,14 @@
     distance = apart.astype(jnp.float32)
     heads = [pl.ds(head * HEAD_DIM, HEAD_DIM) for head in range(local_heads)]
 
-    def join(parts):
-        held = [(stats[2 * head], stats[2 * head + 1], near_sum[head]) for head in range(local_heads)]
+    def join(parts, side):
+        held = [
+            (
+                stats[2 * head, :, side].reshape(-1, 1), stats[2 * head + 1, :, side].reshape(-1, 1),
+                near_sum[head, :, side].reshape(-1, HEAD_DIM),
+            )
+            for head in range(local_heads)
+        ]
         joined = []
         for (high, total, part), (held_high, held_total, held_part) in zip(parts, held):
             highest = jnp.maximum(held_high, high)
@@ -488,13 +507,16 @@
             joined.append((
                 highest, held_total * held_share + total * share, held_part * held_share + part * share
             ))
-        keep(joined)
-
-    def keep(parts):
+        keep(joined, side)
+
+    def keep(parts, side):
+        shape = (n, -1, part_rows) if isinstance(side, slice) else (n, part_rows)
         for head, (high, total, part) in enumerate(parts):
-            stats[2 * head] = high
-            stats[2 * head + 1] = total
-            near_sum[head] = part
+            stats[2 * head, :, side] = high.reshape(*shape, 1)
+            stats[2 * head + 1, :, side] = total.reshape(*shape, 1)
+            near_sum[head, :, side] = part.reshape(*shape, HEAD_DIM)
+
+    both = slice(0, 2)
 
     def partial_of(query, key_value, slopes, distance, valid):
         weighed = [
@@ -507,16 +529,16 @@
         ]
 
     near_slopes = [slope_of(head, NEAR_WINDOW) for head in range(local_heads)]
-    keep(partial_of(near_query, near_own, near_slopes, distance, valid))
+    keep(partial_of(near_query, near_own, near_slopes, distance, valid), both)
 
     def near_rest():
         near_key.wait_recv()
         near_value.wait_recv()
-        row, column = grid(rows, NEAR_WINDOW)
-        apart = scatter_token(row) + NEAR_WINDOW - column
+        row, column = grid(low_rows, NEAR_WINDOW)
+        apart = scatter_token(low_row(row)) + NEAR_WINDOW - column
         valid = (apart >= 0) & (apart <= NEAR_WINDOW)
         distance = apart.astype(jnp.float32)
-        join(partial_of(near_query, near_held, near_slopes, distance, valid))
+        join(partial_of(near_low, near_held, near_slopes, distance, valid), 0)
 
     @pl.when(odd)
     def _():
@@ -541,43 +563,43 @@
     slot = lax.broadcasted_iota(jnp.int32, (rows, HEAD_DIM), 0) & (chunk - 1)
     of_slot = lane == slot
 
-    def far_part(head, part, first_row, last_row):
-        place = head * 3 + part
-        source = first_held
-        if place >= 2 * local_heads:
-            place -= 2 * local_heads
-            source = second_held
-        return source[first_row:last_row, place * HEAD_DIM : (place + 1) * HEAD_DIM]
-
+    blocks = ((0, reach), (reach, rows))
+    weighed = []
     for head in range(local_heads):
-        if head == local_heads - 1:
-            far_whole(second_send, second_held, second_sem).wait_recv()
-        logs = []
-        shares = []
-        for first_row, last_row in ((0, reach), (reach, rows)):
+        at = pl.ds(2 * head * HEAD_DIM, HEAD_DIM)
+        key_at = pl.ds((2 * head + 1) * HEAD_DIM, HEAD_DIM)
+        for first_row, last_row in blocks:
             row, column = grid(last_row - first_row, last_row)
             apart = row + first_row - column
-            highest, weights, total = weigh(
-                scores_of(far_part(head, 0, first_row, last_row), far_part(head, 1, 0, last_row)),
+            weighed.append(weigh(
+                scores_of(first_held[first_row:last_row, at], first_held[:last_row, key_at]),
                 slope_of(head, FAR_WINDOW), (apart * FAR_DILATION).astype(jnp.float32),
                 (apart >= 0) & (apart <= reach),
-            )
-            logs.append(highest + jnp.log(total))
-            shares.append(weights * (1.0 / total))
-        packed = jnp.where(of_slot, jnp.concatenate(logs, axis=0), 0.0)
-        log_send[head] = jnp.sum(packed.reshape(n, chunk, HEAD_DIM), axis=1, keepdims=True)
-        for (first_row, last_row), share in zip(((0, reach), (reach, rows)), shares):
-            back_send[head, first_row:last_row] = apply(
-                share, far_part(head, 2, 0, last_row)
+            ))
+    packed = []
+    for head in range(local_heads):
+        parts = weighed[head * len(blocks) : (head + 1) * len(blocks)]
+        logs = jnp.concatenate([high + jnp.log(total) for high, _, total in parts], axis=0)
+        packed.append(jnp.sum(
+            jnp.where(of_slot, logs, 0.0).reshape(n, chunk, HEAD_DIM), axis=1, keepdims=True
+        ))
+    log_send[...] = jnp.concatenate(packed, axis=2)
+    for head in range(local_heads):
+        parts = weighed[head * len(blocks) : (head + 1) * len(blocks)]
+        for (first_row, last_row), (_, weights, total) in zip(blocks, parts):
+            probs[head, first_row:last_row, :last_row] = (weights * (1.0 / total)).astype(jnp.bfloat16)
+    each(lambda k: log_copy(k).start())
+    log_held[me] = log_send[me]
+
+    far_whole(second_send, second_held, second_sem).wait_recv()
+    for head, at in enumerate(heads):
+        for first_row, last_row in blocks:
+            back_send[first_row:last_row, at] = jnp.dot(
+                probs[head, first_row:last_row, :last_row], second_held[:last_row, at],
+                preferred_element_type=jnp.float32,
             ).astype(jnp.bfloat16)
-
-        def send_back(k):
-            log_copy(head, k).start()
-            back_copy(head, k).start()
-
-        each(send_back)
-        log_held[head, me] = log_send[head, me]
-        back_held[head, at_rows(me), :] = back_send[head, at_rows(me), :]
+    each(lambda k: back_copy(k).start())
+    back_held[at_rows(me), :] = back_send[at_rows(me), :]
 
     @pl.when(me >= 1)
     def _():
@@ -621,44 +643,102 @@
             for group in range(classes)
         ], axis=0))
         for at, (high, weights, total) in zip(heads, weighed)
-    ])
-
-    @pl.when(even & (me >= 1))
-    def _():
+    ], both)
+
+    block = members * part_rows
+
+    def merged_copy(group, side):
+        place = pl.ds(pl.multiple_of(side * low_rows + group * block, block), block)
+        return pltpu.make_async_remote_copy(
+            src_ref=merged_own.at[place],
+            dst_ref=merged_held.at[place],
+            send_sem=merged_ssem.at[group, side],
+            recv_sem=merged_rsem.at[group, side],
+            device_id=(me, peer),
+            device_id_type=MESH,
+        )
+
+    lane = lax.broadcasted_iota(jnp.int32, (block, HEAD_DIM), 1)
+    slot = lax.broadcasted_iota(jnp.int32, (block, HEAD_DIM), 0) & (part_rows - 1)
+
+    def factors(group, side):
+        some = pl.ds(group * members, members)
+        split = jnp.zeros((block, HEAD_DIM), jnp.float32)
+        shares = []
+        held = log_held[some]
+        for head in range(local_heads):
+            spread = jnp.broadcast_to(
+                held[:, :, head * HEAD_DIM : (head + 1) * HEAD_DIM], (members, part_rows, HEAD_DIM)
+            ).reshape(block, HEAD_DIM)
+            far_log = jnp.sum(jnp.where(lane == slot + side * part_rows, spread, 0.0), axis=-1, keepdims=True)
+            pair_log = stats[2 * head, some, side].reshape(block, 1)
+            pair_sum = stats[2 * head + 1, some, side].reshape(block, 1)
+            highest = jnp.maximum(pair_log, far_log)
+            pair_part, far_part = jnp.exp(pair_log - highest), jnp.exp(far_log - highest)
+            mass = pair_sum * pair_part + far_part
+            inverse = 1.0 / mass
+            pair_term = near_sum[head, some, side].reshape(block, HEAD_DIM) * (pair_part * inverse)
+            shares.append((pair_term, far_part * inverse))
+            rest = highest + jnp.log(mass)
+            for term in range(3):
+                piece = rest.astype(jnp.bfloat16).astype(jnp.float32)
+                split = jnp.where(lane == 3 * head + term, piece, split)
+                rest = rest - piece
+        return shares, split
+
+    def merge(group, side, shares, split):
+        source = pl.ds(pl.multiple_of(group * members * chunk, members * chunk), members * chunk)
+        place = pl.ds(pl.multiple_of(side * low_rows + group * block, block), block)
+        merged = []
+        for at, (pair_term, share) in zip(heads, shares):
+            far = back_held[source, at].astype(jnp.float32).reshape(members, 2, part_rows, HEAD_DIM)
+            merged.append((pair_term + far[:, side].reshape(block, HEAD_DIM) * share).astype(jnp.bfloat16))
+        for at, value in zip(heads, merged):
+            merged_own[place, at] = value
+        merged_copy(group, side).start()
+        terms[place] = split.astype(jnp.bfloat16)
+
+    twin = plane + 1 - 2 * lax.rem(plane, 2)
+    below = (1 - upper) * (planes // 2)
+    soon = ((plane, members - 1), (twin, members), (below, members))
+    late = below + 1
+    waits_near = (lax.rem(me, members) == 0) & (plane == planes // 2)
+
+    @pl.when(jnp.logical_not(waits_near))
+    def _():
+        @pl.when(even & (me >= 1))
+        def _():
+            near_rest()
+
+        for lot in (soon, ((late, members),)):
+            for group, count in lot:
+                log_some(count, group).wait_recv()
+            ready = [[factors(group, side) for side in range(2)] for group, _ in lot]
+            for (group, count), sides in zip(lot, ready):
+                back_some(count, group).wait_recv()
+                for side, held in enumerate(sides):
+                    merge(group, side, *held)
+
+    @pl.when(waits_near)
+    def _():
+        for group, count in soon:
+            log_some(count, group).wait_recv()
+        ready = [factors(group, 1) for group, _ in soon]
+        for (group, count), held in zip(soon, ready):
+            back_some(count, group).wait_recv()
+            merge(group, 1, *held)
         near_rest()
-
-    def merged_copy(head):
-        return pltpu.make_async_remote_copy(
-            src_ref=merged_own.at[head],
-            dst_ref=merged_held.at[head],
-            send_sem=merged_ssem.at[head],
-            recv_sem=merged_rsem.at[head],
-            device_id=(me, peer),
-            device_id_type=MESH,
-        )
-
-    split = jnp.zeros((rows, HEAD_DIM), jnp.float32)
-    for head in range(local_heads):
-        log_whole(head).wait_recv()
-        spread = jnp.broadcast_to(log_held[head], (n, chunk, HEAD_DIM)).reshape(rows, HEAD_DIM)
-        far_log = jnp.sum(jnp.where(of_slot, spread, 0.0), axis=-1, keepdims=True)
-        pair_log, pair_sum = stats[2 * head], stats[2 * head + 1]
-        highest = jnp.maximum(pair_log, far_log)
-        pair_share, far_share = jnp.exp(pair_log - highest), jnp.exp(far_log - highest)
-        mass = pair_sum * pair_share + far_share
-        inverse = 1.0 / mass
-        back_whole(head).wait_recv()
-        merged = near_sum[head] * (pair_share * inverse)
-        merged = merged + back_held[head].astype(jnp.float32) * (far_share * inverse)
-        merged_own[head] = merged.astype(jnp.bfloat16)
-        merged_copy(head).start()
-        rest = highest + jnp.log(mass)
-        for term in range(3):
-            piece = rest.astype(jnp.bfloat16).astype(jnp.float32)
-            split = jnp.where(lane == 3 * head + term, piece, split)
-            rest = rest - piece
-
-    totals = jnp.dot(to_tokens, split.astype(jnp.bfloat16), preferred_element_type=jnp.float32)
+        ready = [factors(group, 0) for group, _ in soon]
+        for (group, _), held in zip(soon, ready):
+            merge(group, 0, *held)
+        log_some(members, late).wait_recv()
+        ready = [factors(late, side) for side in range(2)]
+        back_some(members, late).wait_recv()
+        for side, held in enumerate(ready):
+            merge(late, side, *held)
+
+    lane = lax.broadcasted_iota(jnp.int32, (rows, HEAD_DIM), 1)
+    totals = jnp.dot(to_tokens, terms[...], preferred_element_type=jnp.float32)
     summed = jnp.zeros((rows, HEAD_DIM), jnp.float32)
     for head in range(local_heads):
         total = jnp.sum(
@@ -668,15 +748,14 @@
     totals_ref[...] = summed
     wo_load.wait()
     partial_ref[...] = jnp.dot(
-        moved(to_tokens, jnp.concatenate([merged_own[head] for head in range(local_heads)], axis=1)), wo[pl.ds(pl.multiple_of(tp * width, width), width), :],
+        moved(to_tokens, merged_own[...]), wo[pl.ds(pl.multiple_of(tp * width, width), width), :],
         preferred_element_type=jnp.float32,
     )
 
     far_whole(first_send, first_held, first_sem).wait_send()
     far_whole(second_send, second_held, second_sem).wait_send()
-    for head in range(local_heads):
-        log_whole(head).wait_send()
-        back_whole(head).wait_send()
+    log_some(n - 1, 0).wait_send()
+    back_some(n - 1, 0).wait_send()
 
     @pl.when(crosses)
     def _():
@@ -713,11 +792,13 @@
         relay_key.wait_send()
         relay_value.wait_send()
 
-    for head in range(local_heads):
-        merged_copy(head).wait_recv()
-    peer_ref[...] = moved(to_tokens, jnp.concatenate([merged_held[head] for head in range(local_heads)], axis=1))
-    for head in range(local_heads):
-        merged_copy(head).wait_send()
+    for group in range(planes):
+        for side in range(2):
+            merged_copy(group, side).wait_recv()
+    peer_ref[...] = moved(to_tokens, merged_held[...])
+    for group in range(planes):
+        for side in range(2):
+            merged_copy(group, side).wait_send()
 
 
 def mix(partial_ref, peer_ref, totals_ref, wo_ref, mixed_ref, log_ref):
@@ -734,6 +815,7 @@
     out_columns = out_weight.shape[1]
     local_heads = columns // (3 * HEAD_DIM)
     width = local_heads * HEAD_DIM
+    planes = MIDDLE_DILATION
     dma = pltpu.SemaphoreType.DMA
     half = jnp.bfloat16
     full = jnp.float32
@@ -750,30 +832,35 @@
         out_specs=(whole, whole, whole),
         scratch_shapes=[
             pltpu.VMEM((rows, depth), half),
+            pltpu.VMEM((rows, depth), half),
+            pltpu.VMEM((rows, 2 * width), full),
             pltpu.VMEM((depth, 3 * columns), half),
             pltpu.VMEM(out_weight.shape, half),
             pltpu.VMEM((rows, 2 * width), half),
             pltpu.VMEM((rows, 2 * width), half),
             pltpu.VMEM((rows, width), half),
             pltpu.VMEM((rows, width), half),
-            pltpu.VMEM((local_heads, rows, HEAD_DIM), half),
-            pltpu.VMEM((local_heads, rows, HEAD_DIM), half),
-            pltpu.VMEM((local_heads, n, 1, HEAD_DIM), full),
-            pltpu.VMEM((local_heads, n, 1, HEAD_DIM), full),
+            pltpu.VMEM((rows, width), half),
+            pltpu.VMEM((rows, width), half),
+            pltpu.VMEM((n, 1, width), full),
+            pltpu.VMEM((n, 1, width), full),
+            pltpu.VMEM((local_heads, rows, rows), half),
             pltpu.VMEM((rows, width), half),
             pltpu.VMEM((2, rows, width), half),
             pltpu.VMEM((2, 2, rows, width), half),
             pltpu.VMEM((rows, width), half),
             pltpu.VMEM((rows, width), half),
+            pltpu.VMEM((rows // 2, width), half),
             pltpu.VMEM((2, rows, width), half),
             pltpu.VMEM((2, NEAR_WINDOW, width), half),
-            pltpu.VMEM((2 * local_heads, rows, 1), full),
-            pltpu.VMEM((local_heads, rows, HEAD_DIM), half),
-            pltpu.VMEM((local_heads, rows, HEAD_DIM), half),
-            pltpu.VMEM((local_heads, rows, HEAD_DIM), full),
+            pltpu.VMEM((2 * local_heads, n, 2, rows // (2 * n), 1), full),
+            pltpu.VMEM((rows, HEAD_DIM), half),
+            pltpu.VMEM((rows, width), half),
+            pltpu.VMEM((rows, width), half),
+            pltpu.VMEM((local_heads, n, 2, rows // (2 * n), HEAD_DIM), full),
             dma((1 + 9 * local_heads,)), dma((2, 1 + 2 * local_heads)), dma((2,)), dma((2,)),
-            dma((local_heads,)), dma((local_heads,)), dma((local_heads,)), dma((local_heads,)),
-            dma((4, 2)), dma((2, 2)), dma((1,)), dma((1,)), dma((2,)), dma((2,)), dma((local_heads,)), dma((local_heads,)),
+            dma(()), dma((planes,)), dma(()), dma((planes,)),
+            dma((4, 2)), dma((2, 2)), dma((1,)), dma((1,)), dma((2,)), dma((2,)), dma((planes, 2)), dma((planes, 2)),
         ],
         compiler_params=pltpu.CompilerParams(
             collective_id=0, has_side_effects=True, vmem_limit_bytes=53000 * 1024

time: 28.6 us -> 28.1 us (0.983)
  the two profiles are of different devices: /device:TPU:16 before, /device:TPU:0 now
where the time goes in v5:
time: 28.1 us; the launch traced here: 27.9 us
  Pallas kernels  27.3 us (97%)
  between operations  0.65 us (2%)
    pallas_call x1, Pallas kernels, fused(): pl.pallas_call(functools.partial(kernel, n, local_heads), out_shape=(jax....  26.2 us
    pallas_call x1, Pallas kernels, fused(): pl.pallas_call(mix, out_shape=(jax.ShapeDtypeStruct((rows, out_columns),...  1.11 us

profile of v5, /device:TPU:0, one launch (start us, length us, event | category | flops | bytes accessed | tf_op | source)
XLA Modules:
  0.0 27.9 jit_solution(8553683568109992322)
XLA Ops:
  0.6 0.0 copy-start
  0.6 26.2 %shard_map.68 = (f32[256,1024]{1,0:T(8,128)S(1)}, bf16[256,256]{1,0:T(8,128)(2,1)S(1)}, f32[256,128]{1,0:T(8,128)S(1)}) custom-call(bf16[256,2048]{1,0:T(8,128)(2,1)} %tok_hbm.1, bf16[2048,768]{1,0:T(8,128)(2,1)} %wq_hbm.1, bf16[2048,768]{1,0:T(8,128)(2,1)} %wk_hbm.1, bf16[2048,768]{1,0:T(8,128)(2,1)} %wv_hbm.1, bf16[512,1024]{1,0:T(8,128)(2,1)} %wo_ref.1), custom_call_target="tpu_custom_call" | custom-call | tf_op jit(solution)/shard_map/pallas_call | solution.py:824
  26.8 0.0 copy-done
  26.8 1.1 %shard_map.69 = (bf16[256,1024]{1,0:T(8,128)(2,1)}, f32[2,256]{1,0:T(2,128)}) custom-call(f32[256,1024]{1,0:T(8,128)S(1)} %get-tuple-element.5.partial_ref, bf16[256,256]{1,0:T(8,128)(2,1)S(1)} %get-tuple-element.6.peer_ref, f32[256,128]{1,0:T(8,128)S(1)} %get-tuple-element.7.totals_ref, bf16[512,1024]{1,0:T(8,128)(2,1)S(1)} %copy-done), custom_call_target="tpu_custom_call" | custom-call | tf_op jit(solution)/shard_map/pallas_call | solution.py:869
Async XLA Ops:
  0.6 26.2 %copy-start = (bf16[512,1024]{1,0:T(8,128)(2,1)S(1)}, bf16[512,1024]{1,0:T(8,128)(2,1)}, u32[]{:S(2)}) copy-start(bf16[512,1024]{1,0:T(8,128)(2,1)} %wo_ref.1) | copy-start | bytes 3145732

commit v6 on v5

--- a/solution.py
+++ b/solution.py
@@ -179,10 +179,10 @@
     tok_hbm, wq_hbm, wk_hbm, wv_hbm, wo_hbm,
     partial_ref, peer_ref, totals_ref,
     tok, scattered, product, weight, wo, first_send, first_held, second_send, second_held, back_send, back_held, log_send, log_held, probs,
-    mid_query, mid_own, mid_held, via_held, near_query, near_low, near_own, near_held,
+    mid_query, mid_own, mid_held, via_held, near_query, near_low, near_own, near_held, guest_query, guest_out, guest_log, guest_back, guest_back_log,
     stats, terms, merged_own, merged_held, near_sum,
-    load_sem, half_sem, first_sem, second_sem, back_ssem, back_rsem, log_ssem, log_rsem,
-    mid_ssem, mid_rsem, via_ssem, via_rsem, near_ssem, near_rsem, merged_ssem, merged_rsem,
+    load_sem, first_sem, second_sem, back_ssem, back_rsem, log_ssem, log_rsem,
+    mid_ssem, mid_rsem, via_rsem, near_ssem, near_rsem, guest_sem, merged_sem,
 ):
     me = lax.axis_index("sp")
     tp = lax.axis_index("tp")
@@ -200,13 +200,16 @@
     depth = tok.shape[1]
     halves = (pl.ds(0, depth // 2), pl.ds(depth // 2, depth // 2))
     tok_loads = [
-        pltpu.make_async_copy(tok_hbm.at[:, part], tok.at[:, part], half_sem.at[side, 0])
+        pltpu.make_async_copy(tok_hbm.at[:, part], tok.at[:, part], load_sem.at[side])
         for side, part in enumerate(halves)
     ]
-    wo_load = pltpu.make_async_copy(wo_hbm, wo, load_sem.at[0])
+    wo_load = pltpu.make_async_copy(wo_hbm, wo, load_sem.at[4])
     loads = []
-    order = [(2, part, head) for head in range(local_heads) for part in (0, 1)]
-    for group, part in ((1, 1), (1, 2), (2, 2), (0, 0), (0, 1), (0, 2), (1, 0)):
+    far_order = [(2, part, head) for head in range(local_heads) for part in range(3)]
+    order = far_order[: 2 * local_heads]
+    order += [(1, part, head) for part in (1, 2) for head in range(local_heads)]
+    order += far_order[2 * local_heads :]
+    for group, part in ((0, 0), (0, 1), (0, 2), (1, 0)):
         order += [(group, part, head) for head in range(local_heads)]
     first = 2 * local_heads
     early = 4 * local_heads
@@ -215,11 +218,11 @@
         target = weight.at[:, pl.ds(place * HEAD_DIM, HEAD_DIM)]
         if place < first:
             loads.append([
-                pltpu.make_async_copy(source.at[side], target.at[side], half_sem.at[index, 1 + place])
+                pltpu.make_async_copy(source.at[side], target.at[side], load_sem.at[2 + index])
                 for index, side in enumerate(halves)
             ])
         else:
-            loads.append(pltpu.make_async_copy(source, target, load_sem.at[1 + place]))
+            loads.append(pltpu.make_async_copy(source, target, load_sem.at[4 + place // first]))
     for copy in tok_loads:
         copy.start()
     for side in range(2):
@@ -246,8 +249,8 @@
         mid_held[1] = jnp.zeros((2, rows, width), jnp.bfloat16)
 
     def project(source, first, last):
-        for copy in loads[first * local_heads : last * local_heads]:
-            copy.wait()
+        part = weight.at[:, pl.ds(first * width, (last - first) * width)]
+        pltpu.make_async_copy(part, part, load_sem.at[4 + first // 2]).wait()
         return jnp.dot(
             source[...], weight[:, first * width : last * width], preferred_element_type=jnp.float32
         ).astype(jnp.bfloat16)
@@ -318,46 +321,46 @@
     plane = me // members
     planes = n // members
 
-    def back_copy(k):
+    def back_copy(head, k):
         to = target_of(k)
         return pltpu.make_async_remote_copy(
-            src_ref=back_send.at[at_rows(to)],
-            dst_ref=back_held.at[at_rows(me)],
+            src_ref=back_send.at[head, at_rows(to)],
+            dst_ref=back_held.at[head, at_rows(me)],
             send_sem=back_ssem,
-            recv_sem=back_rsem.at[plane],
+            recv_sem=back_rsem.at[head, plane],
             device_id=(to, tp),
             device_id_type=MESH,
         )
 
-    def back_some(count, group):
+    def back_some(head, count, group):
         some = pl.ds(0, count * chunk)
         return pltpu.make_async_remote_copy(
-            src_ref=back_send.at[some],
-            dst_ref=back_held.at[some],
+            src_ref=back_send.at[head, some],
+            dst_ref=back_held.at[head, some],
             send_sem=back_ssem,
-            recv_sem=back_rsem.at[group],
+            recv_sem=back_rsem.at[head, group],
             device_id=(lax.rem(me + 1, n), tp),
             device_id_type=MESH,
         )
 
-    def log_copy(k):
+    def log_copy(head, k):
         to = target_of(k)
         return pltpu.make_async_remote_copy(
-            src_ref=log_send.at[to],
-            dst_ref=log_held.at[me],
+            src_ref=log_send.at[head, to],
+            dst_ref=log_held.at[head, me],
             send_sem=log_ssem,
-            recv_sem=log_rsem.at[plane],
+            recv_sem=log_rsem.at[head, plane],
             device_id=(to, tp),
             device_id_type=MESH,
         )
 
-    def log_some(count, group):
+    def log_some(head, count, group):
         some = pl.ds(0, count)
         return pltpu.make_async_remote_copy(
-            src_ref=log_send.at[some],
-            dst_ref=log_held.at[some],
+            src_ref=log_send.at[head, some],
+            dst_ref=log_held.at[head, some],
             send_sem=log_ssem,
-            recv_sem=log_rsem.at[group],
+            recv_sem=log_rsem.at[head, group],
             device_id=(lax.rem(me + 1, n), tp),
             device_id_type=MESH,
         )
@@ -366,8 +369,8 @@
         copy.wait()
         scattered[:, part] = moved(to_scattered, tok[:, part])
     for side, part in enumerate(halves):
-        for copy in loads[:first]:
-            copy[side].wait()
+        piece = weight.at[part, pl.ds(0, 2 * width)]
+        pltpu.make_async_copy(piece, piece, load_sem.at[2 + side]).wait()
         term = jnp.dot(scattered[:, part], weight[part, : 2 * width], preferred_element_type=jnp.float32)
         if side == 0:
             product[...] = term
@@ -383,7 +386,7 @@
         return pltpu.make_async_remote_copy(
             src_ref=source,
             dst_ref=mid_held.at[slot, part],
-            send_sem=mid_ssem.at[sem, part],
+            send_sem=mid_ssem.at[min(2 * sem + part, 6)],
             recv_sem=mid_rsem.at[slot, part],
             device_id=(lax.rem(me + hop + n, n), tp),
             device_id_type=MESH,
@@ -399,12 +402,12 @@
             device_id_type=MESH,
         )
 
-    def via_copy(which, source, target):
+    def via_copy(source, target):
         return pltpu.make_async_remote_copy(
             src_ref=source,
             dst_ref=target,
-            send_sem=via_ssem.at[which],
-            recv_sem=via_rsem.at[which],
+            send_sem=mid_ssem.at[1],
+            recv_sem=via_rsem,
             device_id=(lax.rem(me + -2 + n, n), tp),
             device_id_type=MESH,
         )
@@ -416,11 +419,25 @@
     value_one = mid_copy(1, 1, mid_own.at[1], 1, 1)
     near_key = near_copy(1, near_own.at[0, near_tail], 0, 0)
     near_value = near_copy(1, near_own.at[1, near_tail], 1, 1)
-    via_mid = via_copy(0, mid_own.at[1], via_held)
+    via_mid = via_copy(mid_own.at[1], via_held)
     onward_even = mid_copy(0, 4, via_held, 1, 3)
     onward_odd = mid_copy(1, 3, via_held, 1, 3)
     relay_key = mid_copy(0, 1, mid_held.at[1, 0], 0, 2)
     relay_value = mid_copy(0, 1, mid_held.at[1, 1], 1, 2)
+
+    def guest_copy(hop, source, target, ssem, rsem):
+        return pltpu.make_async_remote_copy(
+            src_ref=source,
+            dst_ref=target,
+            send_sem=ssem,
+            recv_sem=rsem,
+            device_id=(lax.rem(me + hop + n, n), tp),
+            device_id_type=MESH,
+        )
+
+    guest_ask = guest_copy(-1, near_low, guest_query, guest_sem.at[0], guest_sem.at[1])
+    guest_tell = guest_copy(1, guest_out, guest_back, near_ssem.at[0], near_rsem.at[0])
+    guest_tell_log = guest_copy(1, guest_log, guest_back_log, near_ssem.at[1], near_rsem.at[1])
 
     even = lax.rem(me, 2) == 0
     odd = jnp.logical_not(even)
@@ -431,6 +448,8 @@
     crosses = (lax.rem(me, 4) >= 2) & above
     stays = jnp.logical_not(crosses)
     forwards = (lax.rem(me, 4) < 2) & above
+    hosts = odd & sends_one
+    guests = even & (me >= 1)
     direct = sends_one & jnp.logical_not(crosses & odd)
 
     pair = moved(to_classes, project(tok, 2, 4))
@@ -442,12 +461,20 @@
         via_mid.start()
 
     pair = project(scattered, 4, 6)
-    second_send[...] = pair[:, :width]
+    for head in range(local_heads):
+        second_send[head] = pair[:, head * HEAD_DIM : (head + 1) * HEAD_DIM]
     near_query[...] = pair[:, width:]
     near_low[...] = moved(one_hot(rows, low_row)[:low_rows], pair[:, width:])
-    each(lambda k: far_copy(second_send, second_held, second_sem, k).start())
-    second_held[at_rows(me), :] = second_send[at_rows(me), :]
+    for piece in range(2):
+        each(lambda k: far_copy(
+            second_send.at[piece], second_held.at[piece], second_sem.at[piece], k
+        ).start())
+    second_held[:, at_rows(me), :] = second_send[:, at_rows(me), :]
     wo_load.start()
+
+    @pl.when(guests)
+    def _():
+        guest_ask.start()
 
     @pl.when(sends_two & stays)
     def _():
@@ -471,7 +498,7 @@
     near_own[0] = pair[:, :width]
     near_own[1] = pair[:, width:]
 
-    @pl.when(sends_one)
+    @pl.when(even)
     def _():
         near_key.start()
         near_value.start()
@@ -531,6 +558,39 @@
     near_slopes = [slope_of(head, NEAR_WINDOW) for head in range(local_heads)]
     keep(partial_of(near_query, near_own, near_slopes, distance, valid), both)
 
+    def class_slot(row):
+        group, index = split_by(row, chunk)
+        return index * members + split_by(group, members)[1]
+
+    def own_rows(part, group, at):
+        return mid_own[part, pl.ds(group * stretch, stretch), at]
+
+    def held_rows(part, group, at):
+        of_class = pl.ds(group * stretch, stretch)
+        return jnp.concatenate((mid_held[0, part, of_class, at], mid_held[1, part, of_class, at]), axis=0)
+
+    def middle_of(rows_of, apart, valid):
+        distance = (apart * classes).astype(jnp.float32)
+        weighed = []
+        for head, at in enumerate(heads):
+            scores = jnp.concatenate([
+                scores_of(mid_query[group * stretch : (group + 1) * stretch, at], rows_of(0, group, at))
+                for group in range(classes)
+            ], axis=0)
+            weighed.append(weigh(scores, slope_of(head, MIDDLE_WINDOW), distance, valid))
+        return [
+            (high, total, jnp.concatenate([
+                apply(weights[group * stretch : (group + 1) * stretch], rows_of(1, group, at))
+                for group in range(classes)
+            ], axis=0))
+            for at, (high, weights, total) in zip(heads, weighed)
+        ]
+
+    row, column = grid(rows, stretch)
+    apart = class_slot(row) - column
+    join(middle_of(own_rows, apart, apart >= 0), both)
+
+
     def near_rest():
         near_key.wait_recv()
         near_value.wait_recv()
@@ -540,6 +600,38 @@
         distance = apart.astype(jnp.float32)
         join(partial_of(near_low, near_held, near_slopes, distance, valid), 0)
 
+    def near_join():
+        guest_tell.wait_recv()
+        guest_tell_log.wait_recv()
+        row, column = grid(low_rows, HEAD_DIM)
+        parts = []
+        for at in heads:
+            log = jnp.sum(
+                jnp.where(row == column, jnp.broadcast_to(guest_back_log[:, at], (low_rows, HEAD_DIM)), 0.0),
+                axis=-1, keepdims=True,
+            )
+            parts.append((log, jnp.ones_like(log), guest_back[:, at].astype(jnp.float32)))
+        join(parts, 0)
+
+    def near_host():
+        guest_ask.wait_recv()
+        row, column = grid(low_rows, NEAR_WINDOW)
+        apart = scatter_token(low_row(row)) + NEAR_WINDOW - column
+        valid = (apart >= 0) & (apart <= NEAR_WINDOW)
+        distance = apart.astype(jnp.float32)
+        weighed = [
+            weigh(scores_of(guest_query[:, at], near_own[0, near_tail, at]), slope, distance, valid)
+            for at, slope in zip(heads, near_slopes)
+        ]
+        row, column = grid(low_rows, HEAD_DIM)
+        for at, (high, weights, total) in zip(heads, weighed):
+            guest_out[:, at] = apply(weights * (1.0 / total), near_own[1, near_tail, at]).astype(jnp.bfloat16)
+            guest_log[:, at] = jnp.sum(
+                jnp.where(row == column, high + jnp.log(total), 0.0), axis=0, keepdims=True
+            )
+        guest_tell_log.start()
+        guest_tell.start()
+
     @pl.when(odd)
     def _():
         near_rest()
@@ -564,51 +656,65 @@
     of_slot = lane == slot
 
     blocks = ((0, reach), (reach, rows))
-    weighed = []
+
+    def far_part(head, part, first_row, last_row):
+        place = head * 3 + part
+        if place < 2 * local_heads:
+            return first_held[first_row:last_row, place * HEAD_DIM : (place + 1) * HEAD_DIM]
+        return second_held[place - 2 * local_heads, first_row:last_row]
+
+    def second_arrives(piece):
+        far_whole(second_send.at[piece], second_held.at[piece], second_sem.at[piece]).wait_recv()
+
     for head in range(local_heads):
-        at = pl.ds(2 * head * HEAD_DIM, HEAD_DIM)
-        key_at = pl.ds((2 * head + 1) * HEAD_DIM, HEAD_DIM)
+        if head == local_heads - 1:
+            second_arrives(0)
+        parts = []
         for first_row, last_row in blocks:
             row, column = grid(last_row - first_row, last_row)
             apart = row + first_row - column
-            weighed.append(weigh(
-                scores_of(first_held[first_row:last_row, at], first_held[:last_row, key_at]),
+            high, weights, total = weigh(
+                scores_of(far_part(head, 0, first_row, last_row), far_part(head, 1, 0, last_row)),
                 slope_of(head, FAR_WINDOW), (apart * FAR_DILATION).astype(jnp.float32),
                 (apart >= 0) & (apart <= reach),
-            ))
-    packed = []
-    for head in range(local_heads):
-        parts = weighed[head * len(blocks) : (head + 1) * len(blocks)]
-        logs = jnp.concatenate([high + jnp.log(total) for high, _, total in parts], axis=0)
-        packed.append(jnp.sum(
+            )
+            parts.append((high + jnp.log(total), weights * (1.0 / total)))
+        logs = jnp.concatenate([log for log, _ in parts], axis=0)
+        log_send[head] = jnp.sum(
             jnp.where(of_slot, logs, 0.0).reshape(n, chunk, HEAD_DIM), axis=1, keepdims=True
-        ))
-    log_send[...] = jnp.concatenate(packed, axis=2)
-    for head in range(local_heads):
-        parts = weighed[head * len(blocks) : (head + 1) * len(blocks)]
-        for (first_row, last_row), (_, weights, total) in zip(blocks, parts):
-            probs[head, first_row:last_row, :last_row] = (weights * (1.0 / total)).astype(jnp.bfloat16)
-    each(lambda k: log_copy(k).start())
-    log_held[me] = log_send[me]
-
-    far_whole(second_send, second_held, second_sem).wait_recv()
-    for head, at in enumerate(heads):
+        )
+        for (first_row, last_row), (_, shares) in zip(blocks, parts):
+            probs[first_row:last_row, :last_row] = shares.astype(jnp.bfloat16)
+        each(lambda k: log_copy(head, k).start())
+        log_held[head, me] = log_send[head, me]
+        if head == local_heads - 1:
+            second_arrives(1)
         for first_row, last_row in blocks:
-            back_send[first_row:last_row, at] = jnp.dot(
-                probs[head, first_row:last_row, :last_row], second_held[:last_row, at],
+            back_send[head, first_row:last_row] = jnp.dot(
+                probs[first_row:last_row, :last_row], far_part(head, 2, 0, last_row),
                 preferred_element_type=jnp.float32,
             ).astype(jnp.bfloat16)
-    each(lambda k: back_copy(k).start())
-    back_held[at_rows(me), :] = back_send[at_rows(me), :]
+        each(lambda k: back_copy(head, k).start())
+        back_held[head, at_rows(me), :] = back_send[head, at_rows(me), :]
+
+    @pl.when(hosts)
+    def _():
+        near_host()
 
     @pl.when(me >= 1)
     def _():
         value_one.wait_recv()
+
+    @pl.when(relays)
+    def _():
+        relay_value.start()
+
+    @pl.when(me >= 1)
+    def _():
         key_one.wait_recv()
 
     @pl.when(relays)
     def _():
-        relay_value.start()
         relay_key.start()
 
     @pl.when(me >= 2)
@@ -616,44 +722,21 @@
         key_two.wait_recv()
         value_two.wait_recv()
 
-    keys = MIDDLE_WINDOW // classes + stretch
-    row, column = grid(rows, keys)
-    group, index = split_by(row, chunk)
-    apart = index * members + split_by(group, members)[1] + MIDDLE_WINDOW // classes - column
-    valid = (apart >= 0) & (apart <= MIDDLE_WINDOW // classes)
-    valid = valid & (column + me * stretch >= MIDDLE_WINDOW // classes)
-    distance = (apart * classes).astype(jnp.float32)
-
-    def class_rows(part, group, at):
-        of_class = pl.ds(group * stretch, stretch)
-        return jnp.concatenate(
-            (mid_held[0, part, of_class, at], mid_held[1, part, of_class, at], mid_own[part, of_class, at]), axis=0
-        )
-
-    weighed = []
-    for head, at in enumerate(heads):
-        scores = jnp.concatenate([
-            scores_of(mid_query[group * stretch : (group + 1) * stretch, at], class_rows(0, group, at))
-            for group in range(classes)
-        ], axis=0)
-        weighed.append(weigh(scores, slope_of(head, MIDDLE_WINDOW), distance, valid))
-    join([
-        (high, total, jnp.concatenate([
-            apply(weights[group * stretch : (group + 1) * stretch], class_rows(1, group, at))
-            for group in range(classes)
-        ], axis=0))
-        for at, (high, weights, total) in zip(heads, weighed)
-    ], both)
+    reach_slots = MIDDLE_WINDOW // classes
+    row, column = grid(rows, reach_slots)
+    apart = class_slot(row) + reach_slots - column
+    valid = (apart >= 0) & (apart <= reach_slots) & (column + me * stretch >= reach_slots)
+    join(middle_of(held_rows, apart, valid), both)
 
     block = members * part_rows
 
-    def merged_copy(group, side):
+    def merged_copy(head, group, side):
         place = pl.ds(pl.multiple_of(side * low_rows + group * block, block), block)
         return pltpu.make_async_remote_copy(
-            src_ref=merged_own.at[place],
-            dst_ref=merged_held.at[place],
-            send_sem=merged_ssem.at[group, side],
-            recv_sem=merged_rsem.at[group, side],
+            src_ref=merged_own.at[head, place],
+            dst_ref=merged_held.at[head, place],
+            send_sem=merged_sem.at[0],
+            recv_sem=merged_sem.at[1],
             device_id=(me, peer),
             device_id_type=MESH,
         )
@@ -661,84 +744,90 @@
     lane = lax.broadcasted_iota(jnp.int32, (block, HEAD_DIM), 1)
     slot = lax.broadcasted_iota(jnp.int32, (block, HEAD_DIM), 0) & (part_rows - 1)
 
-    def factors(group, side):
+    def factors(head, group, side):
         some = pl.ds(group * members, members)
+        spread = jnp.broadcast_to(
+            log_held[head, some], (members, part_rows, HEAD_DIM)
+        ).reshape(block, HEAD_DIM)
+        far_log = jnp.sum(jnp.where(lane == slot + side * part_rows, spread, 0.0), axis=-1, keepdims=True)
+        pair_log = stats[2 * head, some, side].reshape(block, 1)
+        pair_sum = stats[2 * head + 1, some, side].reshape(block, 1)
+        highest = jnp.maximum(pair_log, far_log)
+        pair_part, far_share = jnp.exp(pair_log - highest), jnp.exp(far_log - highest)
+        mass = pair_sum * pair_part + far_share
+        inverse = 1.0 / mass
+        pair_term = near_sum[head, some, side].reshape(block, HEAD_DIM) * (pair_part * inverse)
+        rest = highest + jnp.log(mass)
         split = jnp.zeros((block, HEAD_DIM), jnp.float32)
-        shares = []
-        held = log_held[some]
-        for head in range(local_heads):
-            spread = jnp.broadcast_to(
-                held[:, :, head * HEAD_DIM : (head + 1) * HEAD_DIM], (members, part_rows, HEAD_DIM)
-            ).reshape(block, HEAD_DIM)
-            far_log = jnp.sum(jnp.where(lane == slot + side * part_rows, spread, 0.0), axis=-1, keepdims=True)
-            pair_log = stats[2 * head, some, side].reshape(block, 1)
-            pair_sum = stats[2 * head + 1, some, side].reshape(block, 1)
-            highest = jnp.maximum(pair_log, far_log)
-            pair_part, far_part = jnp.exp(pair_log - highest), jnp.exp(far_log - highest)
-            mass = pair_sum * pair_part + far_part
-            inverse = 1.0 / mass
-            pair_term = near_sum[head, some, side].reshape(block, HEAD_DIM) * (pair_part * inverse)
-            shares.append((pair_term, far_part * inverse))
-            rest = highest + jnp.log(mass)
-            for term in range(3):
-                piece = rest.astype(jnp.bfloat16).astype(jnp.float32)
-                split = jnp.where(lane == 3 * head + term, piece, split)
-                rest = rest - piece
-        return shares, split
-
-    def merge(group, side, shares, split):
+        for term in range(3):
+            piece = rest.astype(jnp.bfloat16).astype(jnp.float32)
+            split = jnp.where(lane == 3 * head + term, piece, split)
+            rest = rest - piece
+        return pair_term, far_share * inverse, split
+
+    def merge(head, group, side, pair_term, share, split):
         source = pl.ds(pl.multiple_of(group * members * chunk, members * chunk), members * chunk)
         place = pl.ds(pl.multiple_of(side * low_rows + group * block, block), block)
-        merged = []
-        for at, (pair_term, share) in zip(heads, shares):
-            far = back_held[source, at].astype(jnp.float32).reshape(members, 2, part_rows, HEAD_DIM)
-            merged.append((pair_term + far[:, side].reshape(block, HEAD_DIM) * share).astype(jnp.bfloat16))
-        for at, value in zip(heads, merged):
-            merged_own[place, at] = value
-        merged_copy(group, side).start()
-        terms[place] = split.astype(jnp.bfloat16)
+        far = back_held[head, source].astype(jnp.float32).reshape(members, 2, part_rows, HEAD_DIM)
+        merged = pair_term + far[:, side].reshape(block, HEAD_DIM) * share
+        merged_own[head, place] = merged.astype(jnp.bfloat16)
+        merged_copy(head, group, side).start()
+        terms[head, place] = split.astype(jnp.bfloat16)
 
     twin = plane + 1 - 2 * lax.rem(plane, 2)
     below = (1 - upper) * (planes // 2)
     soon = ((plane, members - 1), (twin, members), (below, members))
     late = below + 1
-    waits_near = (lax.rem(me, members) == 0) & (plane == planes // 2)
-
-    @pl.when(jnp.logical_not(waits_near))
-    def _():
-        @pl.when(even & (me >= 1))
-        def _():
-            near_rest()
-
-        for lot in (soon, ((late, members),)):
-            for group, count in lot:
-                log_some(count, group).wait_recv()
-            ready = [[factors(group, side) for side in range(2)] for group, _ in lot]
-            for (group, count), sides in zip(lot, ready):
-                back_some(count, group).wait_recv()
-                for side, held in enumerate(sides):
-                    merge(group, side, *held)
-
-    @pl.when(waits_near)
-    def _():
-        for group, count in soon:
-            log_some(count, group).wait_recv()
-        ready = [factors(group, 1) for group, _ in soon]
-        for (group, count), held in zip(soon, ready):
-            back_some(count, group).wait_recv()
-            merge(group, 1, *held)
-        near_rest()
-        ready = [factors(group, 0) for group, _ in soon]
-        for (group, _), held in zip(soon, ready):
-            merge(group, 0, *held)
-        log_some(members, late).wait_recv()
-        ready = [factors(late, side) for side in range(2)]
-        back_some(members, late).wait_recv()
-        for side, held in enumerate(ready):
-            merge(late, side, *held)
+    def finish(heads_here, lot, sides, arrives):
+        if arrives:
+            for head in heads_here:
+                for group, count in lot:
+                    log_some(head, count, group).wait_recv()
+        ready = [
+            [(head, group, side, factors(head, group, side)) for head in heads_here for side in sides]
+            for group, _ in lot
+        ]
+        for (group, count), held in zip(lot, ready):
+            if arrives:
+                for head in heads_here:
+                    back_some(head, count, group).wait_recv()
+            for head, group, side, values in held:
+                merge(head, group, side, *values)
+
+    late_lot = ((late, members),)
+    every = range(local_heads)
+
+    @pl.when(me < 2)
+    def _():
+        finish((0,), soon + late_lot, (0, 1), True)
+        for head in range(1, local_heads):
+            for one in soon + late_lot:
+                finish((head,), (one,), (0, 1), True)
+
+    @pl.when((upper == 0) & odd & (me >= 2))
+    def _():
+        for head in every:
+            finish((head,), soon + late_lot, (0, 1), True)
+
+    @pl.when((upper == 1) & odd)
+    def _():
+        for head in every:
+            finish((head,), soon, (0, 1), True)
+            finish((head,), late_lot, (0, 1), True)
+
+    @pl.when(guests)
+    def _():
+        for head in every:
+            finish((head,), soon, (1,), True)
+        near_join()
+        finish(every, soon, (0,), False)
+        finish(every, late_lot, (0, 1), True)
 
     lane = lax.broadcasted_iota(jnp.int32, (rows, HEAD_DIM), 1)
-    totals = jnp.dot(to_tokens, terms[...], preferred_element_type=jnp.float32)
+    split = terms[0]
+    for head in range(1, local_heads):
+        split = split + terms[head]
+    totals = jnp.dot(to_tokens, split, preferred_element_type=jnp.float32)
     summed = jnp.zeros((rows, HEAD_DIM), jnp.float32)
     for head in range(local_heads):
         total = jnp.sum(
@@ -748,14 +837,17 @@
     totals_ref[...] = summed
     wo_load.wait()
     partial_ref[...] = jnp.dot(
-        moved(to_tokens, merged_own[...]), wo[pl.ds(pl.multiple_of(tp * width, width), width), :],
+        moved(to_tokens, jnp.concatenate([merged_own[head] for head in range(local_heads)], axis=1)), wo[pl.ds(pl.multiple_of(tp * width, width), width), :],
         preferred_element_type=jnp.float32,
     )
 
     far_whole(first_send, first_held, first_sem).wait_send()
-    far_whole(second_send, second_held, second_sem).wait_send()
-    log_some(n - 1, 0).wait_send()
-    back_some(n - 1, 0).wait_send()
+    for piece in range(2):
+        far_whole(second_send.at[piece], second_held.at[piece], second_sem.at[piece]).wait_send()
+    sent_logs = log_send.at[:, pl.ds(0, n - 1)]
+    pltpu.make_async_copy(sent_logs, sent_logs, log_ssem).wait()
+    sent_back = back_send.at[:, pl.ds(0, rows - chunk)]
+    pltpu.make_async_copy(sent_back, sent_back, back_ssem).wait()
 
     @pl.when(crosses)
     def _():
@@ -772,6 +864,18 @@
     @pl.when(sends_one)
     def _():
         key_one.wait_send()
+
+    @pl.when(hosts)
+    def _():
+        guest_tell.wait_send()
+        guest_tell_log.wait_send()
+
+    @pl.when(guests)
+    def _():
+        guest_ask.wait_send()
+
+    @pl.when(even)
+    def _():
         near_key.wait_send()
         near_value.wait_send()
 
@@ -792,13 +896,9 @@
         relay_key.wait_send()
         relay_value.wait_send()
 
-    for group in range(planes):
-        for side in range(2):
-            merged_copy(group, side).wait_recv()
-    peer_ref[...] = moved(to_tokens, merged_held[...])
-    for group in range(planes):
-        for side in range(2):
-            merged_copy(group, side).wait_send()
+    pltpu.make_async_copy(merged_held, merged_held, merged_sem.at[1]).wait()
+    peer_ref[...] = moved(to_tokens, jnp.concatenate([merged_held[head] for head in range(local_heads)], axis=1))
+    pltpu.make_async_copy(merged_own, merged_own, merged_sem.at[0]).wait()
 
 
 def mix(partial_ref, peer_ref, totals_ref, wo_ref, mixed_ref, log_ref):
@@ -838,13 +938,13 @@
             pltpu.VMEM(out_weight.shape, half),
             pltpu.VMEM((rows, 2 * width), half),
             pltpu.VMEM((rows, 2 * width), half),
-            pltpu.VMEM((rows, width), half),
-            pltpu.VMEM((rows, width), half),
-            pltpu.VMEM((rows, width), half),
-            pltpu.VMEM((rows, width), half),
-            pltpu.VMEM((n, 1, width), full),
-            pltpu.VMEM((n, 1, width), full),
-            pltpu.VMEM((local_heads, rows, rows), half),
+            pltpu.VMEM((local_heads, rows, HEAD_DIM), half),
+            pltpu.VMEM((local_heads, rows, HEAD_DIM), half),
+            pltpu.VMEM((local_heads, rows, HEAD_DIM), half),
+            pltpu.VMEM((local_heads, rows, HEAD_DIM), half),
+            pltpu.VMEM((local_heads, n, 1, HEAD_DIM), full),
+            pltpu.VMEM((local_heads, n, 1, HEAD_DIM), full),
+            pltpu.VMEM((rows, rows), half),
             pltpu.VMEM((rows, width), half),
             pltpu.VMEM((2, rows, width), half),
             pltpu.VMEM((2, 2, rows, width), half),
@@ -853,14 +953,20 @@
             pltpu.VMEM((rows // 2, width), half),
             pltpu.VMEM((2, rows, width), half),
             pltpu.VMEM((2, NEAR_WINDOW, width), half),
+            pltpu.VMEM((rows // 2, width), half),
+            pltpu.VMEM((rows // 2, width), half),
+            pltpu.VMEM((1, width), full),
+            pltpu.VMEM((rows // 2, width), half),
+            pltpu.VMEM((1, width), full),
             pltpu.VMEM((2 * local_heads, n, 2, rows // (2 * n), 1), full),
-            pltpu.VMEM((rows, HEAD_DIM), half),
-            pltpu.VMEM((rows, width), half),
-            pltpu.VMEM((rows, width), half),
+            pltpu.VMEM((local_heads, rows, HEAD_DIM), half),
+            pltpu.VMEM((local_heads, rows, HEAD_DIM), half),
+            pltpu.VMEM((local_heads, rows, HEAD_DIM), half),
             pltpu.VMEM((local_heads, n, 2, rows // (2 * n), HEAD_DIM), full),
-            dma((1 + 9 * local_heads,)), dma((2, 1 + 2 * local_heads)), dma((2,)), dma((2,)),
-            dma(()), dma((planes,)), dma(()), dma((planes,)),
-            dma((4, 2)), dma((2, 2)), dma((1,)), dma((1,)), dma((2,)), dma((2,)), dma((planes, 2)), dma((planes, 2)),
+            dma((9,)), dma((2,)), dma((2, 2)),
+            dma(()), dma((local_heads, planes)), dma(()), dma((local_heads, planes)),
+            dma((7,)), dma((2, 2)), dma(()), dma((2,)), dma((2,)), dma((2,)),
+            dma((2,)),
         ],
         compiler_params=pltpu.CompilerParams(
             collective_id=0, has_side_effects=True, vmem_limit_bytes=53000 * 1024

time: 28.1 us -> 27.6 us (0.982)
  the two profiles are of different devices: /device:TPU:0 before, /device:TPU:16 now
where the time goes in v6:
time: 27.6 us; the launch traced here: 27 us
  Pallas kernels  26.4 us (96%)
  between operations  0.65 us (2%)
    pallas_call x1, Pallas kernels, fused(): pl.pallas_call(functools.partial(kernel, n, local_heads), out_shape=(jax....  25.3 us
    pallas_call x1, Pallas kernels, fused(): pl.pallas_call(mix, out_shape=(jax.ShapeDtypeStruct((rows, out_columns),...  1.11 us

profile of v6, /device:TPU:16, one launch (start us, length us, event | category | flops | bytes accessed | tf_op | source)
XLA Modules:
  0.0 27.0 jit_solution(9653401146218484042)
XLA Ops:
  0.6 0.0 copy-start
  0.6 25.3 %shard_map.68 = (f32[256,1024]{1,0:T(8,128)S(1)}, bf16[256,256]{1,0:T(8,128)(2,1)S(1)}, f32[256,128]{1,0:T(8,128)S(1)}) custom-call(bf16[256,2048]{1,0:T(8,128)(2,1)} %tok_hbm.1, bf16[2048,768]{1,0:T(8,128)(2,1)} %wq_hbm.1, bf16[2048,768]{1,0:T(8,128)(2,1)} %wk_hbm.1, bf16[2048,768]{1,0:T(8,128)(2,1)} %wv_hbm.1, bf16[512,1024]{1,0:T(8,128)(2,1)} %wo_ref.1), custom_call_target="tpu_custom_call" | custom-call | tf_op jit(solution)/shard_map/pallas_call | solution.py:924
  25.9 0.0 copy-done
  25.9 1.1 %shard_map.69 = (bf16[256,1024]{1,0:T(8,128)(2,1)}, f32[2,256]{1,0:T(2,128)}) custom-call(f32[256,1024]{1,0:T(8,128)S(1)} %get-tuple-element.5.partial_ref, bf16[256,256]{1,0:T(8,128)(2,1)S(1)} %get-tuple-element.6.peer_ref, f32[256,128]{1,0:T(8,128)S(1)} %get-tuple-element.7.totals_ref, bf16[512,1024]{1,0:T(8,128)(2,1)S(1)} %copy-done), custom_call_target="tpu_custom_call" | custom-call | tf_op jit(solution)/shard_map/pallas_call | solution.py:975
Async XLA Ops:
  0.6 25.3 %copy-start = (bf16[512,1024]{1,0:T(8,128)(2,1)S(1)}, bf16[512,1024]{1,0:T(8,128)(2,1)}, u32[]{:S(2)}) copy-start(bf16[512,1024]{1,0:T(8,128)(2,1)} %wo_ref.1) | copy-start | bytes 3145732

commit v7 on v6

--- a/solution.py
+++ b/solution.py
@@ -422,6 +422,7 @@
     via_mid = via_copy(mid_own.at[1], via_held)
     onward_even = mid_copy(0, 4, via_held, 1, 3)
     onward_odd = mid_copy(1, 3, via_held, 1, 3)
+    key_pass = mid_copy(0, 1, mid_held.at[1, 0], 0, 0)
     relay_key = mid_copy(0, 1, mid_held.at[1, 0], 0, 2)
     relay_value = mid_copy(0, 1, mid_held.at[1, 1], 1, 2)
 
@@ -476,19 +477,10 @@
     def _():
         guest_ask.start()
 
-    @pl.when(sends_two & stays)
-    def _():
-        value_two.start()
-        key_two.start()
-
     @pl.when(direct)
     def _():
         value_one.start()
         key_one.start()
-
-    @pl.when(crosses & even)
-    def _():
-        key_two.start()
 
     @pl.when(crosses & odd)
     def _():
@@ -636,6 +628,16 @@
     def _():
         near_rest()
 
+    @pl.when(sends_two & stays)
+    def _():
+        value_two.start()
+        key_two.start()
+
+    @pl.when(crosses & odd)
+    def _():
+        key_one.wait_recv()
+        key_pass.start()
+
     @pl.when(forwards)
     def _():
         via_mid.wait_recv()
@@ -709,7 +711,7 @@
     def _():
         relay_value.start()
 
-    @pl.when(me >= 1)
+    @pl.when((me >= 1) & jnp.logical_not(crosses & odd))
     def _():
         key_one.wait_recv()
 
@@ -799,8 +801,7 @@
 
     @pl.when(me < 2)
     def _():
-        finish((0,), soon + late_lot, (0, 1), True)
-        for head in range(1, local_heads):
+        for head in every:
             for one in soon + late_lot:
                 finish((head,), (one,), (0, 1), True)
 
@@ -817,8 +818,7 @@
 
     @pl.when(guests)
     def _():
-        for head in every:
-            finish((head,), soon, (1,), True)
+        finish(every, soon, (1,), True)
         near_join()
         finish(every, soon, (0,), False)
         finish(every, late_lot, (0, 1), True)
@@ -853,7 +853,11 @@
     def _():
         via_mid.wait_send()
 
-    @pl.when(sends_two)
+    @pl.when(crosses & odd)
+    def _():
+        key_pass.wait_send()
+
+    @pl.when(sends_two & stays)
     def _():
         key_two.wait_send()
 

time: 27.6 us -> 27.1 us (0.982); the launches traced: 27 us -> 26.9 us
  no operation moved by 1% of the time
where the time goes in v7:
time: 27.1 us; the launch traced here: 26.9 us
  Pallas kernels  26.3 us (97%)
  between operations  0.65 us (2%)
    pallas_call x1, Pallas kernels, fused(): pl.pallas_call(functools.partial(kernel, n, local_heads), out_shape=(jax....  25.2 us
    pallas_call x1, Pallas kernels, fused(): pl.pallas_call(mix, out_shape=(jax.ShapeDtypeStruct((rows, out_columns),...  1.11 us

profile of v7, /device:TPU:16, one launch (start us, length us, event | category | flops | bytes accessed | tf_op | source)
XLA Modules:
  0.0 26.9 jit_solution(2921738448212729155)
XLA Ops:
  0.6 0.0 copy-start
  0.6 25.2 %shard_map.68 = (f32[256,1024]{1,0:T(8,128)S(1)}, bf16[256,256]{1,0:T(8,128)(2,1)S(1)}, f32[256,128]{1,0:T(8,128)S(1)}) custom-call(bf16[256,2048]{1,0:T(8,128)(2,1)} %tok_hbm.1, bf16[2048,768]{1,0:T(8,128)(2,1)} %wq_hbm.1, bf16[2048,768]{1,0:T(8,128)(2,1)} %wk_hbm.1, bf16[2048,768]{1,0:T(8,128)(2,1)} %wv_hbm.1, bf16[512,1024]{1,0:T(8,128)(2,1)} %wo_ref.1), custom_call_target="tpu_custom_call" | custom-call | tf_op jit(solution)/shard_map/pallas_call | solution.py:928
  25.8 0.0 copy-done
  25.8 1.1 %shard_map.69 = (bf16[256,1024]{1,0:T(8,128)(2,1)}, f32[2,256]{1,0:T(2,128)}) custom-call(f32[256,1024]{1,0:T(8,128)S(1)} %get-tuple-element.5.partial_ref, bf16[256,256]{1,0:T(8,128)(2,1)S(1)} %get-tuple-element.6.peer_ref, f32[256,128]{1,0:T(8,128)S(1)} %get-tuple-element.7.totals_ref, bf16[512,1024]{1,0:T(8,128)(2,1)S(1)} %copy-done), custom_call_target="tpu_custom_call" | custom-call | tf_op jit(solution)/shard_map/pallas_call | solution.py:979
Async XLA Ops:
  0.6 25.2 %copy-start = (bf16[512,1024]{1,0:T(8,128)(2,1)S(1)}, bf16[512,1024]{1,0:T(8,128)(2,1)}, u32[]{:S(2)}) copy-start(bf16[512,1024]{1,0:T(8,128)(2,1)} %wo_ref.1) | copy-start | bytes 3145732

commit v8 on v7

--- a/solution.py
+++ b/solution.py
@@ -231,11 +231,16 @@
 
     barrier = pltpu.get_barrier_semaphore()
 
-    def greet(k, carry):
-        pl.semaphore_signal(barrier, inc=1, device_id=(lax.rem(me + k, n), tp), device_id_type=MESH)
-        return carry
-
-    lax.fori_loop(1, n, greet, 0)
+    upper = me // (n // 2)
+
+    def target_of(k):
+        rising = k - 1 + jnp.where(k - 1 >= me, 1, 0)
+        falling = n - k - jnp.where(n - k <= me, 1, 0)
+        return jnp.where(upper == 1, rising, falling)
+
+
+    for k in range(1, n):
+        pl.semaphore_signal(barrier, inc=1, device_id=(target_of(k), tp), device_id_type=MESH)
     pl.semaphore_signal(barrier, inc=1, device_id=(me, peer), device_id_type=MESH)
     for copy in loads[first:early]:
         copy.start()
@@ -287,14 +292,6 @@
     def each(action):
         for k in range(1, n):
             action(k)
-
-    upper = me // (n // 2)
-
-    def target_of(k):
-        rising = k - 1 + jnp.where(k - 1 >= me, 1, 0)
-        falling = n - k - jnp.where(n - k <= me, 1, 0)
-        return jnp.where(upper == 1, rising, falling)
-
 
     def far_copy(source, target, sem, k):
         to = target_of(k)
@@ -466,10 +463,23 @@
         second_send[head] = pair[:, head * HEAD_DIM : (head + 1) * HEAD_DIM]
     near_query[...] = pair[:, width:]
     near_low[...] = moved(one_hot(rows, low_row)[:low_rows], pair[:, width:])
-    for piece in range(2):
-        each(lambda k: far_copy(
-            second_send.at[piece], second_held.at[piece], second_sem.at[piece], k
-        ).start())
+
+    def send_second(ks):
+        for piece in range(2):
+            for k in ks:
+                far_copy(
+                    second_send.at[piece], second_held.at[piece], second_sem.at[piece], k
+                ).start()
+
+    inner = (plane >= 1) & (plane < planes - 1)
+    outward = range(1, n - members + 1)
+
+    @pl.when(inner)
+    def _():
+        send_second(outward)
+
+    send_second(range(n - members + 1, n))
+
     second_held[:, at_rows(me), :] = second_send[:, at_rows(me), :]
     wo_load.start()
 
@@ -482,7 +492,7 @@
         value_one.start()
         key_one.start()
 
-    @pl.when(crosses & odd)
+    @pl.when(crosses & odd & inner)
     def _():
         key_one.start()
 
@@ -623,6 +633,14 @@
             )
         guest_tell_log.start()
         guest_tell.start()
+
+    @pl.when(jnp.logical_not(inner))
+    def _():
+        send_second(outward)
+
+    @pl.when(crosses & odd & jnp.logical_not(inner))
+    def _():
+        key_one.start()
 
     @pl.when(odd)
     def _():

time: 27.1 us -> 27.1 us (level)
  no operation moved by 1% of the time
where the time goes in v8:
time: 27.1 us; the launch traced here: 26.9 us
  Pallas kernels  26.2 us (97%)
  between operations  0.65 us (2%)
    pallas_call x1, Pallas kernels, fused(): pl.pallas_call(functools.partial(kernel, n, local_heads), out_shape=(jax....  25.1 us
    pallas_call x1, Pallas kernels, fused(): pl.pallas_call(mix, out_shape=(jax.ShapeDtypeStruct((rows, out_columns),...  1.11 us

profile of v8, /device:TPU:16, one launch (start us, length us, event | category | flops | bytes accessed | tf_op | source)
XLA Modules:
  0.0 26.9 jit_solution(356080495220235905)
XLA Ops:
  0.6 0.0 copy-start
  0.6 25.1 %shard_map.68 = (f32[256,1024]{1,0:T(8,128)S(1)}, bf16[256,256]{1,0:T(8,128)(2,1)S(1)}, f32[256,128]{1,0:T(8,128)S(1)}) custom-call(bf16[256,2048]{1,0:T(8,128)(2,1)} %tok_hbm.1, bf16[2048,768]{1,0:T(8,128)(2,1)} %wq_hbm.1, bf16[2048,768]{1,0:T(8,128)(2,1)} %wk_hbm.1, bf16[2048,768]{1,0:T(8,128)(2,1)} %wv_hbm.1, bf16[512,1024]{1,0:T(8,128)(2,1)} %wo_ref.1), custom_call_target="tpu_custom_call" | custom-call | tf_op jit(solution)/shard_map/pallas_call | solution.py:946
  25.8 0.0 copy-done
  25.8 1.1 %shard_map.69 = (bf16[256,1024]{1,0:T(8,128)(2,1)}, f32[2,256]{1,0:T(2,128)}) custom-call(f32[256,1024]{1,0:T(8,128)S(1)} %get-tuple-element.5.partial_ref, bf16[256,256]{1,0:T(8,128)(2,1)S(1)} %get-tuple-element.6.peer_ref, f32[256,128]{1,0:T(8,128)S(1)} %get-tuple-element.7.totals_ref, bf16[512,1024]{1,0:T(8,128)(2,1)S(1)} %copy-done), custom_call_target="tpu_custom_call" | custom-call | tf_op jit(solution)/shard_map/pallas_call | solution.py:997
Async XLA Ops:
  0.6 25.1 %copy-start = (bf16[512,1024]{1,0:T(8,128)(2,1)S(1)}, bf16[512,1024]{1,0:T(8,128)(2,1)}, u32[]{:S(2)}) copy-start(bf16[512,1024]{1,0:T(8,128)(2,1)} %wo_ref.1) | copy-start | bytes 3145732

commit v9 on v7

--- a/solution.py
+++ b/solution.py
@@ -321,8 +321,11 @@
     plane = me // members
     planes = n // members
 
+    def rising(k):
+        return k - 1 + jnp.where(k - 1 >= me, 1, 0)
+
     def back_copy(head, k):
-        to = target_of(k)
+        to = rising(k)
         return pltpu.make_async_remote_copy(
             src_ref=back_send.at[head, at_rows(to)],
             dst_ref=back_held.at[head, at_rows(me)],
@@ -344,7 +347,7 @@
         )
 
     def log_copy(head, k):
-        to = target_of(k)
+        to = rising(k)
         return pltpu.make_async_remote_copy(
             src_ref=log_send.at[head, to],
             dst_ref=log_held.at[head, me],

time: 27.1 us -> 27.1 us (level)
  no operation moved by 1% of the time
where the time goes in v9:
time: 27.1 us; the launch traced here: 26.9 us
  Pallas kernels  26.3 us (97%)
  between operations  0.65 us (2%)
    pallas_call x1, Pallas kernels, fused(): pl.pallas_call(functools.partial(kernel, n, local_heads), out_shape=(jax....  25.2 us
    pallas_call x1, Pallas kernels, fused(): pl.pallas_call(mix, out_shape=(jax.ShapeDtypeStruct((rows, out_columns),...  1.11 us

profile of v9, /device:TPU:16, one launch (start us, length us, event | category | flops | bytes accessed | tf_op | source)
XLA Modules:
  0.0 26.9 jit_solution(15590051479109377808)
XLA Ops:
  0.6 0.0 copy-start
  0.6 25.2 %shard_map.68 = (f32[256,1024]{1,0:T(8,128)S(1)}, bf16[256,256]{1,0:T(8,128)(2,1)S(1)}, f32[256,128]{1,0:T(8,128)S(1)}) custom-call(bf16[256,2048]{1,0:T(8,128)(2,1)} %tok_hbm.1, bf16[2048,768]{1,0:T(8,128)(2,1)} %wq_hbm.1, bf16[2048,768]{1,0:T(8,128)(2,1)} %wk_hbm.1, bf16[2048,768]{1,0:T(8,128)(2,1)} %wv_hbm.1, bf16[512,1024]{1,0:T(8,128)(2,1)} %wo_ref.1), custom_call_target="tpu_custom_call" | custom-call | tf_op jit(solution)/shard_map/pallas_call | solution.py:931
  25.8 0.0 copy-done
  25.8 1.1 %shard_map.69 = (bf16[256,1024]{1,0:T(8,128)(2,1)}, f32[2,256]{1,0:T(2,128)}) custom-call(f32[256,1024]{1,0:T(8,128)S(1)} %get-tuple-element.5.partial_ref, bf16[256,256]{1,0:T(8,128)(2,1)S(1)} %get-tuple-element.6.peer_ref, f32[256,128]{1,0:T(8,128)S(1)} %get-tuple-element.7.totals_ref, bf16[512,1024]{1,0:T(8,128)(2,1)S(1)} %copy-done), custom_call_target="tpu_custom_call" | custom-call | tf_op jit(solution)/shard_map/pallas_call | solution.py:982
Async XLA Ops:
  0.6 25.2 %copy-start = (bf16[512,1024]{1,0:T(8,128)(2,1)S(1)}, bf16[512,1024]{1,0:T(8,128)(2,1)}, u32[]{:S(2)}) copy-start(bf16[512,1024]{1,0:T(8,128)(2,1)} %wo_ref.1) | copy-start | bytes 3145732
